TPU v7x, 512 devices: a whole 4x4x16 slice. The times are simulated.
512 devices in a mesh: vp: 128 (over z, x, core), dp: 4 (over y).
Axes of the slice: x: 4, y: 4, z: 16, core: 2. Of those that a mesh axis runs over, the one named last changes fastest.
Arguments:
- stream: bfloat16 [1024, 2048], P(('dp', 'vp')), may hold values from -60 to 60
- hidden: bfloat16 [1024, 5632], P('dp', 'vp'), may hold values from -6 to 6
- w_down: bfloat16 [5632, 2048], P(None, 'vp'), may hold values from -0.078125 to 0.078125
- final_gain: float32 [2048], replicated, may hold values from 0.1 to 1.9
- vocab: bfloat16 [2048, 32768], P(None, 'vp'), may hold values from -2 to 200
- vocab_bias: float32 [32768], P('vp'), may hold values from -5 to 5
- targets: int32 [1024], P('dp'), may hold values from 0 to 32767
Outputs:
- losses: float32 [1024], P(('dp', 'vp'))
- grad_input: float32 [1024, 2048], P(('dp', 'vp'))
- grad_vocab: float32 [2048, 32768], P('dp', 'vp')
All inputs are finite; a program needn't handle non-finite values.
Results may differ from a plain program's by a relative error of at most 0.02.
Values may be sent and summed in bfloat16 or wider, within the bound.
No kernel may reach another device: no remote copies, remote signals or barrier semaphores. Data moves between devices by JAX's collectives and lax.ppermute only.
A program may use at most 64 MiB of HBM per device.

v0:
```python
import jax
import jax.numpy as jnp
import numpy as np
from jax import lax
from jax.experimental import pallas as pl
from jax.experimental.pallas import tpu as pltpu
from jax.sharding import Mesh
from jax.sharding import PartitionSpec as P


Z, X, C = "vp_0", "vp_1", "vp_2"
Q = ("vp_1", "vp_2")
VP = ("vp_0", "vp_1", "vp_2")
DP_VP = ("dp", "vp_0", "vp_1", "vp_2")

norm_eps = 1e-06
zloss_weight = 0.001
f32 = jnp.float32
bf16 = jnp.bfloat16


def exchange(blocks, axes):
    return lax.all_to_all(blocks, axes, split_axis=0, concat_axis=0, tiled=True)


def shared(block, axes, count):
    return exchange(jnp.broadcast_to(block[None], (count, *block.shape)), axes)


def partner(array, axes, step):
    return lax.ppermute(array, axes, [(k, k ^ step) for k in range(lax.axis_size(axes))])


def dot(a, b, da, db):
    return lax.dot_general(a, b, (((da,), (db,)), ((), ())), preferred_element_type=f32)


def merged(stats):
    top = jnp.max(stats[:, 0], axis=0)
    lse = top + jnp.log(jnp.sum(jnp.exp(stats[:, 0] - top), axis=0))
    return jnp.stack([lse, jnp.sum(stats[:, 1], axis=0)])


def halves(array, core):
    first = lax.dynamic_slice_in_dim(array, core * (array.shape[0] // 2), array.shape[0] // 2)
    other = (1 - core) * (array.shape[0] // 2)
    return first, lax.dynamic_slice_in_dim(array, other, array.shape[0] // 2)


def end_kernel(row_ref, values_ref, gain_ref, out_ref):
    values = values_ref[...]
    inv = lax.rsqrt(jnp.mean(values * values, axis=1, keepdims=True) + norm_eps)
    scaled = jnp.sum(row_ref[...].astype(f32), axis=0) * gain_ref[...]
    mean = jnp.mean(values * scaled, axis=1, keepdims=True)
    out_ref[...] = inv * (scaled - values * inv * inv * mean)


def body(stream, hidden, w_down, final_gain, vocab, vocab_bias, targets):
    nz, nx, nc, ny = (lax.axis_size(a) for a in (Z, X, C, "dp"))
    z, x, c, y = (lax.axis_index(a) for a in (Z, X, C, "dp"))
    nq = nx * nc
    own, width = stream.shape
    group, units = hidden.shape
    cols = w_down.shape[1]
    ncols = vocab.shape[1]
    mine = (z * nx + x) * nc + c
    span = nz * own
    half = nx * span
    feats = nq * cols
    rows = -(-(units + own) // 16) * 16

    order = np.arange(group).reshape(nz, nq, own).transpose(1, 0, 2).reshape(-1)
    order = jnp.asarray(np.eye(group, dtype=np.float32)[order], bf16)
    mine_h = hidden.T
    part = stream.reshape(own, nz, feats).transpose(1, 0, 2)
    part = jnp.pad(part, ((0, 0), (units, rows - units - own), (0, group - feats)))
    mine_h = jnp.pad(mine_h, ((0, rows - units), (0, 0)))
    first = exchange(mine_h[None] + part, Z)

    blocks = w_down.T.reshape(cols, nz, nq, units).transpose(2, 0, 1, 3)
    blocks = jnp.pad(blocks, ((0, 0), (0, 0), (0, 0), (0, rows - units)))
    blocks = blocks.reshape(nx, nc, cols, nz * rows).transpose(1, 0, 2, 3)
    kept, sent = halves(blocks, c)
    came = partner(sent, C, 1)
    pair = jnp.concatenate([jnp.where(c == 0, kept, came), jnp.where(c == 0, came, kept)], axis=0)
    pair = pair.transpose(1, 0, 2, 3)
    w_rows = jnp.zeros_like(pair)
    for step in range(nx):
        block = lax.dynamic_slice_in_dim(pair, x ^ step, 1)
        block = partner(block, X, step) if step else block
        w_rows = lax.dynamic_update_slice_in_dim(w_rows, block, x ^ step, 0)

    sorted_h = dot(order, first.reshape(nz * rows, group), 1, 1).astype(bf16)
    partial = dot(sorted_h, w_rows.reshape(feats, nz * rows), 1, 1)
    proj = jnp.sum(exchange(partial.reshape(nq, span, feats), Q), axis=0)
    first, proj = lax.optimization_barrier((first, proj))
    row_part = first[:, units : units + own, :feats].reshape(span, feats)
    normin = (row_part.astype(f32) + proj).astype(bf16)
    gathered = shared(normin, Z, nz)
    values = gathered.transpose(1, 0, 2).reshape(span, width).astype(f32)
    inv = lax.rsqrt(jnp.mean(values * values, axis=1, keepdims=True) + norm_eps)
    normed = (values * inv * final_gain).astype(bf16)
    normed = shared(normed, X, nx).reshape(half, width)

    vocab = (vocab, partner(vocab, C, 1))
    bias = (vocab_bias, partner(vocab_bias.reshape(2, -1), C, 1).reshape(-1))

    line = lax.broadcasted_iota(jnp.int32, (half, group), 0)
    token = (line // own) % nz * (nq * own) + line // span * (nc * own) + c * own + line % own
    goals = jnp.where(token == lax.broadcasted_iota(jnp.int32, (half, group), 1), targets[None, :], 0)
    goals = jnp.sum(goals, axis=1)
    ids = lax.broadcasted_iota(jnp.int32, (half, ncols), 1)
    hit = [ids + k * ncols == goals[:, None] for k in (mine, mine ^ 1)]
    feat_group, last = width // ny, ny - 1
    early = lax.dynamic_slice_in_dim(normed, (y ^ last) * feat_group, feat_group, 1)
    early = partner(early, "dp", last)

    scores = [dot(normed, v, 1, 0) + b for v, b in zip(vocab, bias)]
    top = jnp.maximum(jnp.max(scores[0], axis=1), jnp.max(scores[1], axis=1))
    total = sum(jnp.sum(jnp.exp(s - top[:, None]), axis=1) for s in scores)
    goal = sum(jnp.sum(jnp.where(h, s, 0.0), axis=1) for h, s in zip(hit, scores))
    stats = jnp.stack([top + jnp.log(total), goal])
    stats = merged(shared(stats, X, nx))
    stats = merged(shared(stats, Z, nz))
    lse, goal = stats
    losses = lse - goal + zloss_weight * lse * lse
    losses = lax.dynamic_slice_in_dim(losses, x * span + z * own, own)
    scale = 1.0 + 2.0 * zloss_weight * lse
    dscore = [
        (jnp.exp(s - lse[:, None]) * scale[:, None] - jnp.where(h, 1.0, 0.0)).astype(bf16)
        for s, h in zip(scores, hit)
    ]
    row_term = sum(dot(d, v, 1, 1) for d, v in zip(dscore, vocab)).astype(bf16)

    row_term, *dscore = lax.optimization_barrier((row_term, *dscore))
    theirs, ours = 0.0, 0.0
    for step in (0, ny // 2, 1, last):
        cols_of = jnp.concatenate(dscore, axis=1)
        if step == last:
            piece, cols_of = early, partner(cols_of, "dp", step)
        else:
            piece = lax.dynamic_slice_in_dim(normed, (y ^ step) * feat_group, feat_group, 1)
            if step:
                piece = partner(jnp.concatenate([piece, cols_of], axis=1), "dp", step)
                piece, cols_of = piece[:, :feat_group], piece[:, feat_group:]
        theirs = theirs + dot(piece, cols_of[:, ncols:], 0, 0)
        ours = ours + dot(piece, cols_of[:, :ncols], 0, 0)
    grad_vocab = lax.optimization_barrier(ours) + partner(theirs, C, 1)

    row_x = exchange(row_term.reshape(nx, span, width), X)
    row_x = jnp.sum(row_x.astype(f32), axis=0).astype(bf16)
    row_z = exchange(row_x.reshape(nz, own, width), Z)
    gathered, _ = lax.optimization_barrier((gathered, row_x))
    normin = lax.dynamic_slice_in_dim(gathered, z * own, own, 1).transpose(1, 0, 2).reshape(own, width)
    grad_input = pl.pallas_call(
        end_kernel,
        out_shape=jax.ShapeDtypeStruct((own, width), f32),
        in_specs=[pl.BlockSpec(memory_space=pltpu.VMEM)] * 3,
        out_specs=pl.BlockSpec(memory_space=pltpu.VMEM),
        compiler_params=pltpu.CompilerParams(vmem_limit_bytes=4 << 20),
    )(row_z, normin.astype(f32), final_gain[None])
    return (losses, grad_input, grad_vocab)


def solution(mesh):
    torus = Mesh(mesh.devices.reshape(16, 4, 2, mesh.shape["dp"]), ("vp_0", "vp_1", "vp_2", "dp"))
    return jax.shard_map(
        body,
        mesh=torus,
        in_specs=(P(DP_VP, None), P("dp", VP), P(None, VP), P(), P(None, VP), P(VP), P("dp")),
        out_specs=(P(DP_VP), P(DP_VP, None), P("dp", VP)),
        check_vma=False,
    )
```

profile of v0, /device:TPU:34, one launch (start us, length us, event | category | flops | bytes accessed | tf_op | source)
XLA Modules:
  0.0 161.0 jit_solution(14879713805213764288)
XLA Ops:
  2.2 15.3 %all-to-all-start = ((bf16[16,48,256]{2,1,0:T(8,128)(2,1)}), bf16[16,48,256]{2,1,0:T(8,128)(2,1)S(1)}, u32[]{:S(2)}, u32[]{:S(2)}) async-start(bf16[16,48,256]{2,1,0:T(8,128)(2,1)} %pad_add_fusion), calls=%async_computation | async-start | bytes 786432 | tf_op jit(solution)/shard_map/all_to_all | solution.py:23
  17.5 1.5 reshape.182
  19.7 1.9 %collective-permute-start = (bf16[1,4,16,768]{3,2,1,0:T(8,128)(2,1)S(1)}, bf16[1,4,16,768]{3,2,1,0:T(8,128)(2,1)S(1)}, u32[]{:S(2)}, u32[]{:S(2)}) collective-permute-start(bf16[1,4,16,768]{3,2,1,0:T(8,128)(2,1)S(1)} %dynamic-slice_bitcast_fusion), channel_id=1, source_target_pairs={{0,4},{4,0},{1,5},{5,1},{2,6},{6,2},{3,7},{7,3},{8,12},{12,8},{9,1... | collective-permute-start | bytes 294920 | tf_op jit(solution)/shard_map/ppermute | solution.py:31
  21.7 1.2 collective-permute-done
  23.0 2.4 %collective-permute-start.1 = (bf16[1,2,16,768]{3,2,1,0:T(8,128)(2,1)S(1)}, bf16[1,2,16,768]{3,2,1,0:T(8,128)(2,1)S(1)}, u32[]{:S(2)}, u32[]{:S(2)}) collective-permute-start(bf16[1,2,16,768]{3,2,1,0:T(8,128)(2,1)S(1)} %get-tuple-element.29), channel_id=1, source_target_pairs={{0,8},{8,0},{16,24},{24,16},{1,9},{9,1},{17,25},{25,17},{2,10},{10... | collective-permute-start | bytes 147464 | tf_op jit(solution)/shard_map/ppermute | solution.py:31
  25.4 4.3 %collective-permute-start.2 = (bf16[1,2,16,768]{3,2,1,0:T(8,128)(2,1)S(1)}, bf16[1,2,16,768]{3,2,1,0:T(8,128)(2,1)S(1)}, u32[]{:S(2)}, u32[]{:S(2)}) collective-permute-start(bf16[1,2,16,768]{3,2,1,0:T(8,128)(2,1)S(1)} %get-tuple-element.30), channel_id=1, source_target_pairs={{0,16},{8,24},{16,0},{24,8},{1,17},{9,25},{17,1},{25,9},{2,18},{10... | collective-permute-start | bytes 147464 | tf_op jit(solution)/shard_map/ppermute | solution.py:31
  29.7 2.4 %collective-permute-start.3 = (bf16[1,2,16,768]{3,2,1,0:T(8,128)(2,1)S(1)}, bf16[1,2,16,768]{3,2,1,0:T(8,128)(2,1)S(1)}, u32[]{:S(2)}, u32[]{:S(2)}) collective-permute-start(bf16[1,2,16,768]{3,2,1,0:T(8,128)(2,1)S(1)} %get-tuple-element.28), channel_id=1, source_target_pairs={{0,24},{8,16},{16,8},{24,0},{1,25},{9,17},{17,9},{25,1},{2,26},{10... | collective-permute-start | bytes 147464 | tf_op jit(solution)/shard_map/ppermute | solution.py:31
  32.9 2.8 %collective-permute-done.3 = bf16[1,2,16,768]{3,2,1,0:T(8,128)(2,1)S(1)} collective-permute-done((bf16[1,2,16,768]{3,2,1,0:T(8,128)(2,1)S(1)}, bf16[1,2,16,768]{3,2,1,0:T(8,128)(2,1)S(1)}, u32[]{:S(2)}, u32[]{:S(2)}) %collective-permute-start.3) | collective-permute-done | bytes 49184 | tf_op jit(solution)/shard_map/ppermute | solution.py:31
  35.7 3.6 %all-to-all-done = bf16[16,48,256]{2,1,0:T(8,128)(2,1)S(1)} async-done(((bf16[16,48,256]{2,1,0:T(8,128)(2,1)}), bf16[16,48,256]{2,1,0:T(8,128)(2,1)S(1)}, u32[]{:S(2)}, u32[]{:S(2)}) %all-to-all-start) | async-done | bytes 393248 | tf_op jit(solution)/shard_map/all_to_all | solution.py:23
  39.9 9.3 %all_to_all.40 = f32[8,32,128]{2,1,0:T(8,128)S(1)} all-to-all(f32[8,32,128]{2,1,0:T(8,128)S(1)} %fusion.51), channel_id=1, replica_groups=mesh['vp_0'=16,'vp_1'=4,'vp_2'=2,'dp'=4] {'vp_1','vp_2'}, dimensions={0} | all-to-all | bytes 262144 | tf_op jit(solution)/shard_map/all_to_all | solution.py:23
  49.9 9.2 %all-to-all-start.2 = ((bf16[16,32,128]{2,1,0:T(8,128)(2,1)}), bf16[16,32,128]{2,1,0:T(8,128)(2,1)S(1)}, u32[]{:S(2)}, u32[]{:S(2)}) async-start(bf16[16,32,128]{2,1,0:T(8,128)(2,1)} %broadcast_in_dim.34), calls=%async_computation.2 | async-start | bytes 262144 | tf_op jit(solution)/shard_map/all_to_all | solution.py:23
  59.8 1.9 %collective-permute-start.5 = (f32[2,128]{1,0:T(2,128)S(1)}, f32[2,128]{1,0:T(2,128)S(1)}, u32[]{:S(2)}, u32[]{:S(2)}) collective-permute-start(f32[2,128]{1,0:T(2,128)S(1)} %bitcast.103), channel_id=1, source_target_pairs={{0,4},{4,0},{1,5},{5,1},{2,6},{6,2},{3,7},{7,3},{8,12},{12,8},{9,1... | collective-permute-start | bytes 3080 | tf_op jit(solution)/shard_map/ppermute | solution.py:31
  61.7 2.4 %collective-permute-start.4 = (bf16[2048,256]{1,0:T(8,128)(2,1)S(1)}, bf16[2048,256]{1,0:T(8,128)(2,1)S(1)}, u32[]{:S(2)}, u32[]{:S(2)}) collective-permute-start(bf16[2048,256]{1,0:T(8,128)(2,1)S(1)} %copy-done.1), channel_id=1, source_target_pairs={{0,4},{4,0},{1,5},{5,1},{2,6},{6,2},{3,7},{7,3},{8,12},{12,8},{9,1... | collective-permute-start | bytes 3145736 | tf_op jit(solution)/shard_map/ppermute | solution.py:31
  64.2 8.8 %all-to-all-done.2 = bf16[16,32,128]{2,1,0:T(8,128)(2,1)S(1)} async-done(((bf16[16,32,128]{2,1,0:T(8,128)(2,1)}), bf16[16,32,128]{2,1,0:T(8,128)(2,1)S(1)}, u32[]{:S(2)}, u32[]{:S(2)}) %all-to-all-start.2) | async-done | bytes 131104 | tf_op jit(solution)/shard_map/all_to_all | solution.py:23
  74.1 4.9 %all-to-all-start.3 = ((bf16[4,32,2048]{2,1,0:T(8,128)(2,1)}), bf16[4,32,2048]{2,1,0:T(8,128)(2,1)S(1)}, u32[]{:S(2)}, u32[]{:S(2)}) async-start(bf16[4,32,2048]{2,1,0:T(8,128)(2,1)} %broadcast_in_dim.35), calls=%async_computation.3 | async-start | bytes 1048576 | tf_op jit(solution)/shard_map/all_to_all | solution.py:23
  80.0 5.6 %all-to-all-done.3 = bf16[4,32,2048]{2,1,0:T(8,128)(2,1)S(1)} async-done(((bf16[4,32,2048]{2,1,0:T(8,128)(2,1)}), bf16[4,32,2048]{2,1,0:T(8,128)(2,1)S(1)}, u32[]{:S(2)}, u32[]{:S(2)}) %all-to-all-start.3) | async-done | bytes 524320 | tf_op jit(solution)/shard_map/all_to_all | solution.py:23
  87.4 4.7 %all-to-all-start.4 = ((f32[4,2,128]{2,1,0:T(2,128)}), f32[4,2,128]{2,1,0:T(2,128)S(1)}, u32[]{:S(2)}, u32[]{:S(2)}) async-start(f32[4,2,128]{2,1,0:T(2,128)} %broadcast_in_dim.38), calls=%async_computation.4 | async-start | bytes 8192 | tf_op jit(solution)/shard_map/all_to_all | solution.py:23
  92.0 3.8 %all-to-all-done.4 = f32[4,2,128]{2,1,0:T(2,128)S(1)} async-done(((f32[4,2,128]{2,1,0:T(2,128)}), f32[4,2,128]{2,1,0:T(2,128)S(1)}, u32[]{:S(2)}, u32[]{:S(2)}) %all-to-all-start.4) | async-done | bytes 4128 | tf_op jit(solution)/shard_map/all_to_all | solution.py:23
  96.6 5.6 %all-to-all-start.5 = ((f32[16,2,128]{2,1,0:T(2,128)}), f32[16,2,128]{2,1,0:T(2,128)S(1)}, u32[]{:S(2)}, u32[]{:S(2)}) async-start(f32[16,2,128]{2,1,0:T(2,128)} %broadcast_in_dim.39), calls=%async_computation.5 | async-start | bytes 32768 | tf_op jit(solution)/shard_map/all_to_all | solution.py:23
  102.8 4.9 %collective-permute-start.8 = (bf16[128,512]{1,0:T(8,128)(2,1)}, bf16[128,512]{1,0:T(8,128)(2,1)}, u32[]{:S(2)}, u32[]{:S(2)}) collective-permute-start(bf16[128,512]{1,0:T(8,128)(2,1)} %get-tuple-element.24), channel_id=1, source_target_pairs={{0,3},{1,2},{2,1},{3,0},{4,7},{5,6},{6,5},{7,4},{8,11},{9,10},{10,... | collective-permute-start | bytes 393224 | tf_op jit(solution)/shard_map/ppermute | solution.py:31
  107.8 5.7 %all-to-all-done.5 = f32[16,2,128]{2,1,0:T(2,128)S(1)} async-done(((f32[16,2,128]{2,1,0:T(2,128)}), f32[16,2,128]{2,1,0:T(2,128)S(1)}, u32[]{:S(2)}, u32[]{:S(2)}) %all-to-all-start.5) | async-done | bytes 16416 | tf_op jit(solution)/shard_map/all_to_all | solution.py:23
  114.2 1.3 fusion
  115.4 4.9 %all-to-all-start.6 = ((bf16[4,32,2048]{2,1,0:T(8,128)(2,1)}), bf16[4,32,2048]{2,1,0:T(8,128)(2,1)S(1)}, u32[]{:S(2)}, u32[]{:S(2)}) async-start(bf16[4,32,2048]{2,1,0:T(8,128)(2,1)} %bitcast.31), calls=%async_computation.6 | async-start | bytes 1048576 | tf_op jit(solution)/shard_map/all_to_all | solution.py:23
  120.4 4.9 %collective-permute-start.9 = (bf16[128,512]{1,0:T(8,128)(2,1)S(1)}, bf16[128,512]{1,0:T(8,128)(2,1)S(1)}, u32[]{:S(2)}, u32[]{:S(2)}) collective-permute-start(bf16[128,512]{1,0:T(8,128)(2,1)S(1)} %pad_maximum_fusion.4), channel_id=1, source_target_pairs={{0,3},{1,2},{2,1},{3,0},{4,7},{5,6},{6,5},{7,4},{8,11},{9,10},{10,... | collective-permute-start | bytes 393224 | tf_op jit(solution)/shard_map/ppermute | solution.py:31
  125.6 2.5 %collective-permute-start.6 = (bf16[128,1024]{1,0:T(8,128)(2,1)S(1)}, bf16[128,1024]{1,0:T(8,128)(2,1)S(1)}, u32[]{:S(2)}, u32[]{:S(2)}) collective-permute-start(bf16[128,1024]{1,0:T(8,128)(2,1)S(1)} %get-tuple-element.32), channel_id=1, source_target_pairs={{0,2},{1,3},{2,0},{3,1},{4,6},{5,7},{6,4},{7,5},{8,10},{9,11},{10,... | collective-permute-start | bytes 786440 | tf_op jit(solution)/shard_map/ppermute | solution.py:31
  128.1 2.4 %collective-permute-start.7 = (bf16[128,1024]{1,0:T(8,128)(2,1)S(1)}, bf16[128,1024]{1,0:T(8,128)(2,1)S(1)}, u32[]{:S(2)}, u32[]{:S(2)}) collective-permute-start(bf16[128,1024]{1,0:T(8,128)(2,1)S(1)} %get-tuple-element.31), channel_id=1, source_target_pairs={{0,1},{1,0},{2,3},{3,2},{4,5},{5,4},{6,7},{7,6},{8,9},{9,8},{10,11... | collective-permute-start | bytes 786440 | tf_op jit(solution)/shard_map/ppermute | solution.py:31
  131.4 1.1 fusion.30
  132.5 1.1 fusion.26
  133.7 1.7 %collective-permute-done.6 = bf16[128,1024]{1,0:T(8,128)(2,1)S(1)} collective-permute-done((bf16[128,1024]{1,0:T(8,128)(2,1)S(1)}, bf16[128,1024]{1,0:T(8,128)(2,1)S(1)}, u32[]{:S(2)}, u32[]{:S(2)}) %collective-permute-start.6) | collective-permute-done | bytes 262176 | tf_op jit(solution)/shard_map/ppermute | solution.py:31
  136.7 1.9 %collective-permute-start.10 = (f32[512,256]{1,0:T(8,128)S(1)}, f32[512,256]{1,0:T(8,128)S(1)}, u32[]{:S(2)}, u32[]{:S(2)}) collective-permute-start(f32[512,256]{1,0:T(8,128)S(1)} %fusion.2), channel_id=1, source_target_pairs={{0,4},{4,0},{1,5},{5,1},{2,6},{6,2},{3,7},{7,3},{8,12},{12,8},{9,1... | collective-permute-start | bytes 1572872 | tf_op jit(solution)/shard_map/ppermute | solution.py:31
  139.7 6.0 %all-to-all-start.7 = ((bf16[16,2,2048]{2,1,0:T(2,128)(2,1)}), bf16[16,2,2048]{2,1,0:T(2,128)(2,1)S(1)}, u32[]{:S(2)}, u32[]{:S(2)}) async-start(bf16[16,2,2048]{2,1,0:T(2,128)(2,1)} %reshape.188), calls=%async_computation.7 | async-start | bytes 262144 | tf_op jit(solution)/shard_map/all_to_all | solution.py:23
  146.8 13.3 %all-to-all-done.7.row_ref = bf16[16,2,2048]{2,1,0:T(2,128)(2,1)S(1)} async-done(((bf16[16,2,2048]{2,1,0:T(2,128)(2,1)}), bf16[16,2,2048]{2,1,0:T(2,128)(2,1)S(1)}, u32[]{:S(2)}, u32[]{:S(2)}) %all-to-all-start.7) | async-done | bytes 131104 | tf_op jit(solution)/shard_map/all_to_all | solution.py:23
  (91 shorter events, 16.2 us)
Async XLA Ops:
  0.6 0.8 copy-start.4
  2.2 15.3 %copy-start.2 = (bf16[5632,16]{0,1:T(8,128)(2,1)S(1)}, bf16[5632,16]{0,1:T(8,128)(2,1)}, u32[]{:S(2)}) copy-start(bf16[5632,16]{0,1:T(8,128)(2,1)} %param.10) | copy-start | bytes 540676
  2.2 37.2 %all-to-all-start = ((bf16[16,48,256]{2,1,0:T(8,128)(2,1)}), bf16[16,48,256]{2,1,0:T(8,128)(2,1)S(1)}, u32[]{:S(2)}, u32[]{:S(2)}) async-start(bf16[16,48,256]{2,1,0:T(8,128)(2,1)} %pad_add_fusion), calls=%async_computation | async-start | bytes 786432 | tf_op jit(solution)/shard_map/all_to_all | solution.py:23
  19.7 3.2 %collective-permute-start = (bf16[1,4,16,768]{3,2,1,0:T(8,128)(2,1)S(1)}, bf16[1,4,16,768]{3,2,1,0:T(8,128)(2,1)S(1)}, u32[]{:S(2)}, u32[]{:S(2)}) collective-permute-start(bf16[1,4,16,768]{3,2,1,0:T(8,128)(2,1)S(1)} %dynamic-slice_bitcast_fusion), channel_id=1, source_target_pairs={{0,4},{4,0},{1,5},{5,1},{2,6},{6,2},{3,7},{7,3},{8,12},{12,8},{9,1... | collective-permute-start | bytes 294920 | tf_op jit(solution)/shard_map/ppermute | solution.py:31
  23.0 9.3 %collective-permute-start.1 = (bf16[1,2,16,768]{3,2,1,0:T(8,128)(2,1)S(1)}, bf16[1,2,16,768]{3,2,1,0:T(8,128)(2,1)S(1)}, u32[]{:S(2)}, u32[]{:S(2)}) collective-permute-start(bf16[1,2,16,768]{3,2,1,0:T(8,128)(2,1)S(1)} %get-tuple-element.29), channel_id=1, source_target_pairs={{0,8},{8,0},{16,24},{24,16},{1,9},{9,1},{17,25},{25,17},{2,10},{10... | collective-permute-start | bytes 147464 | tf_op jit(solution)/shard_map/ppermute | solution.py:31
  25.4 7.5 %collective-permute-start.2 = (bf16[1,2,16,768]{3,2,1,0:T(8,128)(2,1)S(1)}, bf16[1,2,16,768]{3,2,1,0:T(8,128)(2,1)S(1)}, u32[]{:S(2)}, u32[]{:S(2)}) collective-permute-start(bf16[1,2,16,768]{3,2,1,0:T(8,128)(2,1)S(1)} %get-tuple-element.30), channel_id=1, source_target_pairs={{0,16},{8,24},{16,0},{24,8},{1,17},{9,25},{17,1},{25,9},{2,18},{10... | collective-permute-start | bytes 147464 | tf_op jit(solution)/shard_map/ppermute | solution.py:31
  29.7 6.0 %collective-permute-start.3 = (bf16[1,2,16,768]{3,2,1,0:T(8,128)(2,1)S(1)}, bf16[1,2,16,768]{3,2,1,0:T(8,128)(2,1)S(1)}, u32[]{:S(2)}, u32[]{:S(2)}) collective-permute-start(bf16[1,2,16,768]{3,2,1,0:T(8,128)(2,1)S(1)} %get-tuple-element.28), channel_id=1, source_target_pairs={{0,24},{8,16},{16,8},{24,0},{1,25},{9,17},{17,9},{25,1},{2,26},{10... | collective-permute-start | bytes 147464 | tf_op jit(solution)/shard_map/ppermute | solution.py:31
  32.2 7.1 %copy-start.3 = (bf16[256,256]{1,0:T(8,128)(2,1)S(1)}, bf16[256,256]{1,0:T(8,128)(2,1)}, u32[]{:S(2)}) copy-start(bf16[256,256]{1,0:T(8,128)(2,1)} %constant.113.clone) | copy-start | bytes 393220
  39.3 22.4 %copy-start.1 = (bf16[2048,256]{1,0:T(8,128)(2,1)S(1)}, bf16[2048,256]{1,0:T(8,128)(2,1)}, u32[]{:S(2)}) copy-start(bf16[2048,256]{1,0:T(8,128)(2,1)} %param.12) | copy-start | bytes 3145732
  49.9 23.1 %all-to-all-start.2 = ((bf16[16,32,128]{2,1,0:T(8,128)(2,1)}), bf16[16,32,128]{2,1,0:T(8,128)(2,1)S(1)}, u32[]{:S(2)}, u32[]{:S(2)}) async-start(bf16[16,32,128]{2,1,0:T(8,128)(2,1)} %broadcast_in_dim.34), calls=%async_computation.2 | async-start | bytes 262144 | tf_op jit(solution)/shard_map/all_to_all | solution.py:23
  59.1 0.7 copy-start.6
  59.8 26.2 %collective-permute-start.5 = (f32[2,128]{1,0:T(2,128)S(1)}, f32[2,128]{1,0:T(2,128)S(1)}, u32[]{:S(2)}, u32[]{:S(2)}) collective-permute-start(f32[2,128]{1,0:T(2,128)S(1)} %bitcast.103), channel_id=1, source_target_pairs={{0,4},{4,0},{1,5},{5,1},{2,6},{6,2},{3,7},{7,3},{8,12},{12,8},{9,1... | collective-permute-start | bytes 3080 | tf_op jit(solution)/shard_map/ppermute | solution.py:31
  61.7 24.3 %collective-permute-start.4 = (bf16[2048,256]{1,0:T(8,128)(2,1)S(1)}, bf16[2048,256]{1,0:T(8,128)(2,1)S(1)}, u32[]{:S(2)}, u32[]{:S(2)}) collective-permute-start(bf16[2048,256]{1,0:T(8,128)(2,1)S(1)} %copy-done.1), channel_id=1, source_target_pairs={{0,4},{4,0},{1,5},{5,1},{2,6},{6,2},{3,7},{7,3},{8,12},{12,8},{9,1... | collective-permute-start | bytes 3145736 | tf_op jit(solution)/shard_map/ppermute | solution.py:31
  64.2 9.0 %copy-start = (f32[2048]{0:T(1024)S(1)}, f32[2048]{0:T(1024)}, u32[]{:S(2)}) copy-start(f32[2048]{0:T(1024)} %param.11) | copy-start | bytes 24580
  74.1 11.5 %all-to-all-start.3 = ((bf16[4,32,2048]{2,1,0:T(8,128)(2,1)}), bf16[4,32,2048]{2,1,0:T(8,128)(2,1)S(1)}, u32[]{:S(2)}, u32[]{:S(2)}) async-start(bf16[4,32,2048]{2,1,0:T(8,128)(2,1)} %broadcast_in_dim.35), calls=%async_computation.3 | async-start | bytes 1048576 | tf_op jit(solution)/shard_map/all_to_all | solution.py:23
  79.1 0.7 copy-start.5
  87.4 8.5 %all-to-all-start.4 = ((f32[4,2,128]{2,1,0:T(2,128)}), f32[4,2,128]{2,1,0:T(2,128)S(1)}, u32[]{:S(2)}, u32[]{:S(2)}) async-start(f32[4,2,128]{2,1,0:T(2,128)} %broadcast_in_dim.38), calls=%async_computation.4 | async-start | bytes 8192 | tf_op jit(solution)/shard_map/all_to_all | solution.py:23
  96.6 16.8 %all-to-all-start.5 = ((f32[16,2,128]{2,1,0:T(2,128)}), f32[16,2,128]{2,1,0:T(2,128)S(1)}, u32[]{:S(2)}, u32[]{:S(2)}) async-start(f32[16,2,128]{2,1,0:T(2,128)} %broadcast_in_dim.39), calls=%async_computation.5 | async-start | bytes 32768 | tf_op jit(solution)/shard_map/all_to_all | solution.py:23
  102.8 28.5 %collective-permute-start.8 = (bf16[128,512]{1,0:T(8,128)(2,1)}, bf16[128,512]{1,0:T(8,128)(2,1)}, u32[]{:S(2)}, u32[]{:S(2)}) collective-permute-start(bf16[128,512]{1,0:T(8,128)(2,1)} %get-tuple-element.24), channel_id=1, source_target_pairs={{0,3},{1,2},{2,1},{3,0},{4,7},{5,6},{6,5},{7,4},{8,11},{9,10},{10,... | collective-permute-start | bytes 393224 | tf_op jit(solution)/shard_map/ppermute | solution.py:31
  115.4 23.4 %all-to-all-start.6 = ((bf16[4,32,2048]{2,1,0:T(8,128)(2,1)}), bf16[4,32,2048]{2,1,0:T(8,128)(2,1)S(1)}, u32[]{:S(2)}, u32[]{:S(2)}) async-start(bf16[4,32,2048]{2,1,0:T(8,128)(2,1)} %bitcast.31), calls=%async_computation.6 | async-start | bytes 1048576 | tf_op jit(solution)/shard_map/all_to_all | solution.py:23
  120.4 11.0 %collective-permute-start.9 = (bf16[128,512]{1,0:T(8,128)(2,1)S(1)}, bf16[128,512]{1,0:T(8,128)(2,1)S(1)}, u32[]{:S(2)}, u32[]{:S(2)}) collective-permute-start(bf16[128,512]{1,0:T(8,128)(2,1)S(1)} %pad_maximum_fusion.4), channel_id=1, source_target_pairs={{0,3},{1,2},{2,1},{3,0},{4,7},{5,6},{6,5},{7,4},{8,11},{9,10},{10,... | collective-permute-start | bytes 393224 | tf_op jit(solution)/shard_map/ppermute | solution.py:31
  125.6 9.8 %collective-permute-start.6 = (bf16[128,1024]{1,0:T(8,128)(2,1)S(1)}, bf16[128,1024]{1,0:T(8,128)(2,1)S(1)}, u32[]{:S(2)}, u32[]{:S(2)}) collective-permute-start(bf16[128,1024]{1,0:T(8,128)(2,1)S(1)} %get-tuple-element.32), channel_id=1, source_target_pairs={{0,2},{1,3},{2,0},{3,1},{4,6},{5,7},{6,4},{7,5},{8,10},{9,11},{10,... | collective-permute-start | bytes 786440 | tf_op jit(solution)/shard_map/ppermute | solution.py:31
  128.1 8.3 %collective-permute-start.7 = (bf16[128,1024]{1,0:T(8,128)(2,1)S(1)}, bf16[128,1024]{1,0:T(8,128)(2,1)S(1)}, u32[]{:S(2)}, u32[]{:S(2)}) collective-permute-start(bf16[128,1024]{1,0:T(8,128)(2,1)S(1)} %get-tuple-element.31), channel_id=1, source_target_pairs={{0,1},{1,0},{2,3},{3,2},{4,5},{5,4},{6,7},{7,6},{8,9},{9,8},{10,11... | collective-permute-start | bytes 786440 | tf_op jit(solution)/shard_map/ppermute | solution.py:31
  136.7 9.3 %collective-permute-start.10 = (f32[512,256]{1,0:T(8,128)S(1)}, f32[512,256]{1,0:T(8,128)S(1)}, u32[]{:S(2)}, u32[]{:S(2)}) collective-permute-start(f32[512,256]{1,0:T(8,128)S(1)} %fusion.2), channel_id=1, source_target_pairs={{0,4},{4,0},{1,5},{5,1},{2,6},{6,2},{3,7},{7,3},{8,12},{12,8},{9,1... | collective-permute-start | bytes 1572872 | tf_op jit(solution)/shard_map/ppermute | solution.py:31
  139.7 20.4 %all-to-all-start.7 = ((bf16[16,2,2048]{2,1,0:T(2,128)(2,1)}), bf16[16,2,2048]{2,1,0:T(2,128)(2,1)S(1)}, u32[]{:S(2)}, u32[]{:S(2)}) async-start(bf16[16,2,2048]{2,1,0:T(2,128)(2,1)} %reshape.188), calls=%async_computation.7 | async-start | bytes 262144 | tf_op jit(solution)/shard_map/all_to_all | solution.py:23
where the time goes:
time: 162 us; the launch traced here: 161 us
  starting transfers between devices  82.7 us (51%)
  waiting for transfers between devices  48 us (30%)
  blocking collectives  9.27 us (6%)
  local copies, waits for them, and re-layouts  9.09 us (6%)
  matrix products  6.89 us (4%)
  other arithmetic  3.01 us (2%)
    all_to_all x7, starting transfers between devices, exchange(): return lax.all_to_all(blocks, axes, split_axis=0, concat_axis=0, tiled=True)  50.6 us
    all_to_all x7, waiting for transfers between devices, exchange(): return lax.all_to_all(blocks, axes, split_axis=0, concat_axis=0, tiled=True)  40.9 us
    ppermute x11, starting transfers between devices, partner(): lax.ppermute(array, axes, [(k, k ^ step) for k in range(lax.axis_size(axe...  32.1 us
    all_to_all x1, blocking collectives, exchange(): return lax.all_to_all(blocks, axes, split_axis=0, concat_axis=0, tiled=True)  9.27 us
    ppermute x11, waiting for transfers between devices, partner(): lax.ppermute(array, axes, [(k, k ^ step) for k in range(lax.axis_size(axe...  7.16 us
    dot_general x14, matrix products, dot(): lax.dot_general(a, b, (((da,), (db,)), ((), ())), preferred_element_type=...  6.89 us
  transfers between devices with their start and end apart: 18, of which 11 were waited for; matrix products, arithmetic and copies ran while one was open for 8% of the time, Pallas kernels for 0%

commit v1 on v0

--- a/solution.py
+++ b/solution.py
@@ -39,6 +39,15 @@
     top = jnp.max(stats[:, 0], axis=0)
     lse = top + jnp.log(jnp.sum(jnp.exp(stats[:, 0] - top), axis=0))
     return jnp.stack([lse, jnp.sum(stats[:, 1], axis=0)])
+
+
+def parts_of(array):
+    parts = []
+    for _ in range(3):
+        part = lax.reduce_precision(array, 8, 7)
+        parts.append(part.astype(bf16))
+        array = array - part
+    return jnp.stack(parts)
 
 
 def halves(array, core):
@@ -90,6 +99,21 @@
         block = partner(block, X, step) if step else block
         w_rows = lax.dynamic_update_slice_in_dim(w_rows, block, x ^ step, 0)
 
+    vocab = (vocab, partner(vocab, C, 1))
+    bias = (vocab_bias, partner(vocab_bias.reshape(2, -1), C, 1).reshape(-1))
+
+    line = lax.broadcasted_iota(jnp.int32, (half, group), 0)
+    token = (line // own) % nz * (nq * own) + line // span * (nc * own) + c * own + line % own
+    goals = jnp.where(token == lax.broadcasted_iota(jnp.int32, (half, group), 1), targets[None, :], 0)
+    goals = jnp.sum(goals, axis=1)
+    ids = lax.broadcasted_iota(jnp.int32, (half, ncols), 1)
+    hit = [ids + k * ncols == goals[:, None] for k in (mine, mine ^ 1)]
+    goal_rows = sum(dot(h.astype(bf16), v, 1, 1) for h, v in zip(hit, vocab)).astype(bf16)
+    pieces = []
+    for step in range(nx):
+        piece = lax.dynamic_slice_in_dim(goal_rows, (x ^ step) * span, span)
+        pieces.append(partner(piece, X, step) if step else piece)
+
     sorted_h = dot(order, first.reshape(nz * rows, group), 1, 1).astype(bf16)
     partial = dot(sorted_h, w_rows.reshape(feats, nz * rows), 1, 1)
     proj = jnp.sum(exchange(partial.reshape(nq, span, feats), Q), axis=0)
@@ -102,26 +126,29 @@
     normed = (values * inv * final_gain).astype(bf16)
     normed = shared(normed, X, nx).reshape(half, width)
 
-    vocab = (vocab, partner(vocab, C, 1))
-    bias = (vocab_bias, partner(vocab_bias.reshape(2, -1), C, 1).reshape(-1))
-
-    line = lax.broadcasted_iota(jnp.int32, (half, group), 0)
-    token = (line // own) % nz * (nq * own) + line // span * (nc * own) + c * own + line % own
-    goals = jnp.where(token == lax.broadcasted_iota(jnp.int32, (half, group), 1), targets[None, :], 0)
-    goals = jnp.sum(goals, axis=1)
-    ids = lax.broadcasted_iota(jnp.int32, (half, ncols), 1)
-    hit = [ids + k * ncols == goals[:, None] for k in (mine, mine ^ 1)]
-    feat_group, last = width // ny, ny - 1
-    early = lax.dynamic_slice_in_dim(normed, (y ^ last) * feat_group, feat_group, 1)
-    early = partner(early, "dp", last)
+    feat_group, far, last = width // ny, ny // 2, ny - 1
+    early = {}
+    for step in (far, last):
+        piece = lax.dynamic_slice_in_dim(normed, (y ^ step) * feat_group, feat_group, 1)
+        early[step] = partner(piece, "dp", step)
 
     scores = [dot(normed, v, 1, 0) + b for v, b in zip(vocab, bias)]
     top = jnp.maximum(jnp.max(scores[0], axis=1), jnp.max(scores[1], axis=1))
     total = sum(jnp.sum(jnp.exp(s - top[:, None]), axis=1) for s in scores)
     goal = sum(jnp.sum(jnp.where(h, s, 0.0), axis=1) for h, s in zip(hit, scores))
-    stats = jnp.stack([top + jnp.log(total), goal])
-    stats = merged(shared(stats, X, nx))
-    stats = merged(shared(stats, Z, nz))
+    local = top + jnp.log(total)
+    terms = sum(
+        dot(jnp.where(h, 0.0, jnp.exp(s - local[:, None])).astype(bf16), v, 1, 1)
+        for h, s, v in zip(hit, scores, vocab)
+    ).astype(bf16)
+    stats = parts_of(jnp.stack([local, goal])).reshape(6, half)
+    stats = jnp.broadcast_to(jnp.pad(stats, ((0, span - 6), (0, 0)))[None], (nx, span, half))
+    terms = exchange(jnp.concatenate([terms.reshape(nx, span, width), stats], axis=2), X)
+    terms, *pieces = lax.optimization_barrier((terms, *pieces))
+    goal_rows = sum(p.astype(f32) for p in pieces).astype(bf16)
+    near = jnp.sum(terms[:, :6, width:].reshape(nx, 3, 2, half).astype(f32), axis=1)
+    terms = terms[:, :, :width]
+    stats = merged(shared(merged(near), Z, nz))
     lse, goal = stats
     losses = lse - goal + zloss_weight * lse * lse
     losses = lax.dynamic_slice_in_dim(losses, x * span + z * own, own)
@@ -130,14 +157,17 @@
         (jnp.exp(s - lse[:, None]) * scale[:, None] - jnp.where(h, 1.0, 0.0)).astype(bf16)
         for s, h in zip(scores, hit)
     ]
-    row_term = sum(dot(d, v, 1, 1) for d, v in zip(dscore, vocab)).astype(bf16)
-
-    row_term, *dscore = lax.optimization_barrier((row_term, *dscore))
+    shares = jnp.concatenate([jnp.exp(near[:, 0] - lse) * scale, (jnp.exp(goal - lse) * scale - 1.0)[None]])
+    shares = lax.dynamic_slice_in_dim(shares, x * span, span, 1)
+    row_x = shares[-1][:, None] * goal_rows.astype(f32)
+    row_x = (row_x + jnp.sum(shares[:-1, :, None] * terms.astype(f32), axis=0)).astype(bf16)
+
+    row_x, *dscore = lax.optimization_barrier((row_x, *dscore))
     theirs, ours = 0.0, 0.0
-    for step in (0, ny // 2, 1, last):
+    for step in (0, far, 1, last):
         cols_of = jnp.concatenate(dscore, axis=1)
-        if step == last:
-            piece, cols_of = early, partner(cols_of, "dp", step)
+        if step in early:
+            piece, cols_of = early[step], partner(cols_of, "dp", step)
         else:
             piece = lax.dynamic_slice_in_dim(normed, (y ^ step) * feat_group, feat_group, 1)
             if step:
@@ -147,8 +177,6 @@
         ours = ours + dot(piece, cols_of[:, :ncols], 0, 0)
     grad_vocab = lax.optimization_barrier(ours) + partner(theirs, C, 1)
 
-    row_x = exchange(row_term.reshape(nx, span, width), X)
-    row_x = jnp.sum(row_x.astype(f32), axis=0).astype(bf16)
     row_z = exchange(row_x.reshape(nz, own, width), Z)
     gathered, _ = lax.optimization_barrier((gathered, row_x))
     normin = lax.dynamic_slice_in_dim(gathered, z * own, own, 1).transpose(1, 0, 2).reshape(own, width)

time: 162 us -> 169 us (1.043)
  the two profiles are of different devices: /device:TPU:34 before, /device:TPU:16 now
where the time goes in v1:
time: 169 us; the launch traced here: 168 us
  starting transfers between devices  92.6 us (55%)
  waiting for transfers between devices  51 us (30%)
  matrix products  9.12 us (5%)
  local copies, waits for them, and re-layouts  7.44 us (4%)
  other arithmetic  5.51 us (3%)
    all_to_all x7, starting transfers between devices, exchange(): return lax.all_to_all(blocks, axes, split_axis=0, concat_axis=0, tiled=True)  46.6 us
    ppermute x15, starting transfers between devices, partner(): lax.ppermute(array, axes, [(k, k ^ step) for k in range(lax.axis_size(axe...  46 us
    all_to_all x7, waiting for transfers between devices, exchange(): return lax.all_to_all(blocks, axes, split_axis=0, concat_axis=0, tiled=True)  38.9 us
    ppermute x15, waiting for transfers between devices, partner(): lax.ppermute(array, axes, [(k, k ^ step) for k in range(lax.axis_size(axe...  12 us
    dot_general x16, matrix products, dot(): lax.dot_general(a, b, (((da,), (db,)), ((), ())), preferred_element_type=...  9.12 us
  transfers between devices with their start and end apart: 22, of which 11 were waited for; matrix products, arithmetic and copies ran while one was open for 7% of the time, Pallas kernels for 1%

profile of v1, /device:TPU:16, one launch (start us, length us, event | category | flops | bytes accessed | tf_op | source)
XLA Modules:
  0.0 167.9 jit_solution(9306118280547022465)
XLA Ops:
  2.9 15.2 %all-to-all-start = ((bf16[16,48,256]{2,1,0:T(8,128)(2,1)}), bf16[16,48,256]{2,1,0:T(8,128)(2,1)S(1)}, u32[]{:S(2)}, u32[]{:S(2)}) async-start(bf16[16,48,256]{2,1,0:T(8,128)(2,1)} %pad_add_fusion), calls=%async_computation | async-start | bytes 786432 | tf_op jit(solution)/shard_map/all_to_all | solution.py:23
  20.3 1.9 %collective-permute-start = (bf16[1,4,16,768]{3,2,1,0:T(8,128)(2,1)S(1)}, bf16[1,4,16,768]{3,2,1,0:T(8,128)(2,1)S(1)}, u32[]{:S(2)}, u32[]{:S(2)}) collective-permute-start(bf16[1,4,16,768]{3,2,1,0:T(8,128)(2,1)S(1)} %dynamic-slice_bitcast_fusion), channel_id=1, source_target_pairs={{0,4},{4,0},{1,5},{5,1},{2,6},{6,2},{3,7},{7,3},{8,12},{12,8},{9,1... | collective-permute-start | bytes 294920 | tf_op jit(solution)/shard_map/ppermute | solution.py:31
  23.6 3.4 %collective-permute-start.1 = (bf16[1,2,16,768]{3,2,1,0:T(8,128)(2,1)S(1)}, bf16[1,2,16,768]{3,2,1,0:T(8,128)(2,1)S(1)}, u32[]{:S(2)}, u32[]{:S(2)}) collective-permute-start(bf16[1,2,16,768]{3,2,1,0:T(8,128)(2,1)S(1)} %get-tuple-element.45), channel_id=1, source_target_pairs={{0,8},{8,0},{16,24},{24,16},{1,9},{9,1},{17,25},{25,17},{2,10},{10... | collective-permute-start | bytes 147464 | tf_op jit(solution)/shard_map/ppermute | solution.py:31
  27.0 4.6 %collective-permute-start.2 = (bf16[1,2,16,768]{3,2,1,0:T(8,128)(2,1)S(1)}, bf16[1,2,16,768]{3,2,1,0:T(8,128)(2,1)S(1)}, u32[]{:S(2)}, u32[]{:S(2)}) collective-permute-start(bf16[1,2,16,768]{3,2,1,0:T(8,128)(2,1)S(1)} %get-tuple-element.46), channel_id=1, source_target_pairs={{0,16},{8,24},{16,0},{24,8},{1,17},{9,25},{17,1},{25,9},{2,18},{10... | collective-permute-start | bytes 147464 | tf_op jit(solution)/shard_map/ppermute | solution.py:31
  31.6 2.4 %collective-permute-start.3 = (bf16[1,2,16,768]{3,2,1,0:T(8,128)(2,1)S(1)}, bf16[1,2,16,768]{3,2,1,0:T(8,128)(2,1)S(1)}, u32[]{:S(2)}, u32[]{:S(2)}) collective-permute-start(bf16[1,2,16,768]{3,2,1,0:T(8,128)(2,1)S(1)} %get-tuple-element.44), channel_id=1, source_target_pairs={{0,24},{8,16},{16,8},{24,0},{1,25},{9,17},{17,9},{25,1},{2,26},{10... | collective-permute-start | bytes 147464 | tf_op jit(solution)/shard_map/ppermute | solution.py:31
  34.5 4.3 %collective-permute-done.3 = bf16[1,2,16,768]{3,2,1,0:T(8,128)(2,1)S(1)} collective-permute-done((bf16[1,2,16,768]{3,2,1,0:T(8,128)(2,1)S(1)}, bf16[1,2,16,768]{3,2,1,0:T(8,128)(2,1)S(1)}, u32[]{:S(2)}, u32[]{:S(2)}) %collective-permute-start.3) | collective-permute-done | bytes 49184 | tf_op jit(solution)/shard_map/ppermute | solution.py:31
  38.8 3.1 %all-to-all-done = bf16[16,48,256]{2,1,0:T(8,128)(2,1)S(1)} async-done(((bf16[16,48,256]{2,1,0:T(8,128)(2,1)}), bf16[16,48,256]{2,1,0:T(8,128)(2,1)S(1)}, u32[]{:S(2)}, u32[]{:S(2)}) %all-to-all-start) | async-done | bytes 393248 | tf_op jit(solution)/shard_map/all_to_all | solution.py:23
  43.1 4.3 %all-to-all-start.1 = ((f32[8,32,128]{2,1,0:T(8,128)}), f32[8,32,128]{2,1,0:T(8,128)S(1)}, u32[]{:S(2)}, u32[]{:S(2)}) async-start(f32[8,32,128]{2,1,0:T(8,128)} %fusion.77), calls=%async_computation.1 | async-start | bytes 262144 | tf_op jit(solution)/shard_map/all_to_all | solution.py:23
  47.4 2.4 %collective-permute-start.4 = (bf16[2048,256]{1,0:T(8,128)(2,1)S(1)}, bf16[2048,256]{1,0:T(8,128)(2,1)S(1)}, u32[]{:S(2)}, u32[]{:S(2)}) collective-permute-start(bf16[2048,256]{1,0:T(8,128)(2,1)S(1)} %copy-done.1), channel_id=1, source_target_pairs={{0,4},{4,0},{1,5},{5,1},{2,6},{6,2},{3,7},{7,3},{8,12},{12,8},{9,1... | collective-permute-start | bytes 3145736 | tf_op jit(solution)/shard_map/ppermute | solution.py:31
  49.9 1.9 %collective-permute-start.5 = (f32[2,128]{1,0:T(2,128)S(1)}, f32[2,128]{1,0:T(2,128)S(1)}, u32[]{:S(2)}, u32[]{:S(2)}) collective-permute-start(f32[2,128]{1,0:T(2,128)S(1)} %bitcast.117), channel_id=1, source_target_pairs={{0,4},{4,0},{1,5},{5,1},{2,6},{6,2},{3,7},{7,3},{8,12},{12,8},{9,1... | collective-permute-start | bytes 3080 | tf_op jit(solution)/shard_map/ppermute | solution.py:31
  51.8 1.7 %all-to-all-done.1 = f32[8,32,128]{2,1,0:T(8,128)S(1)} async-done(((f32[8,32,128]{2,1,0:T(8,128)}), f32[8,32,128]{2,1,0:T(8,128)S(1)}, u32[]{:S(2)}, u32[]{:S(2)}) %all-to-all-start.1) | async-done | bytes 131104 | tf_op jit(solution)/shard_map/all_to_all | solution.py:23
  54.3 8.0 %all-to-all-start.2 = ((bf16[16,32,128]{2,1,0:T(8,128)(2,1)}), bf16[16,32,128]{2,1,0:T(8,128)(2,1)S(1)}, u32[]{:S(2)}, u32[]{:S(2)}) async-start(bf16[16,32,128]{2,1,0:T(8,128)(2,1)} %broadcast_in_dim.39), calls=%async_computation.2 | async-start | bytes 262144 | tf_op jit(solution)/shard_map/all_to_all | solution.py:23
  62.6 14.1 %all-to-all-done.2 = bf16[16,32,128]{2,1,0:T(8,128)(2,1)S(1)} async-done(((bf16[16,32,128]{2,1,0:T(8,128)(2,1)}), bf16[16,32,128]{2,1,0:T(8,128)(2,1)S(1)}, u32[]{:S(2)}, u32[]{:S(2)}) %all-to-all-start.2) | async-done | bytes 131104 | tf_op jit(solution)/shard_map/all_to_all | solution.py:23
  77.8 3.5 %all-to-all-start.3 = ((bf16[4,32,2048]{2,1,0:T(8,128)(2,1)}), bf16[4,32,2048]{2,1,0:T(8,128)(2,1)S(1)}, u32[]{:S(2)}, u32[]{:S(2)}) async-start(bf16[4,32,2048]{2,1,0:T(8,128)(2,1)} %broadcast_in_dim.40), calls=%async_computation.3 | async-start | bytes 1048576 | tf_op jit(solution)/shard_map/all_to_all | solution.py:23
  82.8 6.5 %all-to-all-done.3 = bf16[4,32,2048]{2,1,0:T(8,128)(2,1)S(1)} async-done(((bf16[4,32,2048]{2,1,0:T(8,128)(2,1)}), bf16[4,32,2048]{2,1,0:T(8,128)(2,1)S(1)}, u32[]{:S(2)}, u32[]{:S(2)}) %all-to-all-start.3) | async-done | bytes 524320 | tf_op jit(solution)/shard_map/all_to_all | solution.py:23
  92.0 1.7 %fusion = bf16[128,2048]{1,0:T(8,128)(2,1)S(1)} fusion(f32[128,2048]{1,0:T(8,128)} %fusion.31, bf16[2048,256]{1,0:T(8,128)(2,1)S(1)} %collective-permute-done.4, f32[128,256]{1,0:T(8,128)S(1)} %get-tuple-element.59, s32[256]{0:T(256)S(1)} %iota_add_fusion, f32[128]{0:T(128)S(1)} %log_add_fusion.1, s32[128]{0:T(128)S(1)} %select_reduce_fusion), kind=kOutput, calls=%fused_computation.2 | convolution fusion | flops 134873088 | bytes 2754560 | tf_op jit(solution)/shard_map/dot_general | solution.py:35
  94.6 3.5 %all-to-all-start.4 = ((bf16[4,32,2176]{2,1,0:T(8,128)(2,1)}), bf16[4,32,2176]{2,1,0:T(8,128)(2,1)S(1)}, u32[]{:S(2)}, u32[]{:S(2)}) async-start(bf16[4,32,2176]{2,1,0:T(8,128)(2,1)} %pad_maximum_fusion), calls=%async_computation.4 | async-start | bytes 1114112 | tf_op jit(solution)/shard_map/all_to_all | solution.py:23
  98.6 3.9 %collective-permute-start.6 = (bf16[32,2048]{1,0:T(8,128)(2,1)S(1)}, bf16[32,2048]{1,0:T(8,128)(2,1)S(1)}, u32[]{:S(2)}, u32[]{:S(2)}) collective-permute-start(bf16[32,2048]{1,0:T(8,128)(2,1)S(1)} %get-tuple-element.40), channel_id=1, source_target_pairs={{0,8},{8,0},{16,24},{24,16},{1,9},{9,1},{17,25},{25,17},{2,10},{10... | collective-permute-start | bytes 393224 | tf_op jit(solution)/shard_map/ppermute | solution.py:31
  102.5 4.6 %collective-permute-start.7 = (bf16[32,2048]{1,0:T(8,128)(2,1)S(1)}, bf16[32,2048]{1,0:T(8,128)(2,1)S(1)}, u32[]{:S(2)}, u32[]{:S(2)}) collective-permute-start(bf16[32,2048]{1,0:T(8,128)(2,1)S(1)} %get-tuple-element.39), channel_id=1, source_target_pairs={{0,16},{8,24},{16,0},{24,8},{1,17},{9,25},{17,1},{25,9},{2,18},{10... | collective-permute-start | bytes 393224 | tf_op jit(solution)/shard_map/ppermute | solution.py:31
  107.1 2.0 %collective-permute-start.8 = (bf16[32,2048]{1,0:T(8,128)(2,1)S(1)}, bf16[32,2048]{1,0:T(8,128)(2,1)S(1)}, u32[]{:S(2)}, u32[]{:S(2)}) collective-permute-start(bf16[32,2048]{1,0:T(8,128)(2,1)S(1)} %get-tuple-element.38), channel_id=1, source_target_pairs={{0,24},{8,16},{16,8},{24,0},{1,25},{9,17},{17,9},{25,1},{2,26},{10... | collective-permute-start | bytes 393224 | tf_op jit(solution)/shard_map/ppermute | solution.py:31
  109.1 1.8 %collective-permute-done.7 = bf16[32,2048]{1,0:T(8,128)(2,1)S(1)} collective-permute-done((bf16[32,2048]{1,0:T(8,128)(2,1)S(1)}, bf16[32,2048]{1,0:T(8,128)(2,1)S(1)}, u32[]{:S(2)}, u32[]{:S(2)}) %collective-permute-start.7) | collective-permute-done | bytes 131104 | tf_op jit(solution)/shard_map/ppermute | solution.py:31
  110.9 4.3 %collective-permute-done.8 = bf16[32,2048]{1,0:T(8,128)(2,1)S(1)} collective-permute-done((bf16[32,2048]{1,0:T(8,128)(2,1)S(1)}, bf16[32,2048]{1,0:T(8,128)(2,1)S(1)}, u32[]{:S(2)}, u32[]{:S(2)}) %collective-permute-start.8) | collective-permute-done | bytes 131104 | tf_op jit(solution)/shard_map/ppermute | solution.py:31
  115.9 5.4 %all-to-all-start.5 = ((f32[16,2,128]{2,1,0:T(2,128)}), f32[16,2,128]{2,1,0:T(2,128)S(1)}, u32[]{:S(2)}, u32[]{:S(2)}) async-start(f32[16,2,128]{2,1,0:T(2,128)} %broadcast_in_dim.42), calls=%async_computation.5 | async-start | bytes 32768 | tf_op jit(solution)/shard_map/all_to_all | solution.py:23
  122.0 2.2 %collective-permute-start.9 = (bf16[128,512]{1,0:T(8,128)(2,1)}, bf16[128,512]{1,0:T(8,128)(2,1)S(1)}, u32[]{:S(2)}, u32[]{:S(2)}) collective-permute-start(bf16[128,512]{1,0:T(8,128)(2,1)} %get-tuple-element.37), channel_id=1, source_target_pairs={{0,2},{1,3},{2,0},{3,1},{4,6},{5,7},{6,4},{7,5},{8,10},{9,11},{10,... | collective-permute-start | bytes 393224 | tf_op jit(solution)/shard_map/ppermute | solution.py:31
  124.3 4.3 %collective-permute-start.12 = (bf16[128,512]{1,0:T(8,128)(2,1)}, bf16[128,512]{1,0:T(8,128)(2,1)S(1)}, u32[]{:S(2)}, u32[]{:S(2)}) collective-permute-start(bf16[128,512]{1,0:T(8,128)(2,1)} %get-tuple-element.36), channel_id=1, source_target_pairs={{0,3},{1,2},{2,1},{3,0},{4,7},{5,6},{6,5},{7,4},{8,11},{9,10},{10,... | collective-permute-start | bytes 393224 | tf_op jit(solution)/shard_map/ppermute | solution.py:31
  128.6 5.3 %all-to-all-done.5 = f32[16,2,128]{2,1,0:T(2,128)S(1)} async-done(((f32[16,2,128]{2,1,0:T(2,128)}), f32[16,2,128]{2,1,0:T(2,128)S(1)}, u32[]{:S(2)}, u32[]{:S(2)}) %all-to-all-start.5) | async-done | bytes 16416 | tf_op jit(solution)/shard_map/all_to_all | solution.py:23
  134.5 2.3 %collective-permute-start.10 = (bf16[128,512]{1,0:T(8,128)(2,1)S(1)}, bf16[128,512]{1,0:T(8,128)(2,1)S(1)}, u32[]{:S(2)}, u32[]{:S(2)}) collective-permute-start(bf16[128,512]{1,0:T(8,128)(2,1)S(1)} %constant_dynamic-update-slice_fusion), channel_id=1, source_target_pairs={{0,2},{1,3},{2,0},{3,1},{4,6},{5,7},{6,4},{7,5},{8,10},{9,11},{10,... | collective-permute-start | bytes 393224 | tf_op jit(solution)/shard_map/ppermute | solution.py:31
  136.8 4.3 %collective-permute-start.13 = (bf16[128,512]{1,0:T(8,128)(2,1)S(1)}, bf16[128,512]{1,0:T(8,128)(2,1)S(1)}, u32[]{:S(2)}, u32[]{:S(2)}) collective-permute-start(bf16[128,512]{1,0:T(8,128)(2,1)S(1)} %constant_dynamic-update-slice_fusion), channel_id=1, source_target_pairs={{0,3},{1,2},{2,1},{3,0},{4,7},{5,6},{6,5},{7,4},{8,11},{9,10},{10,... | collective-permute-start | bytes 393224 | tf_op jit(solution)/shard_map/ppermute | solution.py:31
  141.7 3.9 %collective-permute-start.11 = (bf16[128,1024]{1,0:T(8,128)(2,1)S(1)}, bf16[128,1024]{1,0:T(8,128)(2,1)S(1)}, u32[]{:S(2)}, u32[]{:S(2)}) collective-permute-start(bf16[128,1024]{1,0:T(8,128)(2,1)S(1)} %pad_maximum_fusion.1), channel_id=1, source_target_pairs={{0,1},{1,0},{2,3},{3,2},{4,5},{5,4},{6,7},{7,6},{8,9},{9,8},{10,11... | collective-permute-start | bytes 786440 | tf_op jit(solution)/shard_map/ppermute | solution.py:31
  146.3 6.8 %all-to-all-start.6 = ((bf16[16,2,2048]{2,1,0:T(2,128)(2,1)}), bf16[16,2,2048]{2,1,0:T(2,128)(2,1)S(1)}, u32[]{:S(2)}, u32[]{:S(2)}) async-start(bf16[16,2,2048]{2,1,0:T(2,128)(2,1)} %reshape.388), calls=%async_computation.6 | async-start | bytes 262144 | tf_op jit(solution)/shard_map/all_to_all | solution.py:23
  155.2 1.9 %collective-permute-start.14 = (f32[512,256]{1,0:T(8,128)S(1)}, f32[512,256]{1,0:T(8,128)S(1)}, u32[]{:S(2)}, u32[]{:S(2)}) collective-permute-start(f32[512,256]{1,0:T(8,128)S(1)} %fusion.3), channel_id=1, source_target_pairs={{0,4},{4,0},{1,5},{5,1},{2,6},{6,2},{3,7},{7,3},{8,12},{12,8},{9,1... | collective-permute-start | bytes 1572872 | tf_op jit(solution)/shard_map/ppermute | solution.py:31
  157.9 8.2 %all-to-all-done.6.row_ref = bf16[16,2,2048]{2,1,0:T(2,128)(2,1)S(1)} async-done(((bf16[16,2,2048]{2,1,0:T(2,128)(2,1)}), bf16[16,2,2048]{2,1,0:T(2,128)(2,1)S(1)}, u32[]{:S(2)}, u32[]{:S(2)}) %all-to-all-start.6) | async-done | bytes 131104 | tf_op jit(solution)/shard_map/all_to_all | solution.py:23
  (116 shorter events, 22.8 us)
Async XLA Ops:
  0.6 17.5 %copy-start.4 = (bf16[5632,16]{0,1:T(8,128)(2,1)S(1)}, bf16[5632,16]{0,1:T(8,128)(2,1)}, u32[]{:S(2)}) copy-start(bf16[5632,16]{0,1:T(8,128)(2,1)} %param.10) | copy-start | bytes 540676
  2.9 39.0 %all-to-all-start = ((bf16[16,48,256]{2,1,0:T(8,128)(2,1)}), bf16[16,48,256]{2,1,0:T(8,128)(2,1)S(1)}, u32[]{:S(2)}, u32[]{:S(2)}) async-start(bf16[16,48,256]{2,1,0:T(8,128)(2,1)} %pad_add_fusion), calls=%async_computation | async-start | bytes 786432 | tf_op jit(solution)/shard_map/all_to_all | solution.py:23
  19.8 22.1 %copy-start.5 = (bf16[256,256]{1,0:T(8,128)(2,1)S(1)}, bf16[256,256]{1,0:T(8,128)(2,1)}, u32[]{:S(2)}) copy-start(bf16[256,256]{1,0:T(8,128)(2,1)} %constant.114.clone) | copy-start | bytes 393220
  20.3 3.2 %collective-permute-start = (bf16[1,4,16,768]{3,2,1,0:T(8,128)(2,1)S(1)}, bf16[1,4,16,768]{3,2,1,0:T(8,128)(2,1)S(1)}, u32[]{:S(2)}, u32[]{:S(2)}) collective-permute-start(bf16[1,4,16,768]{3,2,1,0:T(8,128)(2,1)S(1)} %dynamic-slice_bitcast_fusion), channel_id=1, source_target_pairs={{0,4},{4,0},{1,5},{5,1},{2,6},{6,2},{3,7},{7,3},{8,12},{12,8},{9,1... | collective-permute-start | bytes 294920 | tf_op jit(solution)/shard_map/ppermute | solution.py:31
  23.6 10.5 %collective-permute-start.1 = (bf16[1,2,16,768]{3,2,1,0:T(8,128)(2,1)S(1)}, bf16[1,2,16,768]{3,2,1,0:T(8,128)(2,1)S(1)}, u32[]{:S(2)}, u32[]{:S(2)}) collective-permute-start(bf16[1,2,16,768]{3,2,1,0:T(8,128)(2,1)S(1)} %get-tuple-element.45), channel_id=1, source_target_pairs={{0,8},{8,0},{16,24},{24,16},{1,9},{9,1},{17,25},{25,17},{2,10},{10... | collective-permute-start | bytes 147464 | tf_op jit(solution)/shard_map/ppermute | solution.py:31
  27.0 7.5 %collective-permute-start.2 = (bf16[1,2,16,768]{3,2,1,0:T(8,128)(2,1)S(1)}, bf16[1,2,16,768]{3,2,1,0:T(8,128)(2,1)S(1)}, u32[]{:S(2)}, u32[]{:S(2)}) collective-permute-start(bf16[1,2,16,768]{3,2,1,0:T(8,128)(2,1)S(1)} %get-tuple-element.46), channel_id=1, source_target_pairs={{0,16},{8,24},{16,0},{24,8},{1,17},{9,25},{17,1},{25,9},{2,18},{10... | collective-permute-start | bytes 147464 | tf_op jit(solution)/shard_map/ppermute | solution.py:31
  31.6 7.2 %collective-permute-start.3 = (bf16[1,2,16,768]{3,2,1,0:T(8,128)(2,1)S(1)}, bf16[1,2,16,768]{3,2,1,0:T(8,128)(2,1)S(1)}, u32[]{:S(2)}, u32[]{:S(2)}) collective-permute-start(bf16[1,2,16,768]{3,2,1,0:T(8,128)(2,1)S(1)} %get-tuple-element.44), channel_id=1, source_target_pairs={{0,24},{8,16},{16,8},{24,0},{1,25},{9,17},{17,9},{25,1},{2,26},{10... | collective-permute-start | bytes 147464 | tf_op jit(solution)/shard_map/ppermute | solution.py:31
  34.1 13.4 %copy-start.1 = (bf16[2048,256]{1,0:T(8,128)(2,1)S(1)}, bf16[2048,256]{1,0:T(8,128)(2,1)}, u32[]{:S(2)}) copy-start(bf16[2048,256]{1,0:T(8,128)(2,1)} %param.12) | copy-start | bytes 3145732
  34.1 15.8 %copy-start.7 = (f32[256]{0:T(256)S(1)}, f32[256]{0:T(256)}, u32[]{:S(2)}) copy-start(f32[256]{0:T(256)} %param.13) | copy-start | bytes 3076
  41.9 20.4 %copy-start.6 = (s32[256]{0:T(256)S(1)}, s32[256]{0:T(256)}, u32[]{:S(2)}) copy-start(s32[256]{0:T(256)} %param.14) | copy-start | bytes 3076
  42.2 34.7 %copy-start = (f32[2048]{0:T(1024)S(1)}, f32[2048]{0:T(1024)}, u32[]{:S(2)}) copy-start(f32[2048]{0:T(1024)} %param.11) | copy-start | bytes 24580
  43.1 10.4 %all-to-all-start.1 = ((f32[8,32,128]{2,1,0:T(8,128)}), f32[8,32,128]{2,1,0:T(8,128)S(1)}, u32[]{:S(2)}, u32[]{:S(2)}) async-start(f32[8,32,128]{2,1,0:T(8,128)} %fusion.77), calls=%async_computation.1 | async-start | bytes 262144 | tf_op jit(solution)/shard_map/all_to_all | solution.py:23
  47.4 42.3 %collective-permute-start.4 = (bf16[2048,256]{1,0:T(8,128)(2,1)S(1)}, bf16[2048,256]{1,0:T(8,128)(2,1)S(1)}, u32[]{:S(2)}, u32[]{:S(2)}) collective-permute-start(bf16[2048,256]{1,0:T(8,128)(2,1)S(1)} %copy-done.1), channel_id=1, source_target_pairs={{0,4},{4,0},{1,5},{5,1},{2,6},{6,2},{3,7},{7,3},{8,12},{12,8},{9,1... | collective-permute-start | bytes 3145736 | tf_op jit(solution)/shard_map/ppermute | solution.py:31
  49.9 39.9 %collective-permute-start.5 = (f32[2,128]{1,0:T(2,128)S(1)}, f32[2,128]{1,0:T(2,128)S(1)}, u32[]{:S(2)}, u32[]{:S(2)}) collective-permute-start(f32[2,128]{1,0:T(2,128)S(1)} %bitcast.117), channel_id=1, source_target_pairs={{0,4},{4,0},{1,5},{5,1},{2,6},{6,2},{3,7},{7,3},{8,12},{12,8},{9,1... | collective-permute-start | bytes 3080 | tf_op jit(solution)/shard_map/ppermute | solution.py:31
  54.3 22.4 %all-to-all-start.2 = ((bf16[16,32,128]{2,1,0:T(8,128)(2,1)}), bf16[16,32,128]{2,1,0:T(8,128)(2,1)S(1)}, u32[]{:S(2)}, u32[]{:S(2)}) async-start(bf16[16,32,128]{2,1,0:T(8,128)(2,1)} %broadcast_in_dim.39), calls=%async_computation.2 | async-start | bytes 262144 | tf_op jit(solution)/shard_map/all_to_all | solution.py:23
  76.7 1.1 copy-start.3
  77.8 11.5 %all-to-all-start.3 = ((bf16[4,32,2048]{2,1,0:T(8,128)(2,1)}), bf16[4,32,2048]{2,1,0:T(8,128)(2,1)S(1)}, u32[]{:S(2)}, u32[]{:S(2)}) async-start(bf16[4,32,2048]{2,1,0:T(8,128)(2,1)} %broadcast_in_dim.40), calls=%async_computation.3 | async-start | bytes 1048576 | tf_op jit(solution)/shard_map/all_to_all | solution.py:23
  93.7 4.3 %copy-start.2 = (f32[128,2048]{1,0:T(8,128)S(1)}, f32[128,2048]{1,0:T(8,128)}, u32[]{:S(2)}) copy-start(f32[128,2048]{1,0:T(8,128)} %fusion.8) | copy-start | bytes 3145732
  94.6 20.6 %all-to-all-start.4 = ((bf16[4,32,2176]{2,1,0:T(8,128)(2,1)}), bf16[4,32,2176]{2,1,0:T(8,128)(2,1)S(1)}, u32[]{:S(2)}, u32[]{:S(2)}) async-start(bf16[4,32,2176]{2,1,0:T(8,128)(2,1)} %pad_maximum_fusion), calls=%async_computation.4 | async-start | bytes 1114112 | tf_op jit(solution)/shard_map/all_to_all | solution.py:23
  98.6 10.5 %collective-permute-start.6 = (bf16[32,2048]{1,0:T(8,128)(2,1)S(1)}, bf16[32,2048]{1,0:T(8,128)(2,1)S(1)}, u32[]{:S(2)}, u32[]{:S(2)}) collective-permute-start(bf16[32,2048]{1,0:T(8,128)(2,1)S(1)} %get-tuple-element.40), channel_id=1, source_target_pairs={{0,8},{8,0},{16,24},{24,16},{1,9},{9,1},{17,25},{25,17},{2,10},{10... | collective-permute-start | bytes 393224 | tf_op jit(solution)/shard_map/ppermute | solution.py:31
  102.5 8.4 %collective-permute-start.7 = (bf16[32,2048]{1,0:T(8,128)(2,1)S(1)}, bf16[32,2048]{1,0:T(8,128)(2,1)S(1)}, u32[]{:S(2)}, u32[]{:S(2)}) collective-permute-start(bf16[32,2048]{1,0:T(8,128)(2,1)S(1)} %get-tuple-element.39), channel_id=1, source_target_pairs={{0,16},{8,24},{16,0},{24,8},{1,17},{9,25},{17,1},{25,9},{2,18},{10... | collective-permute-start | bytes 393224 | tf_op jit(solution)/shard_map/ppermute | solution.py:31
  107.1 8.1 %collective-permute-start.8 = (bf16[32,2048]{1,0:T(8,128)(2,1)S(1)}, bf16[32,2048]{1,0:T(8,128)(2,1)S(1)}, u32[]{:S(2)}, u32[]{:S(2)}) collective-permute-start(bf16[32,2048]{1,0:T(8,128)(2,1)S(1)} %get-tuple-element.38), channel_id=1, source_target_pairs={{0,24},{8,16},{16,8},{24,0},{1,25},{9,17},{17,9},{25,1},{2,26},{10... | collective-permute-start | bytes 393224 | tf_op jit(solution)/shard_map/ppermute | solution.py:31
  115.9 18.0 %all-to-all-start.5 = ((f32[16,2,128]{2,1,0:T(2,128)}), f32[16,2,128]{2,1,0:T(2,128)S(1)}, u32[]{:S(2)}, u32[]{:S(2)}) async-start(f32[16,2,128]{2,1,0:T(2,128)} %broadcast_in_dim.42), calls=%async_computation.5 | async-start | bytes 32768 | tf_op jit(solution)/shard_map/all_to_all | solution.py:23
  122.0 32.7 %collective-permute-start.9 = (bf16[128,512]{1,0:T(8,128)(2,1)}, bf16[128,512]{1,0:T(8,128)(2,1)S(1)}, u32[]{:S(2)}, u32[]{:S(2)}) collective-permute-start(bf16[128,512]{1,0:T(8,128)(2,1)} %get-tuple-element.37), channel_id=1, source_target_pairs={{0,2},{1,3},{2,0},{3,1},{4,6},{5,7},{6,4},{7,5},{8,10},{9,11},{10,... | collective-permute-start | bytes 393224 | tf_op jit(solution)/shard_map/ppermute | solution.py:31
  124.3 30.1 %collective-permute-start.12 = (bf16[128,512]{1,0:T(8,128)(2,1)}, bf16[128,512]{1,0:T(8,128)(2,1)S(1)}, u32[]{:S(2)}, u32[]{:S(2)}) collective-permute-start(bf16[128,512]{1,0:T(8,128)(2,1)} %get-tuple-element.36), channel_id=1, source_target_pairs={{0,3},{1,2},{2,1},{3,0},{4,7},{5,6},{6,5},{7,4},{8,11},{9,10},{10,... | collective-permute-start | bytes 393224 | tf_op jit(solution)/shard_map/ppermute | solution.py:31
  134.5 20.2 %collective-permute-start.10 = (bf16[128,512]{1,0:T(8,128)(2,1)S(1)}, bf16[128,512]{1,0:T(8,128)(2,1)S(1)}, u32[]{:S(2)}, u32[]{:S(2)}) collective-permute-start(bf16[128,512]{1,0:T(8,128)(2,1)S(1)} %constant_dynamic-update-slice_fusion), channel_id=1, source_target_pairs={{0,2},{1,3},{2,0},{3,1},{4,6},{5,7},{6,4},{7,5},{8,10},{9,11},{10,... | collective-permute-start | bytes 393224 | tf_op jit(solution)/shard_map/ppermute | solution.py:31
  136.8 17.6 %collective-permute-start.13 = (bf16[128,512]{1,0:T(8,128)(2,1)S(1)}, bf16[128,512]{1,0:T(8,128)(2,1)S(1)}, u32[]{:S(2)}, u32[]{:S(2)}) collective-permute-start(bf16[128,512]{1,0:T(8,128)(2,1)S(1)} %constant_dynamic-update-slice_fusion), channel_id=1, source_target_pairs={{0,3},{1,2},{2,1},{3,0},{4,7},{5,6},{6,5},{7,4},{8,11},{9,10},{10,... | collective-permute-start | bytes 393224 | tf_op jit(solution)/shard_map/ppermute | solution.py:31
  141.7 13.3 %collective-permute-start.11 = (bf16[128,1024]{1,0:T(8,128)(2,1)S(1)}, bf16[128,1024]{1,0:T(8,128)(2,1)S(1)}, u32[]{:S(2)}, u32[]{:S(2)}) collective-permute-start(bf16[128,1024]{1,0:T(8,128)(2,1)S(1)} %pad_maximum_fusion.1), channel_id=1, source_target_pairs={{0,1},{1,0},{2,3},{3,2},{4,5},{5,4},{6,7},{7,6},{8,9},{9,8},{10,11... | collective-permute-start | bytes 786440 | tf_op jit(solution)/shard_map/ppermute | solution.py:31
  146.3 19.9 %all-to-all-start.6 = ((bf16[16,2,2048]{2,1,0:T(2,128)(2,1)}), bf16[16,2,2048]{2,1,0:T(2,128)(2,1)S(1)}, u32[]{:S(2)}, u32[]{:S(2)}) async-start(bf16[16,2,2048]{2,1,0:T(2,128)(2,1)} %reshape.388), calls=%async_computation.6 | async-start | bytes 262144 | tf_op jit(solution)/shard_map/all_to_all | solution.py:23
  155.2 11.8 %collective-permute-start.14 = (f32[512,256]{1,0:T(8,128)S(1)}, f32[512,256]{1,0:T(8,128)S(1)}, u32[]{:S(2)}, u32[]{:S(2)}) collective-permute-start(f32[512,256]{1,0:T(8,128)S(1)} %fusion.3), channel_id=1, source_target_pairs={{0,4},{4,0},{1,5},{5,1},{2,6},{6,2},{3,7},{7,3},{8,12},{12,8},{9,1... | collective-permute-start | bytes 1572872 | tf_op jit(solution)/shard_map/ppermute | solution.py:31

commit v2 on v1

--- a/solution.py
+++ b/solution.py
@@ -41,15 +41,6 @@
     return jnp.stack([lse, jnp.sum(stats[:, 1], axis=0)])
 
 
-def parts_of(array):
-    parts = []
-    for _ in range(3):
-        part = lax.reduce_precision(array, 8, 7)
-        parts.append(part.astype(bf16))
-        array = array - part
-    return jnp.stack(parts)
-
-
 def halves(array, core):
     first = lax.dynamic_slice_in_dim(array, core * (array.shape[0] // 2), array.shape[0] // 2)
     other = (1 - core) * (array.shape[0] // 2)
@@ -62,6 +53,38 @@
     scaled = jnp.sum(row_ref[...].astype(f32), axis=0) * gain_ref[...]
     mean = jnp.mean(values * scaled, axis=1, keepdims=True)
     out_ref[...] = inv * (scaled - values * inv * inv * mean)
+
+
+def head_kernel(base_ref, normed_ref, own_ref, other_ref, bias_ref, goals_ref, block_ref, scores_ref):
+    ncols = own_ref.shape[1]
+    blocks, span, wide = block_ref.shape
+    half, width = normed_ref.shape
+    vocab = (own_ref, other_ref)
+    normed, goals = normed_ref[...], goals_ref[...]
+    scores = [dot(normed, v[...], 1, 0) + bias_ref[k : k + 1] for k, v in enumerate(vocab)]
+    ids = lax.broadcasted_iota(jnp.int32, (half, ncols), 1)
+    hit = [ids + base_ref[k] == goals for k in range(2)]
+    top = jnp.maximum(*(jnp.max(s, axis=1, keepdims=True) for s in scores))
+    total = sum(jnp.sum(jnp.exp(s - top), axis=1, keepdims=True) for s in scores)
+    goal = sum(jnp.sum(jnp.where(h, s, 0.0), axis=1, keepdims=True) for h, s in zip(hit, scores))
+    local = top + jnp.log(total)
+    weights = [jnp.where(h, 0.0, jnp.exp(s - local)).astype(bf16) for h, s in zip(hit, scores)]
+    lane = lax.broadcasted_iota(jnp.int32, (half, wide - width), 1)
+    parts = jnp.zeros((half, wide - width), f32)
+    for k, column in enumerate((local, goal)):
+        for place in range(3):
+            part = column.astype(bf16).astype(f32)
+            parts = jnp.where(lane == 2 * place + k, part, parts)
+            column = column - part
+    parts = parts.T[:span].astype(bf16)
+    for k in range(2):
+        scores_ref[k] = scores[k]
+    for at in range(0, width, 512):
+        terms = sum(dot(w, v[at : at + 512], 1, 1) for w, v in zip(weights, vocab)).astype(bf16)
+        for k in range(blocks):
+            block_ref[k, :, at : at + 512] = terms[k * span : (k + 1) * span]
+    for k in range(blocks):
+        block_ref[k, :, width:] = parts
 
 
 def body(stream, hidden, w_down, final_gain, vocab, vocab_bias, targets):
@@ -132,18 +155,27 @@
         piece = lax.dynamic_slice_in_dim(normed, (y ^ step) * feat_group, feat_group, 1)
         early[step] = partner(piece, "dp", step)
 
-    scores = [dot(normed, v, 1, 0) + b for v, b in zip(vocab, bias)]
-    top = jnp.maximum(jnp.max(scores[0], axis=1), jnp.max(scores[1], axis=1))
-    total = sum(jnp.sum(jnp.exp(s - top[:, None]), axis=1) for s in scores)
-    goal = sum(jnp.sum(jnp.where(h, s, 0.0), axis=1) for h, s in zip(hit, scores))
-    local = top + jnp.log(total)
-    terms = sum(
-        dot(jnp.where(h, 0.0, jnp.exp(s - local[:, None])).astype(bf16), v, 1, 1)
-        for h, s, v in zip(hit, scores, vocab)
-    ).astype(bf16)
-    stats = parts_of(jnp.stack([local, goal])).reshape(6, half)
-    stats = jnp.broadcast_to(jnp.pad(stats, ((0, span - 6), (0, 0)))[None], (nx, span, half))
-    terms = exchange(jnp.concatenate([terms.reshape(nx, span, width), stats], axis=2), X)
+    vmem, smem = (pl.BlockSpec(memory_space=m) for m in (pltpu.VMEM, pltpu.SMEM))
+    block, scores = pl.pallas_call(
+        head_kernel,
+        out_shape=(
+            jax.ShapeDtypeStruct((nx, span, width + half), bf16),
+            jax.ShapeDtypeStruct((2, half, ncols), f32),
+        ),
+        in_specs=[smem, vmem, vmem, vmem, vmem, vmem],
+        out_specs=(vmem, vmem),
+        compiler_params=pltpu.CompilerParams(vmem_limit_bytes=24 << 20),
+        cost_estimate=pl.CostEstimate(
+            flops=8 * half * ncols * width, bytes_accessed=8 * ncols * width, transcendentals=4 * half * ncols
+        ),
+    )(
+        jnp.stack([mine * ncols, (mine ^ 1) * ncols]),
+        normed,
+        *vocab,
+        jnp.stack(bias),
+        goals[:, None],
+    )
+    terms = exchange(block, X)
     terms, *pieces = lax.optimization_barrier((terms, *pieces))
     goal_rows = sum(p.astype(f32) for p in pieces).astype(bf16)
     near = jnp.sum(terms[:, :6, width:].reshape(nx, 3, 2, half).astype(f32), axis=1)
@@ -157,10 +189,10 @@
         (jnp.exp(s - lse[:, None]) * scale[:, None] - jnp.where(h, 1.0, 0.0)).astype(bf16)
         for s, h in zip(scores, hit)
     ]
-    shares = jnp.concatenate([jnp.exp(near[:, 0] - lse) * scale, (jnp.exp(goal - lse) * scale - 1.0)[None]])
-    shares = lax.dynamic_slice_in_dim(shares, x * span, span, 1)
-    row_x = shares[-1][:, None] * goal_rows.astype(f32)
-    row_x = (row_x + jnp.sum(shares[:-1, :, None] * terms.astype(f32), axis=0)).astype(bf16)
+    shares = lax.dynamic_slice_in_dim(jnp.exp(near[:, 0] - lse) * scale, x * span, span, 1)
+    goal_share = lax.dynamic_slice_in_dim(jnp.exp(goal - lse) * scale - 1.0, x * span, span)
+    row_x = jnp.sum(shares[:, :, None] * terms.astype(f32), axis=0)
+    row_x = (row_x + goal_share[:, None] * goal_rows.astype(f32)).astype(bf16)
 
     row_x, *dscore = lax.optimization_barrier((row_x, *dscore))
     theirs, ours = 0.0, 0.0

time: 169 us -> 163 us (0.964)
  the two profiles are of different devices: /device:TPU:16 before, /device:TPU:1 now
where the time goes in v2:
time: 163 us; the launch traced here: 162 us
  starting transfers between devices  104 us (64%)
  waiting for transfers between devices  34.7 us (21%)
  local copies, waits for them, and re-layouts  9.46 us (6%)
  matrix products  5.18 us (3%)
  other arithmetic  3.74 us (2%)
  Pallas kernels  3.59 us (2%)
    all_to_all x7, starting transfers between devices, exchange(): return lax.all_to_all(blocks, axes, split_axis=0, concat_axis=0, tiled=True)  54 us
    ppermute x15, starting transfers between devices, partner(): lax.ppermute(array, axes, [(k, k ^ step) for k in range(lax.axis_size(axe...  49.9 us
    all_to_all x7, waiting for transfers between devices, exchange(): return lax.all_to_all(blocks, axes, split_axis=0, concat_axis=0, tiled=True)  25.1 us
    ppermute x15, waiting for transfers between devices, partner(): lax.ppermute(array, axes, [(k, k ^ step) for k in range(lax.axis_size(axe...  9.62 us
    dot_general x12, matrix products, dot(): lax.dot_general(a, b, (((da,), (db,)), ((), ())), preferred_element_type=...  5.18 us
  transfers between devices with their start and end apart: 22, of which 7 were waited for; matrix products, arithmetic and copies ran while one was open for 8% of the time, Pallas kernels for 1%

profile of v2, /device:TPU:1, one launch (start us, length us, event | category | flops | bytes accessed | tf_op | source)
XLA Modules:
  0.0 161.9 jit_solution(8792357379664704137)
XLA Ops:
  2.2 15.9 %all-to-all-start = ((bf16[16,48,256]{2,1,0:T(8,128)(2,1)}), bf16[16,48,256]{2,1,0:T(8,128)(2,1)S(1)}, u32[]{:S(2)}, u32[]{:S(2)}) async-start(bf16[16,48,256]{2,1,0:T(8,128)(2,1)} %pad_add_fusion), calls=%async_computation | async-start | bytes 786432 | tf_op jit(solution)/shard_map/all_to_all | solution.py:23
  18.1 1.5 reshape.144
  20.3 2.9 %collective-permute-start = (bf16[1,4,16,768]{3,2,1,0:T(8,128)(2,1)S(1)}, bf16[1,4,16,768]{3,2,1,0:T(8,128)(2,1)S(1)}, u32[]{:S(2)}, u32[]{:S(2)}) collective-permute-start(bf16[1,4,16,768]{3,2,1,0:T(8,128)(2,1)S(1)} %dynamic-slice_bitcast_fusion), channel_id=1, source_target_pairs={{0,4},{4,0},{1,5},{5,1},{2,6},{6,2},{3,7},{7,3},{8,12},{12,8},{9,1... | collective-permute-start | bytes 294920 | tf_op jit(solution)/shard_map/ppermute | solution.py:31
  23.1 1.9 %collective-permute-start.5 = (f32[2,128]{1,0:T(2,128)S(1)}, f32[2,128]{1,0:T(2,128)S(1)}, u32[]{:S(2)}, u32[]{:S(2)}) collective-permute-start(f32[2,128]{1,0:T(2,128)S(1)} %bitcast.121), channel_id=1, source_target_pairs={{0,4},{4,0},{1,5},{5,1},{2,6},{6,2},{3,7},{7,3},{8,12},{12,8},{9,1... | collective-permute-start | bytes 3080 | tf_op jit(solution)/shard_map/ppermute | solution.py:31
  25.1 2.4 %collective-permute-start.4 = (bf16[2048,256]{1,0:T(8,128)(2,1)S(1)}, bf16[2048,256]{1,0:T(8,128)(2,1)S(1)}, u32[]{:S(2)}, u32[]{:S(2)}) collective-permute-start(bf16[2048,256]{1,0:T(8,128)(2,1)S(1)} %copy-done), channel_id=1, source_target_pairs={{0,4},{4,0},{1,5},{5,1},{2,6},{6,2},{3,7},{7,3},{8,12},{12,8},{9,1... | collective-permute-start | bytes 3145736 | tf_op jit(solution)/shard_map/ppermute | solution.py:31
  27.6 4.4 %collective-permute-start.3 = (bf16[1,2,16,768]{3,2,1,0:T(8,128)(2,1)S(1)}, bf16[1,2,16,768]{3,2,1,0:T(8,128)(2,1)S(1)}, u32[]{:S(2)}, u32[]{:S(2)}) collective-permute-start(bf16[1,2,16,768]{3,2,1,0:T(8,128)(2,1)S(1)} %get-tuple-element.44), channel_id=1, source_target_pairs={{0,24},{8,16},{16,8},{24,0},{1,25},{9,17},{17,9},{25,1},{2,26},{10... | collective-permute-start | bytes 147464 | tf_op jit(solution)/shard_map/ppermute | solution.py:31
  32.0 1.9 %collective-permute-start.1 = (bf16[1,2,16,768]{3,2,1,0:T(8,128)(2,1)S(1)}, bf16[1,2,16,768]{3,2,1,0:T(8,128)(2,1)S(1)}, u32[]{:S(2)}, u32[]{:S(2)}) collective-permute-start(bf16[1,2,16,768]{3,2,1,0:T(8,128)(2,1)S(1)} %get-tuple-element.45), channel_id=1, source_target_pairs={{0,8},{8,0},{16,24},{24,16},{1,9},{9,1},{17,25},{25,17},{2,10},{10... | collective-permute-start | bytes 147464 | tf_op jit(solution)/shard_map/ppermute | solution.py:31
  33.9 3.3 %collective-permute-start.2 = (bf16[1,2,16,768]{3,2,1,0:T(8,128)(2,1)S(1)}, bf16[1,2,16,768]{3,2,1,0:T(8,128)(2,1)S(1)}, u32[]{:S(2)}, u32[]{:S(2)}) collective-permute-start(bf16[1,2,16,768]{3,2,1,0:T(8,128)(2,1)S(1)} %get-tuple-element.46), channel_id=1, source_target_pairs={{0,16},{8,24},{16,0},{24,8},{1,17},{9,25},{17,1},{25,9},{2,18},{10... | collective-permute-start | bytes 147464 | tf_op jit(solution)/shard_map/ppermute | solution.py:31
  37.3 3.3 %collective-permute-done.2 = bf16[1,2,16,768]{3,2,1,0:T(8,128)(2,1)S(1)} collective-permute-done((bf16[1,2,16,768]{3,2,1,0:T(8,128)(2,1)S(1)}, bf16[1,2,16,768]{3,2,1,0:T(8,128)(2,1)S(1)}, u32[]{:S(2)}, u32[]{:S(2)}) %collective-permute-start.2) | collective-permute-done | bytes 49184 | tf_op jit(solution)/shard_map/ppermute | solution.py:31
  41.8 6.5 %all-to-all-start.1 = ((f32[8,32,128]{2,1,0:T(8,128)}), f32[8,32,128]{2,1,0:T(8,128)S(1)}, u32[]{:S(2)}, u32[]{:S(2)}) async-start(f32[8,32,128]{2,1,0:T(8,128)} %fusion.59), calls=%async_computation.1 | async-start | bytes 262144 | tf_op jit(solution)/shard_map/all_to_all | solution.py:23
  48.3 5.2 %all-to-all-done.1 = f32[8,32,128]{2,1,0:T(8,128)S(1)} async-done(((f32[8,32,128]{2,1,0:T(8,128)}), f32[8,32,128]{2,1,0:T(8,128)S(1)}, u32[]{:S(2)}, u32[]{:S(2)}) %all-to-all-start.1) | async-done | bytes 131104 | tf_op jit(solution)/shard_map/all_to_all | solution.py:23
  54.3 9.9 %all-to-all-start.2 = ((bf16[16,32,128]{2,1,0:T(8,128)(2,1)}), bf16[16,32,128]{2,1,0:T(8,128)(2,1)S(1)}, u32[]{:S(2)}, u32[]{:S(2)}) async-start(bf16[16,32,128]{2,1,0:T(8,128)(2,1)} %broadcast_in_dim.31), calls=%async_computation.2 | async-start | bytes 262144 | tf_op jit(solution)/shard_map/all_to_all | solution.py:23
  65.3 10.9 %all-to-all-done.2 = bf16[16,32,128]{2,1,0:T(8,128)(2,1)S(1)} async-done(((bf16[16,32,128]{2,1,0:T(8,128)(2,1)}), bf16[16,32,128]{2,1,0:T(8,128)(2,1)S(1)}, u32[]{:S(2)}, u32[]{:S(2)}) %all-to-all-start.2) | async-done | bytes 131104 | tf_op jit(solution)/shard_map/all_to_all | solution.py:23
  77.7 3.5 %all-to-all-start.3 = ((bf16[4,32,2048]{2,1,0:T(8,128)(2,1)}), bf16[4,32,2048]{2,1,0:T(8,128)(2,1)S(1)}, u32[]{:S(2)}, u32[]{:S(2)}) async-start(bf16[4,32,2048]{2,1,0:T(8,128)(2,1)} %broadcast_in_dim.32), calls=%async_computation.3 | async-start | bytes 1048576 | tf_op jit(solution)/shard_map/all_to_all | solution.py:23
  81.2 1.5 fusion.7
  82.9 5.2 %all-to-all-done.3 = bf16[4,32,2048]{2,1,0:T(8,128)(2,1)S(1)} async-done(((bf16[4,32,2048]{2,1,0:T(8,128)(2,1)}), bf16[4,32,2048]{2,1,0:T(8,128)(2,1)S(1)}, u32[]{:S(2)}, u32[]{:S(2)}) %all-to-all-start.3) | async-done | bytes 524320 | tf_op jit(solution)/shard_map/all_to_all | solution.py:23
  88.0 2.7 %shard_map.103 = (bf16[4,32,2176]{2,1,0:T(8,128)(2,1)}, f32[2,128,256]{2,1,0:T(8,128)S(1)}) custom-call(s32[2]{0:T(128)S(1)} %pad_add_fusion.1.base_ref, bf16[128,2048]{1,0:T(8,128)(2,1)S(1)} %bitcast.102, bf16[2048,256]{1,0:T(8,128)(2,1)S(1)} %copy-done, bf16[2048,256]{1,0:T(8,128)(2,1)S(1)} %collective-permute-done.4.other_ref, ...), custom_call_target="tpu_custom_call" | custom-call | flops 536870912 | bytes 4194304 | tf_op jit(solution)/shard_map/pallas_call | solution.py:159
  90.8 3.6 %all-to-all-start.4 = ((bf16[4,32,2176]{2,1,0:T(8,128)(2,1)}), bf16[4,32,2176]{2,1,0:T(8,128)(2,1)S(1)}, u32[]{:S(2)}, u32[]{:S(2)}) async-start(bf16[4,32,2176]{2,1,0:T(8,128)(2,1)} %get-tuple-element.18), calls=%async_computation.4 | async-start | bytes 1114112 | tf_op jit(solution)/shard_map/all_to_all | solution.py:23
  95.0 4.5 %collective-permute-start.8 = (bf16[32,2048]{1,0:T(8,128)(2,1)S(1)}, bf16[32,2048]{1,0:T(8,128)(2,1)S(1)}, u32[]{:S(2)}, u32[]{:S(2)}) collective-permute-start(bf16[32,2048]{1,0:T(8,128)(2,1)S(1)} %get-tuple-element.36), channel_id=1, source_target_pairs={{0,24},{8,16},{16,8},{24,0},{1,25},{9,17},{17,9},{25,1},{2,26},{10... | collective-permute-start | bytes 393224 | tf_op jit(solution)/shard_map/ppermute | solution.py:31
  99.5 2.5 %collective-permute-start.7 = (bf16[32,2048]{1,0:T(8,128)(2,1)S(1)}, bf16[32,2048]{1,0:T(8,128)(2,1)S(1)}, u32[]{:S(2)}, u32[]{:S(2)}) collective-permute-start(bf16[32,2048]{1,0:T(8,128)(2,1)S(1)} %get-tuple-element.37), channel_id=1, source_target_pairs={{0,16},{8,24},{16,0},{24,8},{1,17},{9,25},{17,1},{25,9},{2,18},{10... | collective-permute-start | bytes 393224 | tf_op jit(solution)/shard_map/ppermute | solution.py:31
  102.0 2.0 %collective-permute-start.6 = (bf16[32,2048]{1,0:T(8,128)(2,1)S(1)}, bf16[32,2048]{1,0:T(8,128)(2,1)S(1)}, u32[]{:S(2)}, u32[]{:S(2)}) collective-permute-start(bf16[32,2048]{1,0:T(8,128)(2,1)S(1)} %get-tuple-element.38), channel_id=1, source_target_pairs={{0,8},{8,0},{16,24},{24,16},{1,9},{9,1},{17,25},{25,17},{2,10},{10... | collective-permute-start | bytes 393224 | tf_op jit(solution)/shard_map/ppermute | solution.py:31
  104.0 4.5 %collective-permute-done.7 = bf16[32,2048]{1,0:T(8,128)(2,1)S(1)} collective-permute-done((bf16[32,2048]{1,0:T(8,128)(2,1)S(1)}, bf16[32,2048]{1,0:T(8,128)(2,1)S(1)}, u32[]{:S(2)}, u32[]{:S(2)}) %collective-permute-start.7) | collective-permute-done | bytes 131104 | tf_op jit(solution)/shard_map/ppermute | solution.py:31
  109.2 7.4 %all-to-all-start.5 = ((f32[16,2,128]{2,1,0:T(2,128)}), f32[16,2,128]{2,1,0:T(2,128)S(1)}, u32[]{:S(2)}, u32[]{:S(2)}) async-start(f32[16,2,128]{2,1,0:T(2,128)} %broadcast_in_dim.37), calls=%async_computation.5 | async-start | bytes 32768 | tf_op jit(solution)/shard_map/all_to_all | solution.py:23
  117.3 4.6 %collective-permute-start.12 = (bf16[128,512]{1,0:T(8,128)(2,1)}, bf16[128,512]{1,0:T(8,128)(2,1)S(1)}, u32[]{:S(2)}, u32[]{:S(2)}) collective-permute-start(bf16[128,512]{1,0:T(8,128)(2,1)} %get-tuple-element.34), channel_id=1, source_target_pairs={{0,3},{1,2},{2,1},{3,0},{4,7},{5,6},{6,5},{7,4},{8,11},{9,10},{10,... | collective-permute-start | bytes 393224 | tf_op jit(solution)/shard_map/ppermute | solution.py:31
  122.0 2.3 %collective-permute-start.9 = (bf16[128,512]{1,0:T(8,128)(2,1)}, bf16[128,512]{1,0:T(8,128)(2,1)S(1)}, u32[]{:S(2)}, u32[]{:S(2)}) collective-permute-start(bf16[128,512]{1,0:T(8,128)(2,1)} %get-tuple-element.35), channel_id=1, source_target_pairs={{0,2},{1,3},{2,0},{3,1},{4,6},{5,7},{6,4},{7,5},{8,10},{9,11},{10,... | collective-permute-start | bytes 393224 | tf_op jit(solution)/shard_map/ppermute | solution.py:31
  124.2 3.8 %all-to-all-done.5 = f32[16,2,128]{2,1,0:T(2,128)S(1)} async-done(((f32[16,2,128]{2,1,0:T(2,128)}), f32[16,2,128]{2,1,0:T(2,128)S(1)}, u32[]{:S(2)}, u32[]{:S(2)}) %all-to-all-start.5) | async-done | bytes 16416 | tf_op jit(solution)/shard_map/all_to_all | solution.py:23
  128.7 4.6 %collective-permute-start.13 = (bf16[128,512]{1,0:T(8,128)(2,1)S(1)}, bf16[128,512]{1,0:T(8,128)(2,1)S(1)}, u32[]{:S(2)}, u32[]{:S(2)}) collective-permute-start(bf16[128,512]{1,0:T(8,128)(2,1)S(1)} %constant_dynamic-update-slice_fusion), channel_id=1, source_target_pairs={{0,3},{1,2},{2,1},{3,0},{4,7},{5,6},{6,5},{7,4},{8,11},{9,10},{10,... | collective-permute-start | bytes 393224 | tf_op jit(solution)/shard_map/ppermute | solution.py:31
  133.3 2.3 %collective-permute-start.10 = (bf16[128,512]{1,0:T(8,128)(2,1)S(1)}, bf16[128,512]{1,0:T(8,128)(2,1)S(1)}, u32[]{:S(2)}, u32[]{:S(2)}) collective-permute-start(bf16[128,512]{1,0:T(8,128)(2,1)S(1)} %constant_dynamic-update-slice_fusion), channel_id=1, source_target_pairs={{0,2},{1,3},{2,0},{3,1},{4,6},{5,7},{6,4},{7,5},{8,10},{9,11},{10,... | collective-permute-start | bytes 393224 | tf_op jit(solution)/shard_map/ppermute | solution.py:31
  136.9 7.3 %all-to-all-start.6 = ((bf16[16,2,2048]{2,1,0:T(2,128)(2,1)}), bf16[16,2,2048]{2,1,0:T(2,128)(2,1)S(1)}, u32[]{:S(2)}, u32[]{:S(2)}) async-start(bf16[16,2,2048]{2,1,0:T(2,128)(2,1)} %reshape.149), calls=%async_computation.6 | async-start | bytes 262144 | tf_op jit(solution)/shard_map/all_to_all | solution.py:23
  144.2 2.5 %collective-permute-start.11 = (bf16[128,1024]{1,0:T(8,128)(2,1)S(1)}, bf16[128,1024]{1,0:T(8,128)(2,1)S(1)}, u32[]{:S(2)}, u32[]{:S(2)}) collective-permute-start(bf16[128,1024]{1,0:T(8,128)(2,1)S(1)} %pad_maximum_fusion), channel_id=1, source_target_pairs={{0,1},{1,0},{2,3},{3,2},{4,5},{5,4},{6,7},{7,6},{8,9},{9,8},{10,11... | collective-permute-start | bytes 786440 | tf_op jit(solution)/shard_map/ppermute | solution.py:31
  149.4 1.9 %collective-permute-done.11 = bf16[128,1024]{1,0:T(8,128)(2,1)S(1)} collective-permute-done((bf16[128,1024]{1,0:T(8,128)(2,1)S(1)}, bf16[128,1024]{1,0:T(8,128)(2,1)S(1)}, u32[]{:S(2)}, u32[]{:S(2)}) %collective-permute-start.11) | collective-permute-done | bytes 262176 | tf_op jit(solution)/shard_map/ppermute | solution.py:31
  151.6 7.8 %collective-permute-start.14 = (f32[512,256]{1,0:T(8,128)S(1)}, f32[512,256]{1,0:T(8,128)S(1)}, u32[]{:S(2)}, u32[]{:S(2)}) collective-permute-start(f32[512,256]{1,0:T(8,128)S(1)} %fusion.2), channel_id=1, source_target_pairs={{0,4},{4,0},{1,5},{5,1},{2,6},{6,2},{3,7},{7,3},{8,12},{12,8},{9,1... | collective-permute-start | bytes 1572872 | tf_op jit(solution)/shard_map/ppermute | solution.py:31
  (117 shorter events, 16.3 us)
Async XLA Ops:
  0.6 0.8 copy-start.12
  2.2 15.9 %copy-start.6 = (bf16[5632,16]{0,1:T(8,128)(2,1)S(1)}, bf16[5632,16]{0,1:T(8,128)(2,1)}, u32[]{:S(2)}) copy-start(bf16[5632,16]{0,1:T(8,128)(2,1)} %param.10) | copy-start | bytes 540676
  2.2 38.4 %all-to-all-start = ((bf16[16,48,256]{2,1,0:T(8,128)(2,1)}), bf16[16,48,256]{2,1,0:T(8,128)(2,1)S(1)}, u32[]{:S(2)}, u32[]{:S(2)}) async-start(bf16[16,48,256]{2,1,0:T(8,128)(2,1)} %pad_add_fusion), calls=%async_computation | async-start | bytes 786432 | tf_op jit(solution)/shard_map/all_to_all | solution.py:23
  19.6 5.5 %copy-start = (bf16[2048,256]{1,0:T(8,128)(2,1)S(1)}, bf16[2048,256]{1,0:T(8,128)(2,1)}, u32[]{:S(2)}) copy-start(bf16[2048,256]{1,0:T(8,128)(2,1)} %own_ref.1) | copy-start | bytes 3145732
  20.3 2.9 %copy-start.14 = (f32[256]{0:T(256)S(1)}, f32[256]{0:T(256)}, u32[]{:S(2)}) copy-start(f32[256]{0:T(256)} %param.13) | copy-start | bytes 3076
  20.3 7.3 %collective-permute-start = (bf16[1,4,16,768]{3,2,1,0:T(8,128)(2,1)S(1)}, bf16[1,4,16,768]{3,2,1,0:T(8,128)(2,1)S(1)}, u32[]{:S(2)}, u32[]{:S(2)}) collective-permute-start(bf16[1,4,16,768]{3,2,1,0:T(8,128)(2,1)S(1)} %dynamic-slice_bitcast_fusion), channel_id=1, source_target_pairs={{0,4},{4,0},{1,5},{5,1},{2,6},{6,2},{3,7},{7,3},{8,12},{12,8},{9,1... | collective-permute-start | bytes 294920 | tf_op jit(solution)/shard_map/ppermute | solution.py:31
  23.1 59.7 %collective-permute-start.5 = (f32[2,128]{1,0:T(2,128)S(1)}, f32[2,128]{1,0:T(2,128)S(1)}, u32[]{:S(2)}, u32[]{:S(2)}) collective-permute-start(f32[2,128]{1,0:T(2,128)S(1)} %bitcast.121), channel_id=1, source_target_pairs={{0,4},{4,0},{1,5},{5,1},{2,6},{6,2},{3,7},{7,3},{8,12},{12,8},{9,1... | collective-permute-start | bytes 3080 | tf_op jit(solution)/shard_map/ppermute | solution.py:31
  25.1 57.8 %collective-permute-start.4 = (bf16[2048,256]{1,0:T(8,128)(2,1)S(1)}, bf16[2048,256]{1,0:T(8,128)(2,1)S(1)}, u32[]{:S(2)}, u32[]{:S(2)}) collective-permute-start(bf16[2048,256]{1,0:T(8,128)(2,1)S(1)} %copy-done), channel_id=1, source_target_pairs={{0,4},{4,0},{1,5},{5,1},{2,6},{6,2},{3,7},{7,3},{8,12},{12,8},{9,1... | collective-permute-start | bytes 3145736 | tf_op jit(solution)/shard_map/ppermute | solution.py:31
  27.6 13.0 %collective-permute-start.3 = (bf16[1,2,16,768]{3,2,1,0:T(8,128)(2,1)S(1)}, bf16[1,2,16,768]{3,2,1,0:T(8,128)(2,1)S(1)}, u32[]{:S(2)}, u32[]{:S(2)}) collective-permute-start(bf16[1,2,16,768]{3,2,1,0:T(8,128)(2,1)S(1)} %get-tuple-element.44), channel_id=1, source_target_pairs={{0,24},{8,16},{16,8},{24,0},{1,25},{9,17},{17,9},{25,1},{2,26},{10... | collective-permute-start | bytes 147464 | tf_op jit(solution)/shard_map/ppermute | solution.py:31
  32.0 5.3 %collective-permute-start.1 = (bf16[1,2,16,768]{3,2,1,0:T(8,128)(2,1)S(1)}, bf16[1,2,16,768]{3,2,1,0:T(8,128)(2,1)S(1)}, u32[]{:S(2)}, u32[]{:S(2)}) collective-permute-start(bf16[1,2,16,768]{3,2,1,0:T(8,128)(2,1)S(1)} %get-tuple-element.45), channel_id=1, source_target_pairs={{0,8},{8,0},{16,24},{24,16},{1,9},{9,1},{17,25},{25,17},{2,10},{10... | collective-permute-start | bytes 147464 | tf_op jit(solution)/shard_map/ppermute | solution.py:31
  33.9 6.6 %collective-permute-start.2 = (bf16[1,2,16,768]{3,2,1,0:T(8,128)(2,1)S(1)}, bf16[1,2,16,768]{3,2,1,0:T(8,128)(2,1)S(1)}, u32[]{:S(2)}, u32[]{:S(2)}) collective-permute-start(bf16[1,2,16,768]{3,2,1,0:T(8,128)(2,1)S(1)} %get-tuple-element.46), channel_id=1, source_target_pairs={{0,16},{8,24},{16,0},{24,8},{1,17},{9,25},{17,1},{25,9},{2,18},{10... | collective-permute-start | bytes 147464 | tf_op jit(solution)/shard_map/ppermute | solution.py:31
  37.3 3.3 %copy-start.7 = (bf16[256,256]{1,0:T(8,128)(2,1)S(1)}, bf16[256,256]{1,0:T(8,128)(2,1)}, u32[]{:S(2)}) copy-start(bf16[256,256]{1,0:T(8,128)(2,1)} %constant.114.clone) | copy-start | bytes 393220
  41.8 11.7 %all-to-all-start.1 = ((f32[8,32,128]{2,1,0:T(8,128)}), f32[8,32,128]{2,1,0:T(8,128)S(1)}, u32[]{:S(2)}, u32[]{:S(2)}) async-start(f32[8,32,128]{2,1,0:T(8,128)} %fusion.59), calls=%async_computation.1 | async-start | bytes 262144 | tf_op jit(solution)/shard_map/all_to_all | solution.py:23
  54.3 21.9 %all-to-all-start.2 = ((bf16[16,32,128]{2,1,0:T(8,128)(2,1)}), bf16[16,32,128]{2,1,0:T(8,128)(2,1)S(1)}, u32[]{:S(2)}, u32[]{:S(2)}) async-start(bf16[16,32,128]{2,1,0:T(8,128)(2,1)} %broadcast_in_dim.31), calls=%async_computation.2 | async-start | bytes 262144 | tf_op jit(solution)/shard_map/all_to_all | solution.py:23
  65.2 11.1 %copy-start.1 = (f32[2048]{0:T(1024)S(1)}, f32[2048]{0:T(1024)}, u32[]{:S(2)}) copy-start(f32[2048]{0:T(1024)} %param.11) | copy-start | bytes 24580
  77.7 10.4 %all-to-all-start.3 = ((bf16[4,32,2048]{2,1,0:T(8,128)(2,1)}), bf16[4,32,2048]{2,1,0:T(8,128)(2,1)S(1)}, u32[]{:S(2)}, u32[]{:S(2)}) async-start(bf16[4,32,2048]{2,1,0:T(8,128)(2,1)} %broadcast_in_dim.32), calls=%async_computation.3 | async-start | bytes 1048576 | tf_op jit(solution)/shard_map/all_to_all | solution.py:23
  90.8 3.6 %copy-start.2 = (f32[128,2048]{1,0:T(8,128)S(1)}, f32[128,2048]{1,0:T(8,128)}, u32[]{:S(2)}) copy-start(f32[128,2048]{1,0:T(8,128)} %fusion.7) | copy-start | bytes 3145732
  90.8 17.7 %all-to-all-start.4 = ((bf16[4,32,2176]{2,1,0:T(8,128)(2,1)}), bf16[4,32,2176]{2,1,0:T(8,128)(2,1)S(1)}, u32[]{:S(2)}, u32[]{:S(2)}) async-start(bf16[4,32,2176]{2,1,0:T(8,128)(2,1)} %get-tuple-element.18), calls=%async_computation.4 | async-start | bytes 1114112 | tf_op jit(solution)/shard_map/all_to_all | solution.py:23
  95.0 9.0 %collective-permute-start.8 = (bf16[32,2048]{1,0:T(8,128)(2,1)S(1)}, bf16[32,2048]{1,0:T(8,128)(2,1)S(1)}, u32[]{:S(2)}, u32[]{:S(2)}) collective-permute-start(bf16[32,2048]{1,0:T(8,128)(2,1)S(1)} %get-tuple-element.36), channel_id=1, source_target_pairs={{0,24},{8,16},{16,8},{24,0},{1,25},{9,17},{17,9},{25,1},{2,26},{10... | collective-permute-start | bytes 393224 | tf_op jit(solution)/shard_map/ppermute | solution.py:31
  99.5 9.0 %collective-permute-start.7 = (bf16[32,2048]{1,0:T(8,128)(2,1)S(1)}, bf16[32,2048]{1,0:T(8,128)(2,1)S(1)}, u32[]{:S(2)}, u32[]{:S(2)}) collective-permute-start(bf16[32,2048]{1,0:T(8,128)(2,1)S(1)} %get-tuple-element.37), channel_id=1, source_target_pairs={{0,16},{8,24},{16,0},{24,8},{1,17},{9,25},{17,1},{25,9},{2,18},{10... | collective-permute-start | bytes 393224 | tf_op jit(solution)/shard_map/ppermute | solution.py:31
  102.0 6.5 %collective-permute-start.6 = (bf16[32,2048]{1,0:T(8,128)(2,1)S(1)}, bf16[32,2048]{1,0:T(8,128)(2,1)S(1)}, u32[]{:S(2)}, u32[]{:S(2)}) collective-permute-start(bf16[32,2048]{1,0:T(8,128)(2,1)S(1)} %get-tuple-element.38), channel_id=1, source_target_pairs={{0,8},{8,0},{16,24},{24,16},{1,9},{9,1},{17,25},{25,17},{2,10},{10... | collective-permute-start | bytes 393224 | tf_op jit(solution)/shard_map/ppermute | solution.py:31
  109.2 18.8 %all-to-all-start.5 = ((f32[16,2,128]{2,1,0:T(2,128)}), f32[16,2,128]{2,1,0:T(2,128)S(1)}, u32[]{:S(2)}, u32[]{:S(2)}) async-start(f32[16,2,128]{2,1,0:T(2,128)} %broadcast_in_dim.37), calls=%async_computation.5 | async-start | bytes 32768 | tf_op jit(solution)/shard_map/all_to_all | solution.py:23
  117.3 30.8 %collective-permute-start.12 = (bf16[128,512]{1,0:T(8,128)(2,1)}, bf16[128,512]{1,0:T(8,128)(2,1)S(1)}, u32[]{:S(2)}, u32[]{:S(2)}) collective-permute-start(bf16[128,512]{1,0:T(8,128)(2,1)} %get-tuple-element.34), channel_id=1, source_target_pairs={{0,3},{1,2},{2,1},{3,0},{4,7},{5,6},{6,5},{7,4},{8,11},{9,10},{10,... | collective-permute-start | bytes 393224 | tf_op jit(solution)/shard_map/ppermute | solution.py:31
  122.0 26.8 %collective-permute-start.9 = (bf16[128,512]{1,0:T(8,128)(2,1)}, bf16[128,512]{1,0:T(8,128)(2,1)S(1)}, u32[]{:S(2)}, u32[]{:S(2)}) collective-permute-start(bf16[128,512]{1,0:T(8,128)(2,1)} %get-tuple-element.35), channel_id=1, source_target_pairs={{0,2},{1,3},{2,0},{3,1},{4,6},{5,7},{6,4},{7,5},{8,10},{9,11},{10,... | collective-permute-start | bytes 393224 | tf_op jit(solution)/shard_map/ppermute | solution.py:31
  128.7 19.4 %collective-permute-start.13 = (bf16[128,512]{1,0:T(8,128)(2,1)S(1)}, bf16[128,512]{1,0:T(8,128)(2,1)S(1)}, u32[]{:S(2)}, u32[]{:S(2)}) collective-permute-start(bf16[128,512]{1,0:T(8,128)(2,1)S(1)} %constant_dynamic-update-slice_fusion), channel_id=1, source_target_pairs={{0,3},{1,2},{2,1},{3,0},{4,7},{5,6},{6,5},{7,4},{8,11},{9,10},{10,... | collective-permute-start | bytes 393224 | tf_op jit(solution)/shard_map/ppermute | solution.py:31
  133.3 15.4 %collective-permute-start.10 = (bf16[128,512]{1,0:T(8,128)(2,1)S(1)}, bf16[128,512]{1,0:T(8,128)(2,1)S(1)}, u32[]{:S(2)}, u32[]{:S(2)}) collective-permute-start(bf16[128,512]{1,0:T(8,128)(2,1)S(1)} %constant_dynamic-update-slice_fusion), channel_id=1, source_target_pairs={{0,2},{1,3},{2,0},{3,1},{4,6},{5,7},{6,4},{7,5},{8,10},{9,11},{10,... | collective-permute-start | bytes 393224 | tf_op jit(solution)/shard_map/ppermute | solution.py:31
  136.9 23.3 %all-to-all-start.6 = ((bf16[16,2,2048]{2,1,0:T(2,128)(2,1)}), bf16[16,2,2048]{2,1,0:T(2,128)(2,1)S(1)}, u32[]{:S(2)}, u32[]{:S(2)}) async-start(bf16[16,2,2048]{2,1,0:T(2,128)(2,1)} %reshape.149), calls=%async_computation.6 | async-start | bytes 262144 | tf_op jit(solution)/shard_map/all_to_all | solution.py:23
  144.2 7.1 %collective-permute-start.11 = (bf16[128,1024]{1,0:T(8,128)(2,1)S(1)}, bf16[128,1024]{1,0:T(8,128)(2,1)S(1)}, u32[]{:S(2)}, u32[]{:S(2)}) collective-permute-start(bf16[128,1024]{1,0:T(8,128)(2,1)S(1)} %pad_maximum_fusion), channel_id=1, source_target_pairs={{0,1},{1,0},{2,3},{3,2},{4,5},{5,4},{6,7},{7,6},{8,9},{9,8},{10,11... | collective-permute-start | bytes 786440 | tf_op jit(solution)/shard_map/ppermute | solution.py:31
  151.3 8.1 %copy-start.9 = (bf16[128,512]{1,0:T(8,128)(2,1)S(1)}, bf16[128,512]{1,0:T(8,128)(2,1)}, u32[]{:S(2)}) copy-start(bf16[128,512]{1,0:T(8,128)(2,1)} %copy-done.8) | copy-start | bytes 393220
  151.6 8.1 %copy-start.5 = (bf16[128,512]{1,0:T(8,128)(2,1)S(1)}, bf16[128,512]{1,0:T(8,128)(2,1)}, u32[]{:S(2)}) copy-start(bf16[128,512]{1,0:T(8,128)(2,1)} %copy-done.4) | copy-start | bytes 393220
  151.6 8.1 %copy-start.11 = (bf16[128,512]{1,0:T(8,128)(2,1)S(1)}, bf16[128,512]{1,0:T(8,128)(2,1)}, u32[]{:S(2)}) copy-start(bf16[128,512]{1,0:T(8,128)(2,1)} %copy-done.10) | copy-start | bytes 393220
  151.6 9.5 %collective-permute-start.14 = (f32[512,256]{1,0:T(8,128)S(1)}, f32[512,256]{1,0:T(8,128)S(1)}, u32[]{:S(2)}, u32[]{:S(2)}) collective-permute-start(f32[512,256]{1,0:T(8,128)S(1)} %fusion.2), channel_id=1, source_target_pairs={{0,4},{4,0},{1,5},{5,1},{2,6},{6,2},{3,7},{7,3},{8,12},{12,8},{9,1... | collective-permute-start | bytes 1572872 | tf_op jit(solution)/shard_map/ppermute | solution.py:31
  (5 other events, 3.3 us)

commit v3 on v0

--- a/solution.py
+++ b/solution.py
@@ -53,6 +53,48 @@
     scaled = jnp.sum(row_ref[...].astype(f32), axis=0) * gain_ref[...]
     mean = jnp.mean(values * scaled, axis=1, keepdims=True)
     out_ref[...] = inv * (scaled - values * inv * inv * mean)
+
+
+def head_kernel(base_ref, normed_ref, own_ref, other_ref, bias_ref, goals_ref, stats_ref, scores_ref):
+    half, ncols = normed_ref.shape[0], own_ref.shape[1]
+    vocab = (own_ref, other_ref)
+    normed, goals = normed_ref[...], goals_ref[...]
+    scores = [dot(normed, v[...], 1, 0) + bias_ref[k : k + 1] for k, v in enumerate(vocab)]
+    ids = lax.broadcasted_iota(jnp.int32, (half, ncols), 1)
+    hit = [ids + base_ref[k] == goals for k in range(2)]
+    top = jnp.maximum(*(jnp.max(s, axis=1, keepdims=True) for s in scores))
+    total = sum(jnp.sum(jnp.exp(s - top), axis=1, keepdims=True) for s in scores)
+    goal = sum(jnp.sum(jnp.where(h, s, 0.0), axis=1, keepdims=True) for h, s in zip(hit, scores))
+    lane = lax.broadcasted_iota(jnp.int32, (half, half), 1)
+    both = jnp.where(lane == 0, top + jnp.log(total), jnp.where(lane == 1, goal, 0.0)).T[:2]
+    for k in range(stats_ref.shape[0]):
+        stats_ref[k] = both
+    for k in range(2):
+        scores_ref[k] = scores[k]
+
+
+def rows_kernel(base_ref, stats_ref, scores_ref, own_ref, other_ref, goals_ref, block_ref, dscore_ref, losses_ref):
+    ncols = own_ref.shape[1]
+    blocks, span, width = block_ref.shape
+    half = blocks * span
+    stats = stats_ref[...]
+    tops = jnp.max(stats, axis=0)
+    lse = tops + jnp.log(jnp.sum(jnp.exp(stats - tops), axis=0))
+    lse, goal = lse[:1], jnp.sum(stats, axis=0)[1:]
+    losses_ref[...] = lse - goal + zloss_weight * lse * lse
+    lse = jnp.broadcast_to(lse, (half, half)).T[:, :1]
+    scale = 1.0 + 2.0 * zloss_weight * lse
+    ids = lax.broadcasted_iota(jnp.int32, (half, ncols), 1)
+    dscore = []
+    for k in range(2):
+        hit = ids + base_ref[k] == goals_ref[...]
+        d = jnp.exp(scores_ref[k] - lse) * scale - jnp.where(hit, 1.0, 0.0)
+        dscore.append(d.astype(bf16))
+        dscore_ref[:, k * ncols : (k + 1) * ncols] = dscore[k]
+    for at in range(0, width, 512):
+        terms = sum(dot(d, v[at : at + 512], 1, 1) for d, v in zip(dscore, (own_ref, other_ref))).astype(bf16)
+        for k in range(blocks):
+            block_ref[k, :, at : at + 512] = terms[k * span : (k + 1) * span]
 
 
 def body(stream, hidden, w_down, final_gain, vocab, vocab_bias, targets):
@@ -109,37 +151,54 @@
     token = (line // own) % nz * (nq * own) + line // span * (nc * own) + c * own + line % own
     goals = jnp.where(token == lax.broadcasted_iota(jnp.int32, (half, group), 1), targets[None, :], 0)
     goals = jnp.sum(goals, axis=1)
-    ids = lax.broadcasted_iota(jnp.int32, (half, ncols), 1)
-    hit = [ids + k * ncols == goals[:, None] for k in (mine, mine ^ 1)]
     feat_group, last = width // ny, ny - 1
     early = lax.dynamic_slice_in_dim(normed, (y ^ last) * feat_group, feat_group, 1)
     early = partner(early, "dp", last)
 
-    scores = [dot(normed, v, 1, 0) + b for v, b in zip(vocab, bias)]
-    top = jnp.maximum(jnp.max(scores[0], axis=1), jnp.max(scores[1], axis=1))
-    total = sum(jnp.sum(jnp.exp(s - top[:, None]), axis=1) for s in scores)
-    goal = sum(jnp.sum(jnp.where(h, s, 0.0), axis=1) for h, s in zip(hit, scores))
-    stats = jnp.stack([top + jnp.log(total), goal])
-    stats = merged(shared(stats, X, nx))
-    stats = merged(shared(stats, Z, nz))
-    lse, goal = stats
-    losses = lse - goal + zloss_weight * lse * lse
-    losses = lax.dynamic_slice_in_dim(losses, x * span + z * own, own)
-    scale = 1.0 + 2.0 * zloss_weight * lse
-    dscore = [
-        (jnp.exp(s - lse[:, None]) * scale[:, None] - jnp.where(h, 1.0, 0.0)).astype(bf16)
-        for s, h in zip(scores, hit)
-    ]
-    row_term = sum(dot(d, v, 1, 1) for d, v in zip(dscore, vocab)).astype(bf16)
-
-    row_term, *dscore = lax.optimization_barrier((row_term, *dscore))
+    vmem, smem = (pl.BlockSpec(memory_space=m) for m in (pltpu.VMEM, pltpu.SMEM))
+    base, goals = jnp.stack([mine * ncols, (mine ^ 1) * ncols]), goals[:, None]
+    params = pltpu.CompilerParams(vmem_limit_bytes=24 << 20)
+    cost = pl.CostEstimate(
+        flops=4 * half * ncols * width, bytes_accessed=4 * ncols * width, transcendentals=2 * half * ncols
+    )
+    stats, scores = pl.pallas_call(
+        head_kernel,
+        out_shape=(
+            jax.ShapeDtypeStruct((nx, 2, half), f32),
+            jax.ShapeDtypeStruct((2, half, ncols), f32),
+        ),
+        in_specs=[smem] + [vmem] * 5,
+        out_specs=(vmem,) * 2,
+        compiler_params=params,
+        cost_estimate=cost,
+    )(base, normed, *vocab, jnp.stack(bias), goals)
+    stats = merged(exchange(stats, X))
+    stats = shared(stats, Z, nz)
+    row_term, dscore, losses = pl.pallas_call(
+        rows_kernel,
+        out_shape=(
+            jax.ShapeDtypeStruct((nx, span, width), bf16),
+            jax.ShapeDtypeStruct((half, 2 * ncols), bf16),
+            jax.ShapeDtypeStruct((1, half), f32),
+        ),
+        in_specs=[smem] + [vmem] * 5,
+        out_specs=(vmem,) * 3,
+        compiler_params=params,
+        cost_estimate=cost,
+    )(base, stats, scores, *vocab, goals)
+    row_term, dscore, losses = lax.optimization_barrier((row_term, dscore, losses))
+    losses = lax.dynamic_slice_in_dim(losses[0], x * span + z * own, own)
+
+    row_x = exchange(row_term, X)
+    row_x = jnp.sum(row_x.astype(f32), axis=0).astype(bf16)
+    early, row_x = lax.optimization_barrier((early, row_x))
+    early = lax.optimization_barrier(jnp.where(c >= 0, early, 0))
     theirs, ours = 0.0, 0.0
     for step in (0, ny // 2, 1, last):
-        cols_of = jnp.concatenate(dscore, axis=1)
         if step == last:
-            piece, cols_of = early, partner(cols_of, "dp", step)
+            piece, cols_of = early, partner(dscore, "dp", step)
         else:
-            piece = lax.dynamic_slice_in_dim(normed, (y ^ step) * feat_group, feat_group, 1)
+            piece, cols_of = lax.dynamic_slice_in_dim(normed, (y ^ step) * feat_group, feat_group, 1), dscore
             if step:
                 piece = partner(jnp.concatenate([piece, cols_of], axis=1), "dp", step)
                 piece, cols_of = piece[:, :feat_group], piece[:, feat_group:]
@@ -147,8 +206,6 @@
         ours = ours + dot(piece, cols_of[:, :ncols], 0, 0)
     grad_vocab = lax.optimization_barrier(ours) + partner(theirs, C, 1)
 
-    row_x = exchange(row_term.reshape(nx, span, width), X)
-    row_x = jnp.sum(row_x.astype(f32), axis=0).astype(bf16)
     row_z = exchange(row_x.reshape(nz, own, width), Z)
     gathered, _ = lax.optimization_barrier((gathered, row_x))
     normin = lax.dynamic_slice_in_dim(gathered, z * own, own, 1).transpose(1, 0, 2).reshape(own, width)

time: 162 us -> 161 us (level)
  the two profiles are of different devices: /device:TPU:34 before, /device:TPU:32 now
where the time goes in v3:
time: 161 us; the launch traced here: 160 us
  starting transfers between devices  77.2 us (48%)
  waiting for transfers between devices  50.4 us (31%)
  blocking collectives  10.2 us (6%)
  local copies, waits for them, and re-layouts  7.91 us (5%)
  Pallas kernels  4.91 us (3%)
  matrix products  4.28 us (3%)
  other arithmetic  4.21 us (3%)
    all_to_all x7, starting transfers between devices, exchange(): return lax.all_to_all(blocks, axes, split_axis=0, concat_axis=0, tiled=True)  44.6 us
    all_to_all x7, waiting for transfers between devices, exchange(): return lax.all_to_all(blocks, axes, split_axis=0, concat_axis=0, tiled=True)  44.5 us
    ppermute x11, starting transfers between devices, partner(): lax.ppermute(array, axes, [(k, k ^ step) for k in range(lax.axis_size(axe...  32.7 us
    all_to_all x1, blocking collectives, exchange(): return lax.all_to_all(blocks, axes, split_axis=0, concat_axis=0, tiled=True)  10.2 us
    ppermute x11, waiting for transfers between devices, partner(): lax.ppermute(array, axes, [(k, k ^ step) for k in range(lax.axis_size(axe...  5.97 us
    dot_general x10, matrix products, dot(): lax.dot_general(a, b, (((da,), (db,)), ((), ())), preferred_element_type=...  4.28 us
  transfers between devices with their start and end apart: 18, of which 10 were waited for; matrix products, arithmetic and copies ran while one was open for 7% of the time, Pallas kernels for 1%

profile of v3, /device:TPU:32, one launch (start us, length us, event | category | flops | bytes accessed | tf_op | source)
XLA Modules:
  0.0 160.4 jit_solution(17829267620250314488)
XLA Ops:
  2.2 15.3 %all-to-all-start = ((bf16[16,48,256]{2,1,0:T(8,128)(2,1)}), bf16[16,48,256]{2,1,0:T(8,128)(2,1)S(1)}, u32[]{:S(2)}, u32[]{:S(2)}) async-start(bf16[16,48,256]{2,1,0:T(8,128)(2,1)} %pad_add_fusion), calls=%async_computation | async-start | bytes 786432 | tf_op jit(solution)/shard_map/all_to_all | solution.py:23
  17.5 1.5 reshape.114
  19.7 1.9 %collective-permute-start = (bf16[1,4,16,768]{3,2,1,0:T(8,128)(2,1)S(1)}, bf16[1,4,16,768]{3,2,1,0:T(8,128)(2,1)S(1)}, u32[]{:S(2)}, u32[]{:S(2)}) collective-permute-start(bf16[1,4,16,768]{3,2,1,0:T(8,128)(2,1)S(1)} %dynamic-slice_bitcast_fusion), channel_id=1, source_target_pairs={{0,4},{4,0},{1,5},{5,1},{2,6},{6,2},{3,7},{7,3},{8,12},{12,8},{9,1... | collective-permute-start | bytes 294920 | tf_op jit(solution)/shard_map/ppermute | solution.py:31
  21.7 1.2 collective-permute-done
  23.0 3.4 %collective-permute-start.1 = (bf16[1,2,16,768]{3,2,1,0:T(8,128)(2,1)S(1)}, bf16[1,2,16,768]{3,2,1,0:T(8,128)(2,1)S(1)}, u32[]{:S(2)}, u32[]{:S(2)}) collective-permute-start(bf16[1,2,16,768]{3,2,1,0:T(8,128)(2,1)S(1)} %get-tuple-element.31), channel_id=1, source_target_pairs={{0,8},{8,0},{16,24},{24,16},{1,9},{9,1},{17,25},{25,17},{2,10},{10... | collective-permute-start | bytes 147464 | tf_op jit(solution)/shard_map/ppermute | solution.py:31
  26.4 4.6 %collective-permute-start.2 = (bf16[1,2,16,768]{3,2,1,0:T(8,128)(2,1)S(1)}, bf16[1,2,16,768]{3,2,1,0:T(8,128)(2,1)S(1)}, u32[]{:S(2)}, u32[]{:S(2)}) collective-permute-start(bf16[1,2,16,768]{3,2,1,0:T(8,128)(2,1)S(1)} %get-tuple-element.32), channel_id=1, source_target_pairs={{0,16},{8,24},{16,0},{24,8},{1,17},{9,25},{17,1},{25,9},{2,18},{10... | collective-permute-start | bytes 147464 | tf_op jit(solution)/shard_map/ppermute | solution.py:31
  31.0 2.4 %collective-permute-start.3 = (bf16[1,2,16,768]{3,2,1,0:T(8,128)(2,1)S(1)}, bf16[1,2,16,768]{3,2,1,0:T(8,128)(2,1)S(1)}, u32[]{:S(2)}, u32[]{:S(2)}) collective-permute-start(bf16[1,2,16,768]{3,2,1,0:T(8,128)(2,1)S(1)} %get-tuple-element.30), channel_id=1, source_target_pairs={{0,24},{8,16},{16,8},{24,0},{1,25},{9,17},{17,9},{25,1},{2,26},{10... | collective-permute-start | bytes 147464 | tf_op jit(solution)/shard_map/ppermute | solution.py:31
  33.9 4.3 %collective-permute-done.3 = bf16[1,2,16,768]{3,2,1,0:T(8,128)(2,1)S(1)} collective-permute-done((bf16[1,2,16,768]{3,2,1,0:T(8,128)(2,1)S(1)}, bf16[1,2,16,768]{3,2,1,0:T(8,128)(2,1)S(1)}, u32[]{:S(2)}, u32[]{:S(2)}) %collective-permute-start.3) | collective-permute-done | bytes 49184 | tf_op jit(solution)/shard_map/ppermute | solution.py:31
  38.2 1.1 all-to-all-done
  39.9 10.2 %all_to_all.40 = f32[8,32,128]{2,1,0:T(8,128)S(1)} all-to-all(f32[8,32,128]{2,1,0:T(8,128)S(1)} %fusion.42), channel_id=1, replica_groups=mesh['vp_0'=16,'vp_1'=4,'vp_2'=2,'dp'=4] {'vp_1','vp_2'}, dimensions={0} | all-to-all | bytes 262144 | tf_op jit(solution)/shard_map/all_to_all | solution.py:23
  50.8 9.2 %all-to-all-start.2 = ((bf16[16,32,128]{2,1,0:T(8,128)(2,1)}), bf16[16,32,128]{2,1,0:T(8,128)(2,1)S(1)}, u32[]{:S(2)}, u32[]{:S(2)}) async-start(bf16[16,32,128]{2,1,0:T(8,128)(2,1)} %broadcast_in_dim.26), calls=%async_computation.2 | async-start | bytes 262144 | tf_op jit(solution)/shard_map/all_to_all | solution.py:23
  60.1 1.9 %collective-permute-start.4 = (bf16[2048,256]{1,0:T(8,128)(2,1)S(1)}, bf16[2048,256]{1,0:T(8,128)(2,1)S(1)}, u32[]{:S(2)}, u32[]{:S(2)}) collective-permute-start(bf16[2048,256]{1,0:T(8,128)(2,1)S(1)} %copy-done), channel_id=1, source_target_pairs={{0,4},{4,0},{1,5},{5,1},{2,6},{6,2},{3,7},{7,3},{8,12},{12,8},{9,1... | collective-permute-start | bytes 3145736 | tf_op jit(solution)/shard_map/ppermute | solution.py:31
  62.0 2.4 %collective-permute-start.5 = (f32[2,128]{1,0:T(2,128)S(1)}, f32[2,128]{1,0:T(2,128)S(1)}, u32[]{:S(2)}, u32[]{:S(2)}) collective-permute-start(f32[2,128]{1,0:T(2,128)S(1)} %bitcast.84), channel_id=1, source_target_pairs={{0,4},{4,0},{1,5},{5,1},{2,6},{6,2},{3,7},{7,3},{8,12},{12,8},{9,1... | collective-permute-start | bytes 3080 | tf_op jit(solution)/shard_map/ppermute | solution.py:31
  64.5 9.5 %all-to-all-done.2 = bf16[16,32,128]{2,1,0:T(8,128)(2,1)S(1)} async-done(((bf16[16,32,128]{2,1,0:T(8,128)(2,1)}), bf16[16,32,128]{2,1,0:T(8,128)(2,1)S(1)}, u32[]{:S(2)}, u32[]{:S(2)}) %all-to-all-start.2) | async-done | bytes 131104 | tf_op jit(solution)/shard_map/all_to_all | solution.py:23
  75.1 3.5 %all-to-all-start.3 = ((bf16[4,32,2048]{2,1,0:T(8,128)(2,1)}), bf16[4,32,2048]{2,1,0:T(8,128)(2,1)S(1)}, u32[]{:S(2)}, u32[]{:S(2)}) async-start(bf16[4,32,2048]{2,1,0:T(8,128)(2,1)} %broadcast_in_dim.27), calls=%async_computation.3 | async-start | bytes 1048576 | tf_op jit(solution)/shard_map/all_to_all | solution.py:23
  79.8 6.8 %all-to-all-done.3 = bf16[4,32,2048]{2,1,0:T(8,128)(2,1)S(1)} async-done(((bf16[4,32,2048]{2,1,0:T(8,128)(2,1)}), bf16[4,32,2048]{2,1,0:T(8,128)(2,1)S(1)}, u32[]{:S(2)}, u32[]{:S(2)}) %all-to-all-start.3) | async-done | bytes 524320 | tf_op jit(solution)/shard_map/all_to_all | solution.py:23
  86.6 1.8 %shard_map.103 = (f32[4,2,128]{2,1,0:T(2,128)}, f32[2,128,256]{2,1,0:T(8,128)S(1)}) custom-call(s32[2]{0:T(128)S(1)} %pad_add_fusion.1.base_ref, bf16[128,2048]{1,0:T(8,128)(2,1)S(1)} %bitcast.68, bf16[2048,256]{1,0:T(8,128)(2,1)S(1)} %copy-done, bf16[2048,256]{1,0:T(8,128)(2,1)S(1)} %collective-permute-done.4.other_ref, ...), custom_call_target="tpu_custom_call" | custom-call | flops 268435456 | bytes 2097152 | tf_op jit(solution)/shard_map/pallas_call | solution.py:164
  88.4 3.2 %all-to-all-start.4 = ((f32[4,2,128]{2,1,0:T(2,128)}), f32[4,2,128]{2,1,0:T(2,128)S(1)}, u32[]{:S(2)}, u32[]{:S(2)}) async-start(f32[4,2,128]{2,1,0:T(2,128)} %get-tuple-element.15), calls=%async_computation.4 | async-start | bytes 8192 | tf_op jit(solution)/shard_map/all_to_all | solution.py:23
  91.7 5.2 %all-to-all-done.4 = f32[4,2,128]{2,1,0:T(2,128)S(1)} async-done(((f32[4,2,128]{2,1,0:T(2,128)}), f32[4,2,128]{2,1,0:T(2,128)S(1)}, u32[]{:S(2)}, u32[]{:S(2)}) %all-to-all-start.4) | async-done | bytes 4128 | tf_op jit(solution)/shard_map/all_to_all | solution.py:23
  97.6 5.1 %all-to-all-start.5 = ((f32[16,2,128]{2,1,0:T(2,128)}), f32[16,2,128]{2,1,0:T(2,128)S(1)}, u32[]{:S(2)}, u32[]{:S(2)}) async-start(f32[16,2,128]{2,1,0:T(2,128)} %broadcast_in_dim.51), calls=%async_computation.5 | async-start | bytes 32768 | tf_op jit(solution)/shard_map/all_to_all | solution.py:23
  103.4 10.6 %all-to-all-done.5.stats_ref = f32[16,2,128]{2,1,0:T(2,128)S(1)} async-done(((f32[16,2,128]{2,1,0:T(2,128)}), f32[16,2,128]{2,1,0:T(2,128)S(1)}, u32[]{:S(2)}, u32[]{:S(2)}) %all-to-all-start.5) | async-done | bytes 16416 | tf_op jit(solution)/shard_map/all_to_all | solution.py:23
  114.0 2.3 %shard_map.104 = (bf16[4,32,2048]{2,1,0:T(8,128)(2,1)}, bf16[128,512]{1,0:T(8,128)(2,1)S(1)}, f32[1,128]{1,0:T(1,128)S(1)}) custom-call(s32[2]{0:T(128)S(1)} %pad_add_fusion.1.base_ref, f32[16,2,128]{2,1,0:T(2,128)S(1)} %all-to-all-done.5.stats_ref, f32[2,128,256]{2,1,0:T(8,128)S(1)} %get-tuple-element.16.scores_ref, bf16[2048,256]{1,0:T(8,128)(2,1)S(1)} %copy-done, ...), custom_call_target="tpu_custom_call" | custom-call | flops 268435456 | bytes 2097152 | tf_op jit(solution)/shard_map/pallas_call | solution.py:177
  117.0 5.1 %collective-permute-start.7 = (bf16[128,1024]{1,0:T(8,128)(2,1)S(1)}, bf16[128,1024]{1,0:T(8,128)(2,1)S(1)}, u32[]{:S(2)}, u32[]{:S(2)}) collective-permute-start(bf16[128,1024]{1,0:T(8,128)(2,1)S(1)} %get-tuple-element.34), channel_id=1, source_target_pairs={{0,2},{1,3},{2,0},{3,1},{4,6},{5,7},{6,4},{7,5},{8,10},{9,11},{10,... | collective-permute-start | bytes 786440 | tf_op jit(solution)/shard_map/ppermute | solution.py:31
  122.1 3.0 %collective-permute-start.6 = (bf16[128,512]{1,0:T(8,128)(2,1)}, bf16[128,512]{1,0:T(8,128)(2,1)}, u32[]{:S(2)}, u32[]{:S(2)}) collective-permute-start(bf16[128,512]{1,0:T(8,128)(2,1)} %get-tuple-element.27), channel_id=1, source_target_pairs={{0,3},{1,2},{2,1},{3,0},{4,7},{5,6},{6,5},{7,4},{8,11},{9,10},{10,... | collective-permute-start | bytes 393224 | tf_op jit(solution)/shard_map/ppermute | solution.py:31
  125.1 4.1 %collective-permute-start.9 = (bf16[128,512]{1,0:T(8,128)(2,1)S(1)}, bf16[128,512]{1,0:T(8,128)(2,1)}, u32[]{:S(2)}, u32[]{:S(2)}) collective-permute-start(bf16[128,512]{1,0:T(8,128)(2,1)S(1)} %get-tuple-element.21), channel_id=1, source_target_pairs={{0,3},{1,2},{2,1},{3,0},{4,7},{5,6},{6,5},{7,4},{8,11},{9,10},{10,... | collective-permute-start | bytes 393224 | tf_op jit(solution)/shard_map/ppermute | solution.py:31
  129.2 3.5 %all-to-all-start.6 = ((bf16[4,32,2048]{2,1,0:T(8,128)(2,1)}), bf16[4,32,2048]{2,1,0:T(8,128)(2,1)S(1)}, u32[]{:S(2)}, u32[]{:S(2)}) async-start(bf16[4,32,2048]{2,1,0:T(8,128)(2,1)} %get-tuple-element.18), calls=%async_computation.6 | async-start | bytes 1048576 | tf_op jit(solution)/shard_map/all_to_all | solution.py:23
  132.7 1.9 %collective-permute-start.8 = (bf16[128,1024]{1,0:T(8,128)(2,1)}, bf16[128,1024]{1,0:T(8,128)(2,1)S(1)}, u32[]{:S(2)}, u32[]{:S(2)}) collective-permute-start(bf16[128,1024]{1,0:T(8,128)(2,1)} %get-tuple-element.33), channel_id=1, source_target_pairs={{0,1},{1,0},{2,3},{3,2},{4,5},{5,4},{6,7},{7,6},{8,9},{9,8},{10,11... | collective-permute-start | bytes 786440 | tf_op jit(solution)/shard_map/ppermute | solution.py:31
  136.3 4.5 %all-to-all-done.6 = bf16[4,32,2048]{2,1,0:T(8,128)(2,1)S(1)} async-done(((bf16[4,32,2048]{2,1,0:T(8,128)(2,1)}), bf16[4,32,2048]{2,1,0:T(8,128)(2,1)S(1)}, u32[]{:S(2)}, u32[]{:S(2)}) %all-to-all-start.6) | async-done | bytes 524320 | tf_op jit(solution)/shard_map/all_to_all | solution.py:23
  141.6 4.7 %all-to-all-start.7 = ((bf16[16,2,2048]{2,1,0:T(2,128)(2,1)}), bf16[16,2,2048]{2,1,0:T(2,128)(2,1)S(1)}, u32[]{:S(2)}, u32[]{:S(2)}) async-start(bf16[16,2,2048]{2,1,0:T(2,128)(2,1)} %reshape.119), calls=%async_computation.7 | async-start | bytes 262144 | tf_op jit(solution)/shard_map/all_to_all | solution.py:23
  147.2 1.1 fusion.19
  148.6 1.9 %collective-permute-start.10 = (f32[512,256]{1,0:T(8,128)S(1)}, f32[512,256]{1,0:T(8,128)S(1)}, u32[]{:S(2)}, u32[]{:S(2)}) collective-permute-start(f32[512,256]{1,0:T(8,128)S(1)} %fusion.1), channel_id=1, source_target_pairs={{0,4},{4,0},{1,5},{5,1},{2,6},{6,2},{3,7},{7,3},{8,12},{12,8},{9,1... | collective-permute-start | bytes 1572872 | tf_op jit(solution)/shard_map/ppermute | solution.py:31
  151.9 6.7 %all-to-all-done.7.row_ref = bf16[16,2,2048]{2,1,0:T(2,128)(2,1)S(1)} async-done(((bf16[16,2,2048]{2,1,0:T(2,128)(2,1)}), bf16[16,2,2048]{2,1,0:T(2,128)(2,1)S(1)}, u32[]{:S(2)}, u32[]{:S(2)}) %all-to-all-start.7) | async-done | bytes 131104 | tf_op jit(solution)/shard_map/all_to_all | solution.py:23
  (76 shorter events, 15.1 us)
Async XLA Ops:
  0.6 0.8 copy-start.4
  2.2 15.3 %copy-start.2 = (bf16[5632,16]{0,1:T(8,128)(2,1)S(1)}, bf16[5632,16]{0,1:T(8,128)(2,1)}, u32[]{:S(2)}) copy-start(bf16[5632,16]{0,1:T(8,128)(2,1)} %param.10) | copy-start | bytes 540676
  2.2 37.2 %all-to-all-start = ((bf16[16,48,256]{2,1,0:T(8,128)(2,1)}), bf16[16,48,256]{2,1,0:T(8,128)(2,1)S(1)}, u32[]{:S(2)}, u32[]{:S(2)}) async-start(bf16[16,48,256]{2,1,0:T(8,128)(2,1)} %pad_add_fusion), calls=%async_computation | async-start | bytes 786432 | tf_op jit(solution)/shard_map/all_to_all | solution.py:23
  19.7 3.2 %collective-permute-start = (bf16[1,4,16,768]{3,2,1,0:T(8,128)(2,1)S(1)}, bf16[1,4,16,768]{3,2,1,0:T(8,128)(2,1)S(1)}, u32[]{:S(2)}, u32[]{:S(2)}) collective-permute-start(bf16[1,4,16,768]{3,2,1,0:T(8,128)(2,1)S(1)} %dynamic-slice_bitcast_fusion), channel_id=1, source_target_pairs={{0,4},{4,0},{1,5},{5,1},{2,6},{6,2},{3,7},{7,3},{8,12},{12,8},{9,1... | collective-permute-start | bytes 294920 | tf_op jit(solution)/shard_map/ppermute | solution.py:31
  23.0 10.5 %collective-permute-start.1 = (bf16[1,2,16,768]{3,2,1,0:T(8,128)(2,1)S(1)}, bf16[1,2,16,768]{3,2,1,0:T(8,128)(2,1)S(1)}, u32[]{:S(2)}, u32[]{:S(2)}) collective-permute-start(bf16[1,2,16,768]{3,2,1,0:T(8,128)(2,1)S(1)} %get-tuple-element.31), channel_id=1, source_target_pairs={{0,8},{8,0},{16,24},{24,16},{1,9},{9,1},{17,25},{25,17},{2,10},{10... | collective-permute-start | bytes 147464 | tf_op jit(solution)/shard_map/ppermute | solution.py:31
  26.4 7.5 %collective-permute-start.2 = (bf16[1,2,16,768]{3,2,1,0:T(8,128)(2,1)S(1)}, bf16[1,2,16,768]{3,2,1,0:T(8,128)(2,1)S(1)}, u32[]{:S(2)}, u32[]{:S(2)}) collective-permute-start(bf16[1,2,16,768]{3,2,1,0:T(8,128)(2,1)S(1)} %get-tuple-element.32), channel_id=1, source_target_pairs={{0,16},{8,24},{16,0},{24,8},{1,17},{9,25},{17,1},{25,9},{2,18},{10... | collective-permute-start | bytes 147464 | tf_op jit(solution)/shard_map/ppermute | solution.py:31
  31.0 7.2 %collective-permute-start.3 = (bf16[1,2,16,768]{3,2,1,0:T(8,128)(2,1)S(1)}, bf16[1,2,16,768]{3,2,1,0:T(8,128)(2,1)S(1)}, u32[]{:S(2)}, u32[]{:S(2)}) collective-permute-start(bf16[1,2,16,768]{3,2,1,0:T(8,128)(2,1)S(1)} %get-tuple-element.30), channel_id=1, source_target_pairs={{0,24},{8,16},{16,8},{24,0},{1,25},{9,17},{17,9},{25,1},{2,26},{10... | collective-permute-start | bytes 147464 | tf_op jit(solution)/shard_map/ppermute | solution.py:31
  33.4 5.9 %copy-start.3 = (bf16[256,256]{1,0:T(8,128)(2,1)S(1)}, bf16[256,256]{1,0:T(8,128)(2,1)}, u32[]{:S(2)}) copy-start(bf16[256,256]{1,0:T(8,128)(2,1)} %constant.107.clone) | copy-start | bytes 393220
  39.3 20.7 %copy-start = (bf16[2048,256]{1,0:T(8,128)(2,1)S(1)}, bf16[2048,256]{1,0:T(8,128)(2,1)}, u32[]{:S(2)}) copy-start(bf16[2048,256]{1,0:T(8,128)(2,1)} %own_ref.3) | copy-start | bytes 3145732
  50.8 23.1 %all-to-all-start.2 = ((bf16[16,32,128]{2,1,0:T(8,128)(2,1)}), bf16[16,32,128]{2,1,0:T(8,128)(2,1)S(1)}, u32[]{:S(2)}, u32[]{:S(2)}) async-start(bf16[16,32,128]{2,1,0:T(8,128)(2,1)} %broadcast_in_dim.26), calls=%async_computation.2 | async-start | bytes 262144 | tf_op jit(solution)/shard_map/all_to_all | solution.py:23
  60.1 1.9 %copy-start.6 = (f32[256]{0:T(256)S(1)}, f32[256]{0:T(256)}, u32[]{:S(2)}) copy-start(f32[256]{0:T(256)} %param.13) | copy-start | bytes 3076
  60.1 19.7 %collective-permute-start.4 = (bf16[2048,256]{1,0:T(8,128)(2,1)S(1)}, bf16[2048,256]{1,0:T(8,128)(2,1)S(1)}, u32[]{:S(2)}, u32[]{:S(2)}) collective-permute-start(bf16[2048,256]{1,0:T(8,128)(2,1)S(1)} %copy-done), channel_id=1, source_target_pairs={{0,4},{4,0},{1,5},{5,1},{2,6},{6,2},{3,7},{7,3},{8,12},{12,8},{9,1... | collective-permute-start | bytes 3145736 | tf_op jit(solution)/shard_map/ppermute | solution.py:31
  62.0 17.7 %collective-permute-start.5 = (f32[2,128]{1,0:T(2,128)S(1)}, f32[2,128]{1,0:T(2,128)S(1)}, u32[]{:S(2)}, u32[]{:S(2)}) collective-permute-start(f32[2,128]{1,0:T(2,128)S(1)} %bitcast.84), channel_id=1, source_target_pairs={{0,4},{4,0},{1,5},{5,1},{2,6},{6,2},{3,7},{7,3},{8,12},{12,8},{9,1... | collective-permute-start | bytes 3080 | tf_op jit(solution)/shard_map/ppermute | solution.py:31
  64.5 9.6 %copy-start.1 = (f32[2048]{0:T(1024)S(1)}, f32[2048]{0:T(1024)}, u32[]{:S(2)}) copy-start(f32[2048]{0:T(1024)} %param.11) | copy-start | bytes 24580
  75.1 11.5 %all-to-all-start.3 = ((bf16[4,32,2048]{2,1,0:T(8,128)(2,1)}), bf16[4,32,2048]{2,1,0:T(8,128)(2,1)S(1)}, u32[]{:S(2)}, u32[]{:S(2)}) async-start(bf16[4,32,2048]{2,1,0:T(8,128)(2,1)} %broadcast_in_dim.27), calls=%async_computation.3 | async-start | bytes 1048576 | tf_op jit(solution)/shard_map/all_to_all | solution.py:23
  78.6 0.7 copy-start.5
  88.4 8.5 %all-to-all-start.4 = ((f32[4,2,128]{2,1,0:T(2,128)}), f32[4,2,128]{2,1,0:T(2,128)S(1)}, u32[]{:S(2)}, u32[]{:S(2)}) async-start(f32[4,2,128]{2,1,0:T(2,128)} %get-tuple-element.15), calls=%async_computation.4 | async-start | bytes 8192 | tf_op jit(solution)/shard_map/all_to_all | solution.py:23
  97.6 16.4 %all-to-all-start.5 = ((f32[16,2,128]{2,1,0:T(2,128)}), f32[16,2,128]{2,1,0:T(2,128)S(1)}, u32[]{:S(2)}, u32[]{:S(2)}) async-start(f32[16,2,128]{2,1,0:T(2,128)} %broadcast_in_dim.51), calls=%async_computation.5 | async-start | bytes 32768 | tf_op jit(solution)/shard_map/all_to_all | solution.py:23
  117.0 18.2 %collective-permute-start.7 = (bf16[128,1024]{1,0:T(8,128)(2,1)S(1)}, bf16[128,1024]{1,0:T(8,128)(2,1)S(1)}, u32[]{:S(2)}, u32[]{:S(2)}) collective-permute-start(bf16[128,1024]{1,0:T(8,128)(2,1)S(1)} %get-tuple-element.34), channel_id=1, source_target_pairs={{0,2},{1,3},{2,0},{3,1},{4,6},{5,7},{6,4},{7,5},{8,10},{9,11},{10,... | collective-permute-start | bytes 786440 | tf_op jit(solution)/shard_map/ppermute | solution.py:31
  122.1 18.7 %collective-permute-start.6 = (bf16[128,512]{1,0:T(8,128)(2,1)}, bf16[128,512]{1,0:T(8,128)(2,1)}, u32[]{:S(2)}, u32[]{:S(2)}) collective-permute-start(bf16[128,512]{1,0:T(8,128)(2,1)} %get-tuple-element.27), channel_id=1, source_target_pairs={{0,3},{1,2},{2,1},{3,0},{4,7},{5,6},{6,5},{7,4},{8,11},{9,10},{10,... | collective-permute-start | bytes 393224 | tf_op jit(solution)/shard_map/ppermute | solution.py:31
  125.1 22.1 %collective-permute-start.9 = (bf16[128,512]{1,0:T(8,128)(2,1)S(1)}, bf16[128,512]{1,0:T(8,128)(2,1)}, u32[]{:S(2)}, u32[]{:S(2)}) collective-permute-start(bf16[128,512]{1,0:T(8,128)(2,1)S(1)} %get-tuple-element.21), channel_id=1, source_target_pairs={{0,3},{1,2},{2,1},{3,0},{4,7},{5,6},{6,5},{7,4},{8,11},{9,10},{10,... | collective-permute-start | bytes 393224 | tf_op jit(solution)/shard_map/ppermute | solution.py:31
  129.2 11.5 %all-to-all-start.6 = ((bf16[4,32,2048]{2,1,0:T(8,128)(2,1)}), bf16[4,32,2048]{2,1,0:T(8,128)(2,1)S(1)}, u32[]{:S(2)}, u32[]{:S(2)}) async-start(bf16[4,32,2048]{2,1,0:T(8,128)(2,1)} %get-tuple-element.18), calls=%async_computation.6 | async-start | bytes 1048576 | tf_op jit(solution)/shard_map/all_to_all | solution.py:23
  132.7 15.6 %collective-permute-start.8 = (bf16[128,1024]{1,0:T(8,128)(2,1)}, bf16[128,1024]{1,0:T(8,128)(2,1)S(1)}, u32[]{:S(2)}, u32[]{:S(2)}) collective-permute-start(bf16[128,1024]{1,0:T(8,128)(2,1)} %get-tuple-element.33), channel_id=1, source_target_pairs={{0,1},{1,0},{2,3},{3,2},{4,5},{5,4},{6,7},{7,6},{8,9},{9,8},{10,11... | collective-permute-start | bytes 786440 | tf_op jit(solution)/shard_map/ppermute | solution.py:31
  141.6 17.0 %all-to-all-start.7 = ((bf16[16,2,2048]{2,1,0:T(2,128)(2,1)}), bf16[16,2,2048]{2,1,0:T(2,128)(2,1)S(1)}, u32[]{:S(2)}, u32[]{:S(2)}) async-start(bf16[16,2,2048]{2,1,0:T(2,128)(2,1)} %reshape.119), calls=%async_computation.7 | async-start | bytes 262144 | tf_op jit(solution)/shard_map/all_to_all | solution.py:23
  148.6 10.9 %collective-permute-start.10 = (f32[512,256]{1,0:T(8,128)S(1)}, f32[512,256]{1,0:T(8,128)S(1)}, u32[]{:S(2)}, u32[]{:S(2)}) collective-permute-start(f32[512,256]{1,0:T(8,128)S(1)} %fusion.1), channel_id=1, source_target_pairs={{0,4},{4,0},{1,5},{5,1},{2,6},{6,2},{3,7},{7,3},{8,12},{12,8},{9,1... | collective-permute-start | bytes 1572872 | tf_op jit(solution)/shard_map/ppermute | solution.py:31

commit v4 on v3

--- a/solution.py
+++ b/solution.py
@@ -192,7 +192,8 @@
     row_x = exchange(row_term, X)
     row_x = jnp.sum(row_x.astype(f32), axis=0).astype(bf16)
     early, row_x = lax.optimization_barrier((early, row_x))
-    early = lax.optimization_barrier(jnp.where(c >= 0, early, 0))
+    early = jnp.where(c >= 0, early, 0)
+    early = lax.optimization_barrier(early)
     theirs, ours = 0.0, 0.0
     for step in (0, ny // 2, 1, last):
         if step == last:
@@ -204,7 +205,9 @@
                 piece, cols_of = piece[:, :feat_group], piece[:, feat_group:]
         theirs = theirs + dot(piece, cols_of[:, ncols:], 0, 0)
         ours = ours + dot(piece, cols_of[:, :ncols], 0, 0)
-    grad_vocab = lax.optimization_barrier(ours) + partner(theirs, C, 1)
+    theirs = partner(theirs, C, 1)
+    ours = lax.optimization_barrier(ours)
+    grad_vocab = ours + theirs
 
     row_z = exchange(row_x.reshape(nz, own, width), Z)
     gathered, _ = lax.optimization_barrier((gathered, row_x))

time: 161 us -> 161 us (level)
  no operation moved by 1% of the time
where the time goes in v4:
time: 161 us; the launch traced here: 160 us
  starting transfers between devices  77.2 us (48%)
  waiting for transfers between devices  50.4 us (31%)
  blocking collectives  10.2 us (6%)
  local copies, waits for them, and re-layouts  7.91 us (5%)
  Pallas kernels  4.91 us (3%)
  matrix products  4.28 us (3%)
  other arithmetic  4.21 us (3%)
    all_to_all x7, starting transfers between devices, exchange(): return lax.all_to_all(blocks, axes, split_axis=0, concat_axis=0, tiled=True)  44.6 us
    all_to_all x7, waiting for transfers between devices, exchange(): return lax.all_to_all(blocks, axes, split_axis=0, concat_axis=0, tiled=True)  44.5 us
    ppermute x11, starting transfers between devices, partner(): lax.ppermute(array, axes, [(k, k ^ step) for k in range(lax.axis_size(axe...  32.7 us
    all_to_all x1, blocking collectives, exchange(): return lax.all_to_all(blocks, axes, split_axis=0, concat_axis=0, tiled=True)  10.2 us
    ppermute x11, waiting for transfers between devices, partner(): lax.ppermute(array, axes, [(k, k ^ step) for k in range(lax.axis_size(axe...  5.97 us
    dot_general x10, matrix products, dot(): lax.dot_general(a, b, (((da,), (db,)), ((), ())), preferred_element_type=...  4.28 us
  transfers between devices with their start and end apart: 18, of which 10 were waited for; matrix products, arithmetic and copies ran while one was open for 7% of the time, Pallas kernels for 1%

profile of v4, /device:TPU:32, one launch (start us, length us, event | category | flops | bytes accessed | tf_op | source)
XLA Modules:
  0.0 160.4 jit_solution(17829267620250314488)
XLA Ops:
  2.2 15.3 %all-to-all-start = ((bf16[16,48,256]{2,1,0:T(8,128)(2,1)}), bf16[16,48,256]{2,1,0:T(8,128)(2,1)S(1)}, u32[]{:S(2)}, u32[]{:S(2)}) async-start(bf16[16,48,256]{2,1,0:T(8,128)(2,1)} %pad_add_fusion), calls=%async_computation | async-start | bytes 786432 | tf_op jit(solution)/shard_map/all_to_all | solution.py:23
  17.5 1.5 reshape.114
  19.7 1.9 %collective-permute-start = (bf16[1,4,16,768]{3,2,1,0:T(8,128)(2,1)S(1)}, bf16[1,4,16,768]{3,2,1,0:T(8,128)(2,1)S(1)}, u32[]{:S(2)}, u32[]{:S(2)}) collective-permute-start(bf16[1,4,16,768]{3,2,1,0:T(8,128)(2,1)S(1)} %dynamic-slice_bitcast_fusion), channel_id=1, source_target_pairs={{0,4},{4,0},{1,5},{5,1},{2,6},{6,2},{3,7},{7,3},{8,12},{12,8},{9,1... | collective-permute-start | bytes 294920 | tf_op jit(solution)/shard_map/ppermute | solution.py:31
  21.7 1.2 collective-permute-done
  23.0 3.4 %collective-permute-start.1 = (bf16[1,2,16,768]{3,2,1,0:T(8,128)(2,1)S(1)}, bf16[1,2,16,768]{3,2,1,0:T(8,128)(2,1)S(1)}, u32[]{:S(2)}, u32[]{:S(2)}) collective-permute-start(bf16[1,2,16,768]{3,2,1,0:T(8,128)(2,1)S(1)} %get-tuple-element.31), channel_id=1, source_target_pairs={{0,8},{8,0},{16,24},{24,16},{1,9},{9,1},{17,25},{25,17},{2,10},{10... | collective-permute-start | bytes 147464 | tf_op jit(solution)/shard_map/ppermute | solution.py:31
  26.4 4.6 %collective-permute-start.2 = (bf16[1,2,16,768]{3,2,1,0:T(8,128)(2,1)S(1)}, bf16[1,2,16,768]{3,2,1,0:T(8,128)(2,1)S(1)}, u32[]{:S(2)}, u32[]{:S(2)}) collective-permute-start(bf16[1,2,16,768]{3,2,1,0:T(8,128)(2,1)S(1)} %get-tuple-element.32), channel_id=1, source_target_pairs={{0,16},{8,24},{16,0},{24,8},{1,17},{9,25},{17,1},{25,9},{2,18},{10... | collective-permute-start | bytes 147464 | tf_op jit(solution)/shard_map/ppermute | solution.py:31
  31.0 2.4 %collective-permute-start.3 = (bf16[1,2,16,768]{3,2,1,0:T(8,128)(2,1)S(1)}, bf16[1,2,16,768]{3,2,1,0:T(8,128)(2,1)S(1)}, u32[]{:S(2)}, u32[]{:S(2)}) collective-permute-start(bf16[1,2,16,768]{3,2,1,0:T(8,128)(2,1)S(1)} %get-tuple-element.30), channel_id=1, source_target_pairs={{0,24},{8,16},{16,8},{24,0},{1,25},{9,17},{17,9},{25,1},{2,26},{10... | collective-permute-start | bytes 147464 | tf_op jit(solution)/shard_map/ppermute | solution.py:31
  33.9 4.3 %collective-permute-done.3 = bf16[1,2,16,768]{3,2,1,0:T(8,128)(2,1)S(1)} collective-permute-done((bf16[1,2,16,768]{3,2,1,0:T(8,128)(2,1)S(1)}, bf16[1,2,16,768]{3,2,1,0:T(8,128)(2,1)S(1)}, u32[]{:S(2)}, u32[]{:S(2)}) %collective-permute-start.3) | collective-permute-done | bytes 49184 | tf_op jit(solution)/shard_map/ppermute | solution.py:31
  38.2 1.1 all-to-all-done
  39.9 10.2 %all_to_all.40 = f32[8,32,128]{2,1,0:T(8,128)S(1)} all-to-all(f32[8,32,128]{2,1,0:T(8,128)S(1)} %fusion.42), channel_id=1, replica_groups=mesh['vp_0'=16,'vp_1'=4,'vp_2'=2,'dp'=4] {'vp_1','vp_2'}, dimensions={0} | all-to-all | bytes 262144 | tf_op jit(solution)/shard_map/all_to_all | solution.py:23
  50.8 9.2 %all-to-all-start.2 = ((bf16[16,32,128]{2,1,0:T(8,128)(2,1)}), bf16[16,32,128]{2,1,0:T(8,128)(2,1)S(1)}, u32[]{:S(2)}, u32[]{:S(2)}) async-start(bf16[16,32,128]{2,1,0:T(8,128)(2,1)} %broadcast_in_dim.26), calls=%async_computation.2 | async-start | bytes 262144 | tf_op jit(solution)/shard_map/all_to_all | solution.py:23
  60.1 1.9 %collective-permute-start.4 = (bf16[2048,256]{1,0:T(8,128)(2,1)S(1)}, bf16[2048,256]{1,0:T(8,128)(2,1)S(1)}, u32[]{:S(2)}, u32[]{:S(2)}) collective-permute-start(bf16[2048,256]{1,0:T(8,128)(2,1)S(1)} %copy-done), channel_id=1, source_target_pairs={{0,4},{4,0},{1,5},{5,1},{2,6},{6,2},{3,7},{7,3},{8,12},{12,8},{9,1... | collective-permute-start | bytes 3145736 | tf_op jit(solution)/shard_map/ppermute | solution.py:31
  62.0 2.4 %collective-permute-start.5 = (f32[2,128]{1,0:T(2,128)S(1)}, f32[2,128]{1,0:T(2,128)S(1)}, u32[]{:S(2)}, u32[]{:S(2)}) collective-permute-start(f32[2,128]{1,0:T(2,128)S(1)} %bitcast.84), channel_id=1, source_target_pairs={{0,4},{4,0},{1,5},{5,1},{2,6},{6,2},{3,7},{7,3},{8,12},{12,8},{9,1... | collective-permute-start | bytes 3080 | tf_op jit(solution)/shard_map/ppermute | solution.py:31
  64.5 9.5 %all-to-all-done.2 = bf16[16,32,128]{2,1,0:T(8,128)(2,1)S(1)} async-done(((bf16[16,32,128]{2,1,0:T(8,128)(2,1)}), bf16[16,32,128]{2,1,0:T(8,128)(2,1)S(1)}, u32[]{:S(2)}, u32[]{:S(2)}) %all-to-all-start.2) | async-done | bytes 131104 | tf_op jit(solution)/shard_map/all_to_all | solution.py:23
  75.1 3.5 %all-to-all-start.3 = ((bf16[4,32,2048]{2,1,0:T(8,128)(2,1)}), bf16[4,32,2048]{2,1,0:T(8,128)(2,1)S(1)}, u32[]{:S(2)}, u32[]{:S(2)}) async-start(bf16[4,32,2048]{2,1,0:T(8,128)(2,1)} %broadcast_in_dim.27), calls=%async_computation.3 | async-start | bytes 1048576 | tf_op jit(solution)/shard_map/all_to_all | solution.py:23
  79.8 6.8 %all-to-all-done.3 = bf16[4,32,2048]{2,1,0:T(8,128)(2,1)S(1)} async-done(((bf16[4,32,2048]{2,1,0:T(8,128)(2,1)}), bf16[4,32,2048]{2,1,0:T(8,128)(2,1)S(1)}, u32[]{:S(2)}, u32[]{:S(2)}) %all-to-all-start.3) | async-done | bytes 524320 | tf_op jit(solution)/shard_map/all_to_all | solution.py:23
  86.6 1.8 %shard_map.103 = (f32[4,2,128]{2,1,0:T(2,128)}, f32[2,128,256]{2,1,0:T(8,128)S(1)}) custom-call(s32[2]{0:T(128)S(1)} %pad_add_fusion.1.base_ref, bf16[128,2048]{1,0:T(8,128)(2,1)S(1)} %bitcast.68, bf16[2048,256]{1,0:T(8,128)(2,1)S(1)} %copy-done, bf16[2048,256]{1,0:T(8,128)(2,1)S(1)} %collective-permute-done.4.other_ref, ...), custom_call_target="tpu_custom_call" | custom-call | flops 268435456 | bytes 2097152 | tf_op jit(solution)/shard_map/pallas_call | solution.py:164
  88.4 3.2 %all-to-all-start.4 = ((f32[4,2,128]{2,1,0:T(2,128)}), f32[4,2,128]{2,1,0:T(2,128)S(1)}, u32[]{:S(2)}, u32[]{:S(2)}) async-start(f32[4,2,128]{2,1,0:T(2,128)} %get-tuple-element.15), calls=%async_computation.4 | async-start | bytes 8192 | tf_op jit(solution)/shard_map/all_to_all | solution.py:23
  91.7 5.2 %all-to-all-done.4 = f32[4,2,128]{2,1,0:T(2,128)S(1)} async-done(((f32[4,2,128]{2,1,0:T(2,128)}), f32[4,2,128]{2,1,0:T(2,128)S(1)}, u32[]{:S(2)}, u32[]{:S(2)}) %all-to-all-start.4) | async-done | bytes 4128 | tf_op jit(solution)/shard_map/all_to_all | solution.py:23
  97.6 5.1 %all-to-all-start.5 = ((f32[16,2,128]{2,1,0:T(2,128)}), f32[16,2,128]{2,1,0:T(2,128)S(1)}, u32[]{:S(2)}, u32[]{:S(2)}) async-start(f32[16,2,128]{2,1,0:T(2,128)} %broadcast_in_dim.51), calls=%async_computation.5 | async-start | bytes 32768 | tf_op jit(solution)/shard_map/all_to_all | solution.py:23
  103.4 10.6 %all-to-all-done.5.stats_ref = f32[16,2,128]{2,1,0:T(2,128)S(1)} async-done(((f32[16,2,128]{2,1,0:T(2,128)}), f32[16,2,128]{2,1,0:T(2,128)S(1)}, u32[]{:S(2)}, u32[]{:S(2)}) %all-to-all-start.5) | async-done | bytes 16416 | tf_op jit(solution)/shard_map/all_to_all | solution.py:23
  114.0 2.3 %shard_map.104 = (bf16[4,32,2048]{2,1,0:T(8,128)(2,1)}, bf16[128,512]{1,0:T(8,128)(2,1)S(1)}, f32[1,128]{1,0:T(1,128)S(1)}) custom-call(s32[2]{0:T(128)S(1)} %pad_add_fusion.1.base_ref, f32[16,2,128]{2,1,0:T(2,128)S(1)} %all-to-all-done.5.stats_ref, f32[2,128,256]{2,1,0:T(8,128)S(1)} %get-tuple-element.16.scores_ref, bf16[2048,256]{1,0:T(8,128)(2,1)S(1)} %copy-done, ...), custom_call_target="tpu_custom_call" | custom-call | flops 268435456 | bytes 2097152 | tf_op jit(solution)/shard_map/pallas_call | solution.py:177
  117.0 5.1 %collective-permute-start.7 = (bf16[128,1024]{1,0:T(8,128)(2,1)S(1)}, bf16[128,1024]{1,0:T(8,128)(2,1)S(1)}, u32[]{:S(2)}, u32[]{:S(2)}) collective-permute-start(bf16[128,1024]{1,0:T(8,128)(2,1)S(1)} %get-tuple-element.34), channel_id=1, source_target_pairs={{0,2},{1,3},{2,0},{3,1},{4,6},{5,7},{6,4},{7,5},{8,10},{9,11},{10,... | collective-permute-start | bytes 786440 | tf_op jit(solution)/shard_map/ppermute | solution.py:31
  122.1 3.0 %collective-permute-start.6 = (bf16[128,512]{1,0:T(8,128)(2,1)}, bf16[128,512]{1,0:T(8,128)(2,1)}, u32[]{:S(2)}, u32[]{:S(2)}) collective-permute-start(bf16[128,512]{1,0:T(8,128)(2,1)} %get-tuple-element.27), channel_id=1, source_target_pairs={{0,3},{1,2},{2,1},{3,0},{4,7},{5,6},{6,5},{7,4},{8,11},{9,10},{10,... | collective-permute-start | bytes 393224 | tf_op jit(solution)/shard_map/ppermute | solution.py:31
  125.1 4.1 %collective-permute-start.9 = (bf16[128,512]{1,0:T(8,128)(2,1)S(1)}, bf16[128,512]{1,0:T(8,128)(2,1)}, u32[]{:S(2)}, u32[]{:S(2)}) collective-permute-start(bf16[128,512]{1,0:T(8,128)(2,1)S(1)} %get-tuple-element.21), channel_id=1, source_target_pairs={{0,3},{1,2},{2,1},{3,0},{4,7},{5,6},{6,5},{7,4},{8,11},{9,10},{10,... | collective-permute-start | bytes 393224 | tf_op jit(solution)/shard_map/ppermute | solution.py:31
  129.2 3.5 %all-to-all-start.6 = ((bf16[4,32,2048]{2,1,0:T(8,128)(2,1)}), bf16[4,32,2048]{2,1,0:T(8,128)(2,1)S(1)}, u32[]{:S(2)}, u32[]{:S(2)}) async-start(bf16[4,32,2048]{2,1,0:T(8,128)(2,1)} %get-tuple-element.18), calls=%async_computation.6 | async-start | bytes 1048576 | tf_op jit(solution)/shard_map/all_to_all | solution.py:23
  132.7 1.9 %collective-permute-start.8 = (bf16[128,1024]{1,0:T(8,128)(2,1)}, bf16[128,1024]{1,0:T(8,128)(2,1)S(1)}, u32[]{:S(2)}, u32[]{:S(2)}) collective-permute-start(bf16[128,1024]{1,0:T(8,128)(2,1)} %get-tuple-element.33), channel_id=1, source_target_pairs={{0,1},{1,0},{2,3},{3,2},{4,5},{5,4},{6,7},{7,6},{8,9},{9,8},{10,11... | collective-permute-start | bytes 786440 | tf_op jit(solution)/shard_map/ppermute | solution.py:31
  136.3 4.5 %all-to-all-done.6 = bf16[4,32,2048]{2,1,0:T(8,128)(2,1)S(1)} async-done(((bf16[4,32,2048]{2,1,0:T(8,128)(2,1)}), bf16[4,32,2048]{2,1,0:T(8,128)(2,1)S(1)}, u32[]{:S(2)}, u32[]{:S(2)}) %all-to-all-start.6) | async-done | bytes 524320 | tf_op jit(solution)/shard_map/all_to_all | solution.py:23
  141.6 4.7 %all-to-all-start.7 = ((bf16[16,2,2048]{2,1,0:T(2,128)(2,1)}), bf16[16,2,2048]{2,1,0:T(2,128)(2,1)S(1)}, u32[]{:S(2)}, u32[]{:S(2)}) async-start(bf16[16,2,2048]{2,1,0:T(2,128)(2,1)} %reshape.119), calls=%async_computation.7 | async-start | bytes 262144 | tf_op jit(solution)/shard_map/all_to_all | solution.py:23
  147.2 1.1 fusion.19
  148.6 1.9 %collective-permute-start.10 = (f32[512,256]{1,0:T(8,128)S(1)}, f32[512,256]{1,0:T(8,128)S(1)}, u32[]{:S(2)}, u32[]{:S(2)}) collective-permute-start(f32[512,256]{1,0:T(8,128)S(1)} %fusion.1), channel_id=1, source_target_pairs={{0,4},{4,0},{1,5},{5,1},{2,6},{6,2},{3,7},{7,3},{8,12},{12,8},{9,1... | collective-permute-start | bytes 1572872 | tf_op jit(solution)/shard_map/ppermute | solution.py:31
  151.9 6.7 %all-to-all-done.7.row_ref = bf16[16,2,2048]{2,1,0:T(2,128)(2,1)S(1)} async-done(((bf16[16,2,2048]{2,1,0:T(2,128)(2,1)}), bf16[16,2,2048]{2,1,0:T(2,128)(2,1)S(1)}, u32[]{:S(2)}, u32[]{:S(2)}) %all-to-all-start.7) | async-done | bytes 131104 | tf_op jit(solution)/shard_map/all_to_all | solution.py:23
  (76 shorter events, 15.1 us)
Async XLA Ops:
  0.6 0.8 copy-start.4
  2.2 15.3 %copy-start.2 = (bf16[5632,16]{0,1:T(8,128)(2,1)S(1)}, bf16[5632,16]{0,1:T(8,128)(2,1)}, u32[]{:S(2)}) copy-start(bf16[5632,16]{0,1:T(8,128)(2,1)} %param.10) | copy-start | bytes 540676
  2.2 37.2 %all-to-all-start = ((bf16[16,48,256]{2,1,0:T(8,128)(2,1)}), bf16[16,48,256]{2,1,0:T(8,128)(2,1)S(1)}, u32[]{:S(2)}, u32[]{:S(2)}) async-start(bf16[16,48,256]{2,1,0:T(8,128)(2,1)} %pad_add_fusion), calls=%async_computation | async-start | bytes 786432 | tf_op jit(solution)/shard_map/all_to_all | solution.py:23
  19.7 3.2 %collective-permute-start = (bf16[1,4,16,768]{3,2,1,0:T(8,128)(2,1)S(1)}, bf16[1,4,16,768]{3,2,1,0:T(8,128)(2,1)S(1)}, u32[]{:S(2)}, u32[]{:S(2)}) collective-permute-start(bf16[1,4,16,768]{3,2,1,0:T(8,128)(2,1)S(1)} %dynamic-slice_bitcast_fusion), channel_id=1, source_target_pairs={{0,4},{4,0},{1,5},{5,1},{2,6},{6,2},{3,7},{7,3},{8,12},{12,8},{9,1... | collective-permute-start | bytes 294920 | tf_op jit(solution)/shard_map/ppermute | solution.py:31
  23.0 10.5 %collective-permute-start.1 = (bf16[1,2,16,768]{3,2,1,0:T(8,128)(2,1)S(1)}, bf16[1,2,16,768]{3,2,1,0:T(8,128)(2,1)S(1)}, u32[]{:S(2)}, u32[]{:S(2)}) collective-permute-start(bf16[1,2,16,768]{3,2,1,0:T(8,128)(2,1)S(1)} %get-tuple-element.31), channel_id=1, source_target_pairs={{0,8},{8,0},{16,24},{24,16},{1,9},{9,1},{17,25},{25,17},{2,10},{10... | collective-permute-start | bytes 147464 | tf_op jit(solution)/shard_map/ppermute | solution.py:31
  26.4 7.5 %collective-permute-start.2 = (bf16[1,2,16,768]{3,2,1,0:T(8,128)(2,1)S(1)}, bf16[1,2,16,768]{3,2,1,0:T(8,128)(2,1)S(1)}, u32[]{:S(2)}, u32[]{:S(2)}) collective-permute-start(bf16[1,2,16,768]{3,2,1,0:T(8,128)(2,1)S(1)} %get-tuple-element.32), channel_id=1, source_target_pairs={{0,16},{8,24},{16,0},{24,8},{1,17},{9,25},{17,1},{25,9},{2,18},{10... | collective-permute-start | bytes 147464 | tf_op jit(solution)/shard_map/ppermute | solution.py:31
  31.0 7.2 %collective-permute-start.3 = (bf16[1,2,16,768]{3,2,1,0:T(8,128)(2,1)S(1)}, bf16[1,2,16,768]{3,2,1,0:T(8,128)(2,1)S(1)}, u32[]{:S(2)}, u32[]{:S(2)}) collective-permute-start(bf16[1,2,16,768]{3,2,1,0:T(8,128)(2,1)S(1)} %get-tuple-element.30), channel_id=1, source_target_pairs={{0,24},{8,16},{16,8},{24,0},{1,25},{9,17},{17,9},{25,1},{2,26},{10... | collective-permute-start | bytes 147464 | tf_op jit(solution)/shard_map/ppermute | solution.py:31
  33.4 5.9 %copy-start.3 = (bf16[256,256]{1,0:T(8,128)(2,1)S(1)}, bf16[256,256]{1,0:T(8,128)(2,1)}, u32[]{:S(2)}) copy-start(bf16[256,256]{1,0:T(8,128)(2,1)} %constant.107.clone) | copy-start | bytes 393220
  39.3 20.7 %copy-start = (bf16[2048,256]{1,0:T(8,128)(2,1)S(1)}, bf16[2048,256]{1,0:T(8,128)(2,1)}, u32[]{:S(2)}) copy-start(bf16[2048,256]{1,0:T(8,128)(2,1)} %own_ref.3) | copy-start | bytes 3145732
  50.8 23.1 %all-to-all-start.2 = ((bf16[16,32,128]{2,1,0:T(8,128)(2,1)}), bf16[16,32,128]{2,1,0:T(8,128)(2,1)S(1)}, u32[]{:S(2)}, u32[]{:S(2)}) async-start(bf16[16,32,128]{2,1,0:T(8,128)(2,1)} %broadcast_in_dim.26), calls=%async_computation.2 | async-start | bytes 262144 | tf_op jit(solution)/shard_map/all_to_all | solution.py:23
  60.1 1.9 %copy-start.6 = (f32[256]{0:T(256)S(1)}, f32[256]{0:T(256)}, u32[]{:S(2)}) copy-start(f32[256]{0:T(256)} %param.13) | copy-start | bytes 3076
  60.1 19.7 %collective-permute-start.4 = (bf16[2048,256]{1,0:T(8,128)(2,1)S(1)}, bf16[2048,256]{1,0:T(8,128)(2,1)S(1)}, u32[]{:S(2)}, u32[]{:S(2)}) collective-permute-start(bf16[2048,256]{1,0:T(8,128)(2,1)S(1)} %copy-done), channel_id=1, source_target_pairs={{0,4},{4,0},{1,5},{5,1},{2,6},{6,2},{3,7},{7,3},{8,12},{12,8},{9,1... | collective-permute-start | bytes 3145736 | tf_op jit(solution)/shard_map/ppermute | solution.py:31
  62.0 17.7 %collective-permute-start.5 = (f32[2,128]{1,0:T(2,128)S(1)}, f32[2,128]{1,0:T(2,128)S(1)}, u32[]{:S(2)}, u32[]{:S(2)}) collective-permute-start(f32[2,128]{1,0:T(2,128)S(1)} %bitcast.84), channel_id=1, source_target_pairs={{0,4},{4,0},{1,5},{5,1},{2,6},{6,2},{3,7},{7,3},{8,12},{12,8},{9,1... | collective-permute-start | bytes 3080 | tf_op jit(solution)/shard_map/ppermute | solution.py:31
  64.5 9.6 %copy-start.1 = (f32[2048]{0:T(1024)S(1)}, f32[2048]{0:T(1024)}, u32[]{:S(2)}) copy-start(f32[2048]{0:T(1024)} %param.11) | copy-start | bytes 24580
  75.1 11.5 %all-to-all-start.3 = ((bf16[4,32,2048]{2,1,0:T(8,128)(2,1)}), bf16[4,32,2048]{2,1,0:T(8,128)(2,1)S(1)}, u32[]{:S(2)}, u32[]{:S(2)}) async-start(bf16[4,32,2048]{2,1,0:T(8,128)(2,1)} %broadcast_in_dim.27), calls=%async_computation.3 | async-start | bytes 1048576 | tf_op jit(solution)/shard_map/all_to_all | solution.py:23
  78.6 0.7 copy-start.5
  88.4 8.5 %all-to-all-start.4 = ((f32[4,2,128]{2,1,0:T(2,128)}), f32[4,2,128]{2,1,0:T(2,128)S(1)}, u32[]{:S(2)}, u32[]{:S(2)}) async-start(f32[4,2,128]{2,1,0:T(2,128)} %get-tuple-element.15), calls=%async_computation.4 | async-start | bytes 8192 | tf_op jit(solution)/shard_map/all_to_all | solution.py:23
  97.6 16.4 %all-to-all-start.5 = ((f32[16,2,128]{2,1,0:T(2,128)}), f32[16,2,128]{2,1,0:T(2,128)S(1)}, u32[]{:S(2)}, u32[]{:S(2)}) async-start(f32[16,2,128]{2,1,0:T(2,128)} %broadcast_in_dim.51), calls=%async_computation.5 | async-start | bytes 32768 | tf_op jit(solution)/shard_map/all_to_all | solution.py:23
  117.0 18.2 %collective-permute-start.7 = (bf16[128,1024]{1,0:T(8,128)(2,1)S(1)}, bf16[128,1024]{1,0:T(8,128)(2,1)S(1)}, u32[]{:S(2)}, u32[]{:S(2)}) collective-permute-start(bf16[128,1024]{1,0:T(8,128)(2,1)S(1)} %get-tuple-element.34), channel_id=1, source_target_pairs={{0,2},{1,3},{2,0},{3,1},{4,6},{5,7},{6,4},{7,5},{8,10},{9,11},{10,... | collective-permute-start | bytes 786440 | tf_op jit(solution)/shard_map/ppermute | solution.py:31
  122.1 18.7 %collective-permute-start.6 = (bf16[128,512]{1,0:T(8,128)(2,1)}, bf16[128,512]{1,0:T(8,128)(2,1)}, u32[]{:S(2)}, u32[]{:S(2)}) collective-permute-start(bf16[128,512]{1,0:T(8,128)(2,1)} %get-tuple-element.27), channel_id=1, source_target_pairs={{0,3},{1,2},{2,1},{3,0},{4,7},{5,6},{6,5},{7,4},{8,11},{9,10},{10,... | collective-permute-start | bytes 393224 | tf_op jit(solution)/shard_map/ppermute | solution.py:31
  125.1 22.1 %collective-permute-start.9 = (bf16[128,512]{1,0:T(8,128)(2,1)S(1)}, bf16[128,512]{1,0:T(8,128)(2,1)}, u32[]{:S(2)}, u32[]{:S(2)}) collective-permute-start(bf16[128,512]{1,0:T(8,128)(2,1)S(1)} %get-tuple-element.21), channel_id=1, source_target_pairs={{0,3},{1,2},{2,1},{3,0},{4,7},{5,6},{6,5},{7,4},{8,11},{9,10},{10,... | collective-permute-start | bytes 393224 | tf_op jit(solution)/shard_map/ppermute | solution.py:31
  129.2 11.5 %all-to-all-start.6 = ((bf16[4,32,2048]{2,1,0:T(8,128)(2,1)}), bf16[4,32,2048]{2,1,0:T(8,128)(2,1)S(1)}, u32[]{:S(2)}, u32[]{:S(2)}) async-start(bf16[4,32,2048]{2,1,0:T(8,128)(2,1)} %get-tuple-element.18), calls=%async_computation.6 | async-start | bytes 1048576 | tf_op jit(solution)/shard_map/all_to_all | solution.py:23
  132.7 15.6 %collective-permute-start.8 = (bf16[128,1024]{1,0:T(8,128)(2,1)}, bf16[128,1024]{1,0:T(8,128)(2,1)S(1)}, u32[]{:S(2)}, u32[]{:S(2)}) collective-permute-start(bf16[128,1024]{1,0:T(8,128)(2,1)} %get-tuple-element.33), channel_id=1, source_target_pairs={{0,1},{1,0},{2,3},{3,2},{4,5},{5,4},{6,7},{7,6},{8,9},{9,8},{10,11... | collective-permute-start | bytes 786440 | tf_op jit(solution)/shard_map/ppermute | solution.py:31
  141.6 17.0 %all-to-all-start.7 = ((bf16[16,2,2048]{2,1,0:T(2,128)(2,1)}), bf16[16,2,2048]{2,1,0:T(2,128)(2,1)S(1)}, u32[]{:S(2)}, u32[]{:S(2)}) async-start(bf16[16,2,2048]{2,1,0:T(2,128)(2,1)} %reshape.119), calls=%async_computation.7 | async-start | bytes 262144 | tf_op jit(solution)/shard_map/all_to_all | solution.py:23
  148.6 10.9 %collective-permute-start.10 = (f32[512,256]{1,0:T(8,128)S(1)}, f32[512,256]{1,0:T(8,128)S(1)}, u32[]{:S(2)}, u32[]{:S(2)}) collective-permute-start(f32[512,256]{1,0:T(8,128)S(1)} %fusion.1), channel_id=1, source_target_pairs={{0,4},{4,0},{1,5},{5,1},{2,6},{6,2},{3,7},{7,3},{8,12},{12,8},{9,1... | collective-permute-start | bytes 1572872 | tf_op jit(solution)/shard_map/ppermute | solution.py:31

commit v5 on v3

--- a/solution.py
+++ b/solution.py
@@ -192,9 +192,10 @@
     row_x = exchange(row_term, X)
     row_x = jnp.sum(row_x.astype(f32), axis=0).astype(bf16)
     early, row_x = lax.optimization_barrier((early, row_x))
-    early = lax.optimization_barrier(jnp.where(c >= 0, early, 0))
+    early = jnp.where(c >= 0, early, 0)
+    early = lax.optimization_barrier(early)
     theirs, ours = 0.0, 0.0
-    for step in (0, ny // 2, 1, last):
+    for step in (0, 1, ny // 2, last):
         if step == last:
             piece, cols_of = early, partner(dscore, "dp", step)
         else:

time: 161 us -> 160 us (level)
  the two profiles are of different devices: /device:TPU:32 before, /device:TPU:24 now
where the time goes in v5:
time: 160 us; the launch traced here: 159 us
  starting transfers between devices  71.2 us (44%)
  waiting for transfers between devices  54.9 us (34%)
  blocking collectives  10.2 us (6%)
  local copies, waits for them, and re-layouts  7.92 us (5%)
  Pallas kernels  4.91 us (3%)
  matrix products  4.26 us (3%)
  other arithmetic  4.22 us (3%)
    all_to_all x7, waiting for transfers between devices, exchange(): return lax.all_to_all(blocks, axes, split_axis=0, concat_axis=0, tiled=True)  49 us
    all_to_all x7, starting transfers between devices, exchange(): return lax.all_to_all(blocks, axes, split_axis=0, concat_axis=0, tiled=True)  40.8 us
    ppermute x11, starting transfers between devices, partner(): lax.ppermute(array, axes, [(k, k ^ step) for k in range(lax.axis_size(axe...  30.3 us
    all_to_all x1, blocking collectives, exchange(): return lax.all_to_all(blocks, axes, split_axis=0, concat_axis=0, tiled=True)  10.2 us
    ppermute x11, waiting for transfers between devices, partner(): lax.ppermute(array, axes, [(k, k ^ step) for k in range(lax.axis_size(axe...  5.97 us
    dot_general x10, matrix products, dot(): lax.dot_general(a, b, (((da,), (db,)), ((), ())), preferred_element_type=...  4.26 us
  transfers between devices with their start and end apart: 18, of which 10 were waited for; matrix products, arithmetic and copies ran while one was open for 7% of the time, Pallas kernels for 1%

profile of v5, /device:TPU:24, one launch (start us, length us, event | category | flops | bytes accessed | tf_op | source)
XLA Modules:
  0.0 158.8 jit_solution(15543268440769663097)
XLA Ops:
  2.2 15.3 %all-to-all-start = ((bf16[16,48,256]{2,1,0:T(8,128)(2,1)}), bf16[16,48,256]{2,1,0:T(8,128)(2,1)S(1)}, u32[]{:S(2)}, u32[]{:S(2)}) async-start(bf16[16,48,256]{2,1,0:T(8,128)(2,1)} %pad_add_fusion), calls=%async_computation | async-start | bytes 786432 | tf_op jit(solution)/shard_map/all_to_all | solution.py:23
  17.5 1.5 reshape.114
  19.7 1.9 %collective-permute-start = (bf16[1,4,16,768]{3,2,1,0:T(8,128)(2,1)S(1)}, bf16[1,4,16,768]{3,2,1,0:T(8,128)(2,1)S(1)}, u32[]{:S(2)}, u32[]{:S(2)}) collective-permute-start(bf16[1,4,16,768]{3,2,1,0:T(8,128)(2,1)S(1)} %dynamic-slice_bitcast_fusion), channel_id=1, source_target_pairs={{0,4},{4,0},{1,5},{5,1},{2,6},{6,2},{3,7},{7,3},{8,12},{12,8},{9,1... | collective-permute-start | bytes 294920 | tf_op jit(solution)/shard_map/ppermute | solution.py:31
  21.7 1.2 collective-permute-done
  23.0 3.4 %collective-permute-start.1 = (bf16[1,2,16,768]{3,2,1,0:T(8,128)(2,1)S(1)}, bf16[1,2,16,768]{3,2,1,0:T(8,128)(2,1)S(1)}, u32[]{:S(2)}, u32[]{:S(2)}) collective-permute-start(bf16[1,2,16,768]{3,2,1,0:T(8,128)(2,1)S(1)} %get-tuple-element.31), channel_id=1, source_target_pairs={{0,8},{8,0},{16,24},{24,16},{1,9},{9,1},{17,25},{25,17},{2,10},{10... | collective-permute-start | bytes 147464 | tf_op jit(solution)/shard_map/ppermute | solution.py:31
  26.4 4.6 %collective-permute-start.2 = (bf16[1,2,16,768]{3,2,1,0:T(8,128)(2,1)S(1)}, bf16[1,2,16,768]{3,2,1,0:T(8,128)(2,1)S(1)}, u32[]{:S(2)}, u32[]{:S(2)}) collective-permute-start(bf16[1,2,16,768]{3,2,1,0:T(8,128)(2,1)S(1)} %get-tuple-element.32), channel_id=1, source_target_pairs={{0,16},{8,24},{16,0},{24,8},{1,17},{9,25},{17,1},{25,9},{2,18},{10... | collective-permute-start | bytes 147464 | tf_op jit(solution)/shard_map/ppermute | solution.py:31
  31.0 2.4 %collective-permute-start.3 = (bf16[1,2,16,768]{3,2,1,0:T(8,128)(2,1)S(1)}, bf16[1,2,16,768]{3,2,1,0:T(8,128)(2,1)S(1)}, u32[]{:S(2)}, u32[]{:S(2)}) collective-permute-start(bf16[1,2,16,768]{3,2,1,0:T(8,128)(2,1)S(1)} %get-tuple-element.30), channel_id=1, source_target_pairs={{0,24},{8,16},{16,8},{24,0},{1,25},{9,17},{17,9},{25,1},{2,26},{10... | collective-permute-start | bytes 147464 | tf_op jit(solution)/shard_map/ppermute | solution.py:31
  33.9 4.3 %collective-permute-done.3 = bf16[1,2,16,768]{3,2,1,0:T(8,128)(2,1)S(1)} collective-permute-done((bf16[1,2,16,768]{3,2,1,0:T(8,128)(2,1)S(1)}, bf16[1,2,16,768]{3,2,1,0:T(8,128)(2,1)S(1)}, u32[]{:S(2)}, u32[]{:S(2)}) %collective-permute-start.3) | collective-permute-done | bytes 49184 | tf_op jit(solution)/shard_map/ppermute | solution.py:31
  38.2 3.1 %all-to-all-done = bf16[16,48,256]{2,1,0:T(8,128)(2,1)S(1)} async-done(((bf16[16,48,256]{2,1,0:T(8,128)(2,1)}), bf16[16,48,256]{2,1,0:T(8,128)(2,1)S(1)}, u32[]{:S(2)}, u32[]{:S(2)}) %all-to-all-start) | async-done | bytes 393248 | tf_op jit(solution)/shard_map/all_to_all | solution.py:23
  41.9 10.2 %all_to_all.40 = f32[8,32,128]{2,1,0:T(8,128)S(1)} all-to-all(f32[8,32,128]{2,1,0:T(8,128)S(1)} %fusion.42), channel_id=1, replica_groups=mesh['vp_0'=16,'vp_1'=4,'vp_2'=2,'dp'=4] {'vp_1','vp_2'}, dimensions={0} | all-to-all | bytes 262144 | tf_op jit(solution)/shard_map/all_to_all | solution.py:23
  52.8 7.2 %all-to-all-start.2 = ((bf16[16,32,128]{2,1,0:T(8,128)(2,1)}), bf16[16,32,128]{2,1,0:T(8,128)(2,1)S(1)}, u32[]{:S(2)}, u32[]{:S(2)}) async-start(bf16[16,32,128]{2,1,0:T(8,128)(2,1)} %broadcast_in_dim.26), calls=%async_computation.2 | async-start | bytes 262144 | tf_op jit(solution)/shard_map/all_to_all | solution.py:23
  60.1 1.9 %collective-permute-start.4 = (bf16[2048,256]{1,0:T(8,128)(2,1)S(1)}, bf16[2048,256]{1,0:T(8,128)(2,1)S(1)}, u32[]{:S(2)}, u32[]{:S(2)}) collective-permute-start(bf16[2048,256]{1,0:T(8,128)(2,1)S(1)} %copy-done), channel_id=1, source_target_pairs={{0,4},{4,0},{1,5},{5,1},{2,6},{6,2},{3,7},{7,3},{8,12},{12,8},{9,1... | collective-permute-start | bytes 3145736 | tf_op jit(solution)/shard_map/ppermute | solution.py:31
  62.0 2.4 %collective-permute-start.5 = (f32[2,128]{1,0:T(2,128)S(1)}, f32[2,128]{1,0:T(2,128)S(1)}, u32[]{:S(2)}, u32[]{:S(2)}) collective-permute-start(f32[2,128]{1,0:T(2,128)S(1)} %bitcast.84), channel_id=1, source_target_pairs={{0,4},{4,0},{1,5},{5,1},{2,6},{6,2},{3,7},{7,3},{8,12},{12,8},{9,1... | collective-permute-start | bytes 3080 | tf_op jit(solution)/shard_map/ppermute | solution.py:31
  64.5 10.0 %all-to-all-done.2 = bf16[16,32,128]{2,1,0:T(8,128)(2,1)S(1)} async-done(((bf16[16,32,128]{2,1,0:T(8,128)(2,1)}), bf16[16,32,128]{2,1,0:T(8,128)(2,1)S(1)}, u32[]{:S(2)}, u32[]{:S(2)}) %all-to-all-start.2) | async-done | bytes 131104 | tf_op jit(solution)/shard_map/all_to_all | solution.py:23
  75.6 3.5 %all-to-all-start.3 = ((bf16[4,32,2048]{2,1,0:T(8,128)(2,1)}), bf16[4,32,2048]{2,1,0:T(8,128)(2,1)S(1)}, u32[]{:S(2)}, u32[]{:S(2)}) async-start(bf16[4,32,2048]{2,1,0:T(8,128)(2,1)} %broadcast_in_dim.27), calls=%async_computation.3 | async-start | bytes 1048576 | tf_op jit(solution)/shard_map/all_to_all | solution.py:23
  80.3 6.8 %all-to-all-done.3 = bf16[4,32,2048]{2,1,0:T(8,128)(2,1)S(1)} async-done(((bf16[4,32,2048]{2,1,0:T(8,128)(2,1)}), bf16[4,32,2048]{2,1,0:T(8,128)(2,1)S(1)}, u32[]{:S(2)}, u32[]{:S(2)}) %all-to-all-start.3) | async-done | bytes 524320 | tf_op jit(solution)/shard_map/all_to_all | solution.py:23
  87.2 1.8 %shard_map.103 = (f32[4,2,128]{2,1,0:T(2,128)}, f32[2,128,256]{2,1,0:T(8,128)S(1)}) custom-call(s32[2]{0:T(128)S(1)} %pad_add_fusion.1.base_ref, bf16[128,2048]{1,0:T(8,128)(2,1)S(1)} %bitcast.68, bf16[2048,256]{1,0:T(8,128)(2,1)S(1)} %copy-done, bf16[2048,256]{1,0:T(8,128)(2,1)S(1)} %collective-permute-done.4.other_ref, ...), custom_call_target="tpu_custom_call" | custom-call | flops 268435456 | bytes 2097152 | tf_op jit(solution)/shard_map/pallas_call | solution.py:164
  89.0 3.2 %all-to-all-start.4 = ((f32[4,2,128]{2,1,0:T(2,128)}), f32[4,2,128]{2,1,0:T(2,128)S(1)}, u32[]{:S(2)}, u32[]{:S(2)}) async-start(f32[4,2,128]{2,1,0:T(2,128)} %get-tuple-element.15), calls=%async_computation.4 | async-start | bytes 8192 | tf_op jit(solution)/shard_map/all_to_all | solution.py:23
  92.2 5.2 %all-to-all-done.4 = f32[4,2,128]{2,1,0:T(2,128)S(1)} async-done(((f32[4,2,128]{2,1,0:T(2,128)}), f32[4,2,128]{2,1,0:T(2,128)S(1)}, u32[]{:S(2)}, u32[]{:S(2)}) %all-to-all-start.4) | async-done | bytes 4128 | tf_op jit(solution)/shard_map/all_to_all | solution.py:23
  98.2 4.6 %all-to-all-start.5 = ((f32[16,2,128]{2,1,0:T(2,128)}), f32[16,2,128]{2,1,0:T(2,128)S(1)}, u32[]{:S(2)}, u32[]{:S(2)}) async-start(f32[16,2,128]{2,1,0:T(2,128)} %broadcast_in_dim.51), calls=%async_computation.5 | async-start | bytes 32768 | tf_op jit(solution)/shard_map/all_to_all | solution.py:23
  103.4 11.9 %all-to-all-done.5.stats_ref = f32[16,2,128]{2,1,0:T(2,128)S(1)} async-done(((f32[16,2,128]{2,1,0:T(2,128)}), f32[16,2,128]{2,1,0:T(2,128)S(1)}, u32[]{:S(2)}, u32[]{:S(2)}) %all-to-all-start.5) | async-done | bytes 16416 | tf_op jit(solution)/shard_map/all_to_all | solution.py:23
  115.3 2.3 %shard_map.104 = (bf16[4,32,2048]{2,1,0:T(8,128)(2,1)}, bf16[128,512]{1,0:T(8,128)(2,1)S(1)}, f32[1,128]{1,0:T(1,128)S(1)}) custom-call(s32[2]{0:T(128)S(1)} %pad_add_fusion.1.base_ref, f32[16,2,128]{2,1,0:T(2,128)S(1)} %all-to-all-done.5.stats_ref, f32[2,128,256]{2,1,0:T(8,128)S(1)} %get-tuple-element.16.scores_ref, bf16[2048,256]{1,0:T(8,128)(2,1)S(1)} %copy-done, ...), custom_call_target="tpu_custom_call" | custom-call | flops 268435456 | bytes 2097152 | tf_op jit(solution)/shard_map/pallas_call | solution.py:177
  118.3 2.6 %collective-permute-start.7 = (bf16[128,1024]{1,0:T(8,128)(2,1)S(1)}, bf16[128,1024]{1,0:T(8,128)(2,1)S(1)}, u32[]{:S(2)}, u32[]{:S(2)}) collective-permute-start(bf16[128,1024]{1,0:T(8,128)(2,1)S(1)} %get-tuple-element.34), channel_id=1, source_target_pairs={{0,1},{1,0},{2,3},{3,2},{4,5},{5,4},{6,7},{7,6},{8,9},{9,8},{10,11... | collective-permute-start | bytes 786440 | tf_op jit(solution)/shard_map/ppermute | solution.py:31
  121.0 3.0 %collective-permute-start.6 = (bf16[128,512]{1,0:T(8,128)(2,1)}, bf16[128,512]{1,0:T(8,128)(2,1)}, u32[]{:S(2)}, u32[]{:S(2)}) collective-permute-start(bf16[128,512]{1,0:T(8,128)(2,1)} %get-tuple-element.27), channel_id=1, source_target_pairs={{0,3},{1,2},{2,1},{3,0},{4,7},{5,6},{6,5},{7,4},{8,11},{9,10},{10,... | collective-permute-start | bytes 393224 | tf_op jit(solution)/shard_map/ppermute | solution.py:31
  123.9 4.1 %collective-permute-start.9 = (bf16[128,512]{1,0:T(8,128)(2,1)S(1)}, bf16[128,512]{1,0:T(8,128)(2,1)}, u32[]{:S(2)}, u32[]{:S(2)}) collective-permute-start(bf16[128,512]{1,0:T(8,128)(2,1)S(1)} %get-tuple-element.21), channel_id=1, source_target_pairs={{0,3},{1,2},{2,1},{3,0},{4,7},{5,6},{6,5},{7,4},{8,11},{9,10},{10,... | collective-permute-start | bytes 393224 | tf_op jit(solution)/shard_map/ppermute | solution.py:31
  128.0 3.5 %all-to-all-start.6 = ((bf16[4,32,2048]{2,1,0:T(8,128)(2,1)}), bf16[4,32,2048]{2,1,0:T(8,128)(2,1)S(1)}, u32[]{:S(2)}, u32[]{:S(2)}) async-start(bf16[4,32,2048]{2,1,0:T(8,128)(2,1)} %get-tuple-element.18), calls=%async_computation.6 | async-start | bytes 1048576 | tf_op jit(solution)/shard_map/all_to_all | solution.py:23
  131.5 2.0 %collective-permute-start.8 = (bf16[128,1024]{1,0:T(8,128)(2,1)}, bf16[128,1024]{1,0:T(8,128)(2,1)S(1)}, u32[]{:S(2)}, u32[]{:S(2)}) collective-permute-start(bf16[128,1024]{1,0:T(8,128)(2,1)} %get-tuple-element.33), channel_id=1, source_target_pairs={{0,2},{1,3},{2,0},{3,1},{4,6},{5,7},{6,4},{7,5},{8,10},{9,11},{10,... | collective-permute-start | bytes 786440 | tf_op jit(solution)/shard_map/ppermute | solution.py:31
  135.2 4.4 %all-to-all-done.6 = bf16[4,32,2048]{2,1,0:T(8,128)(2,1)S(1)} async-done(((bf16[4,32,2048]{2,1,0:T(8,128)(2,1)}), bf16[4,32,2048]{2,1,0:T(8,128)(2,1)S(1)}, u32[]{:S(2)}, u32[]{:S(2)}) %all-to-all-start.6) | async-done | bytes 524320 | tf_op jit(solution)/shard_map/all_to_all | solution.py:23
  140.4 3.5 %all-to-all-start.7 = ((bf16[16,2,2048]{2,1,0:T(2,128)(2,1)}), bf16[16,2,2048]{2,1,0:T(2,128)(2,1)S(1)}, u32[]{:S(2)}, u32[]{:S(2)}) async-start(bf16[16,2,2048]{2,1,0:T(2,128)(2,1)} %reshape.119), calls=%async_computation.7 | async-start | bytes 262144 | tf_op jit(solution)/shard_map/all_to_all | solution.py:23
  144.9 1.1 fusion.19
  146.3 1.9 %collective-permute-start.10 = (f32[512,256]{1,0:T(8,128)S(1)}, f32[512,256]{1,0:T(8,128)S(1)}, u32[]{:S(2)}, u32[]{:S(2)}) collective-permute-start(f32[512,256]{1,0:T(8,128)S(1)} %fusion.1), channel_id=1, source_target_pairs={{0,4},{4,0},{1,5},{5,1},{2,6},{6,2},{3,7},{7,3},{8,12},{12,8},{9,1... | collective-permute-start | bytes 1572872 | tf_op jit(solution)/shard_map/ppermute | solution.py:31
  149.6 7.5 %all-to-all-done.7.row_ref = bf16[16,2,2048]{2,1,0:T(2,128)(2,1)S(1)} async-done(((bf16[16,2,2048]{2,1,0:T(2,128)(2,1)}), bf16[16,2,2048]{2,1,0:T(2,128)(2,1)S(1)}, u32[]{:S(2)}, u32[]{:S(2)}) %all-to-all-start.7) | async-done | bytes 131104 | tf_op jit(solution)/shard_map/all_to_all | solution.py:23
  (76 shorter events, 15.1 us)
Async XLA Ops:
  0.6 0.8 copy-start.4
  2.2 15.3 %copy-start.2 = (bf16[5632,16]{0,1:T(8,128)(2,1)S(1)}, bf16[5632,16]{0,1:T(8,128)(2,1)}, u32[]{:S(2)}) copy-start(bf16[5632,16]{0,1:T(8,128)(2,1)} %param.10) | copy-start | bytes 540676
  2.2 39.1 %all-to-all-start = ((bf16[16,48,256]{2,1,0:T(8,128)(2,1)}), bf16[16,48,256]{2,1,0:T(8,128)(2,1)S(1)}, u32[]{:S(2)}, u32[]{:S(2)}) async-start(bf16[16,48,256]{2,1,0:T(8,128)(2,1)} %pad_add_fusion), calls=%async_computation | async-start | bytes 786432 | tf_op jit(solution)/shard_map/all_to_all | solution.py:23
  19.7 3.2 %collective-permute-start = (bf16[1,4,16,768]{3,2,1,0:T(8,128)(2,1)S(1)}, bf16[1,4,16,768]{3,2,1,0:T(8,128)(2,1)S(1)}, u32[]{:S(2)}, u32[]{:S(2)}) collective-permute-start(bf16[1,4,16,768]{3,2,1,0:T(8,128)(2,1)S(1)} %dynamic-slice_bitcast_fusion), channel_id=1, source_target_pairs={{0,4},{4,0},{1,5},{5,1},{2,6},{6,2},{3,7},{7,3},{8,12},{12,8},{9,1... | collective-permute-start | bytes 294920 | tf_op jit(solution)/shard_map/ppermute | solution.py:31
  23.0 10.5 %collective-permute-start.1 = (bf16[1,2,16,768]{3,2,1,0:T(8,128)(2,1)S(1)}, bf16[1,2,16,768]{3,2,1,0:T(8,128)(2,1)S(1)}, u32[]{:S(2)}, u32[]{:S(2)}) collective-permute-start(bf16[1,2,16,768]{3,2,1,0:T(8,128)(2,1)S(1)} %get-tuple-element.31), channel_id=1, source_target_pairs={{0,8},{8,0},{16,24},{24,16},{1,9},{9,1},{17,25},{25,17},{2,10},{10... | collective-permute-start | bytes 147464 | tf_op jit(solution)/shard_map/ppermute | solution.py:31
  26.4 7.5 %collective-permute-start.2 = (bf16[1,2,16,768]{3,2,1,0:T(8,128)(2,1)S(1)}, bf16[1,2,16,768]{3,2,1,0:T(8,128)(2,1)S(1)}, u32[]{:S(2)}, u32[]{:S(2)}) collective-permute-start(bf16[1,2,16,768]{3,2,1,0:T(8,128)(2,1)S(1)} %get-tuple-element.32), channel_id=1, source_target_pairs={{0,16},{8,24},{16,0},{24,8},{1,17},{9,25},{17,1},{25,9},{2,18},{10... | collective-permute-start | bytes 147464 | tf_op jit(solution)/shard_map/ppermute | solution.py:31
  31.0 7.2 %collective-permute-start.3 = (bf16[1,2,16,768]{3,2,1,0:T(8,128)(2,1)S(1)}, bf16[1,2,16,768]{3,2,1,0:T(8,128)(2,1)S(1)}, u32[]{:S(2)}, u32[]{:S(2)}) collective-permute-start(bf16[1,2,16,768]{3,2,1,0:T(8,128)(2,1)S(1)} %get-tuple-element.30), channel_id=1, source_target_pairs={{0,24},{8,16},{16,8},{24,0},{1,25},{9,17},{17,9},{25,1},{2,26},{10... | collective-permute-start | bytes 147464 | tf_op jit(solution)/shard_map/ppermute | solution.py:31
  33.4 7.9 %copy-start.3 = (bf16[256,256]{1,0:T(8,128)(2,1)S(1)}, bf16[256,256]{1,0:T(8,128)(2,1)}, u32[]{:S(2)}) copy-start(bf16[256,256]{1,0:T(8,128)(2,1)} %constant.107.clone) | copy-start | bytes 393220
  41.3 18.8 %copy-start = (bf16[2048,256]{1,0:T(8,128)(2,1)S(1)}, bf16[2048,256]{1,0:T(8,128)(2,1)}, u32[]{:S(2)}) copy-start(bf16[2048,256]{1,0:T(8,128)(2,1)} %own_ref.3) | copy-start | bytes 3145732
  52.8 21.7 %all-to-all-start.2 = ((bf16[16,32,128]{2,1,0:T(8,128)(2,1)}), bf16[16,32,128]{2,1,0:T(8,128)(2,1)S(1)}, u32[]{:S(2)}, u32[]{:S(2)}) async-start(bf16[16,32,128]{2,1,0:T(8,128)(2,1)} %broadcast_in_dim.26), calls=%async_computation.2 | async-start | bytes 262144 | tf_op jit(solution)/shard_map/all_to_all | solution.py:23
  60.1 1.9 %copy-start.6 = (f32[256]{0:T(256)S(1)}, f32[256]{0:T(256)}, u32[]{:S(2)}) copy-start(f32[256]{0:T(256)} %param.13) | copy-start | bytes 3076
  60.1 20.3 %collective-permute-start.4 = (bf16[2048,256]{1,0:T(8,128)(2,1)S(1)}, bf16[2048,256]{1,0:T(8,128)(2,1)S(1)}, u32[]{:S(2)}, u32[]{:S(2)}) collective-permute-start(bf16[2048,256]{1,0:T(8,128)(2,1)S(1)} %copy-done), channel_id=1, source_target_pairs={{0,4},{4,0},{1,5},{5,1},{2,6},{6,2},{3,7},{7,3},{8,12},{12,8},{9,1... | collective-permute-start | bytes 3145736 | tf_op jit(solution)/shard_map/ppermute | solution.py:31
  62.0 18.3 %collective-permute-start.5 = (f32[2,128]{1,0:T(2,128)S(1)}, f32[2,128]{1,0:T(2,128)S(1)}, u32[]{:S(2)}, u32[]{:S(2)}) collective-permute-start(f32[2,128]{1,0:T(2,128)S(1)} %bitcast.84), channel_id=1, source_target_pairs={{0,4},{4,0},{1,5},{5,1},{2,6},{6,2},{3,7},{7,3},{8,12},{12,8},{9,1... | collective-permute-start | bytes 3080 | tf_op jit(solution)/shard_map/ppermute | solution.py:31
  64.5 10.2 %copy-start.1 = (f32[2048]{0:T(1024)S(1)}, f32[2048]{0:T(1024)}, u32[]{:S(2)}) copy-start(f32[2048]{0:T(1024)} %param.11) | copy-start | bytes 24580
  75.6 11.5 %all-to-all-start.3 = ((bf16[4,32,2048]{2,1,0:T(8,128)(2,1)}), bf16[4,32,2048]{2,1,0:T(8,128)(2,1)S(1)}, u32[]{:S(2)}, u32[]{:S(2)}) async-start(bf16[4,32,2048]{2,1,0:T(8,128)(2,1)} %broadcast_in_dim.27), calls=%async_computation.3 | async-start | bytes 1048576 | tf_op jit(solution)/shard_map/all_to_all | solution.py:23
  79.1 0.7 copy-start.5
  89.0 8.5 %all-to-all-start.4 = ((f32[4,2,128]{2,1,0:T(2,128)}), f32[4,2,128]{2,1,0:T(2,128)S(1)}, u32[]{:S(2)}, u32[]{:S(2)}) async-start(f32[4,2,128]{2,1,0:T(2,128)} %get-tuple-element.15), calls=%async_computation.4 | async-start | bytes 8192 | tf_op jit(solution)/shard_map/all_to_all | solution.py:23
  98.2 17.1 %all-to-all-start.5 = ((f32[16,2,128]{2,1,0:T(2,128)}), f32[16,2,128]{2,1,0:T(2,128)S(1)}, u32[]{:S(2)}, u32[]{:S(2)}) async-start(f32[16,2,128]{2,1,0:T(2,128)} %broadcast_in_dim.51), calls=%async_computation.5 | async-start | bytes 32768 | tf_op jit(solution)/shard_map/all_to_all | solution.py:23
  118.3 15.8 %collective-permute-start.7 = (bf16[128,1024]{1,0:T(8,128)(2,1)S(1)}, bf16[128,1024]{1,0:T(8,128)(2,1)S(1)}, u32[]{:S(2)}, u32[]{:S(2)}) collective-permute-start(bf16[128,1024]{1,0:T(8,128)(2,1)S(1)} %get-tuple-element.34), channel_id=1, source_target_pairs={{0,1},{1,0},{2,3},{3,2},{4,5},{5,4},{6,7},{7,6},{8,9},{9,8},{10,11... | collective-permute-start | bytes 786440 | tf_op jit(solution)/shard_map/ppermute | solution.py:31
  121.0 18.7 %collective-permute-start.6 = (bf16[128,512]{1,0:T(8,128)(2,1)}, bf16[128,512]{1,0:T(8,128)(2,1)}, u32[]{:S(2)}, u32[]{:S(2)}) collective-permute-start(bf16[128,512]{1,0:T(8,128)(2,1)} %get-tuple-element.27), channel_id=1, source_target_pairs={{0,3},{1,2},{2,1},{3,0},{4,7},{5,6},{6,5},{7,4},{8,11},{9,10},{10,... | collective-permute-start | bytes 393224 | tf_op jit(solution)/shard_map/ppermute | solution.py:31
  123.9 20.9 %collective-permute-start.9 = (bf16[128,512]{1,0:T(8,128)(2,1)S(1)}, bf16[128,512]{1,0:T(8,128)(2,1)}, u32[]{:S(2)}, u32[]{:S(2)}) collective-permute-start(bf16[128,512]{1,0:T(8,128)(2,1)S(1)} %get-tuple-element.21), channel_id=1, source_target_pairs={{0,3},{1,2},{2,1},{3,0},{4,7},{5,6},{6,5},{7,4},{8,11},{9,10},{10,... | collective-permute-start | bytes 393224 | tf_op jit(solution)/shard_map/ppermute | solution.py:31
  128.0 11.5 %all-to-all-start.6 = ((bf16[4,32,2048]{2,1,0:T(8,128)(2,1)}), bf16[4,32,2048]{2,1,0:T(8,128)(2,1)S(1)}, u32[]{:S(2)}, u32[]{:S(2)}) async-start(bf16[4,32,2048]{2,1,0:T(8,128)(2,1)} %get-tuple-element.18), calls=%async_computation.6 | async-start | bytes 1048576 | tf_op jit(solution)/shard_map/all_to_all | solution.py:23
  131.5 14.5 %collective-permute-start.8 = (bf16[128,1024]{1,0:T(8,128)(2,1)}, bf16[128,1024]{1,0:T(8,128)(2,1)S(1)}, u32[]{:S(2)}, u32[]{:S(2)}) collective-permute-start(bf16[128,1024]{1,0:T(8,128)(2,1)} %get-tuple-element.33), channel_id=1, source_target_pairs={{0,2},{1,3},{2,0},{3,1},{4,6},{5,7},{6,4},{7,5},{8,10},{9,11},{10,... | collective-permute-start | bytes 786440 | tf_op jit(solution)/shard_map/ppermute | solution.py:31
  140.4 16.7 %all-to-all-start.7 = ((bf16[16,2,2048]{2,1,0:T(2,128)(2,1)}), bf16[16,2,2048]{2,1,0:T(2,128)(2,1)S(1)}, u32[]{:S(2)}, u32[]{:S(2)}) async-start(bf16[16,2,2048]{2,1,0:T(2,128)(2,1)} %reshape.119), calls=%async_computation.7 | async-start | bytes 262144 | tf_op jit(solution)/shard_map/all_to_all | solution.py:23
  146.3 11.7 %collective-permute-start.10 = (f32[512,256]{1,0:T(8,128)S(1)}, f32[512,256]{1,0:T(8,128)S(1)}, u32[]{:S(2)}, u32[]{:S(2)}) collective-permute-start(f32[512,256]{1,0:T(8,128)S(1)} %fusion.1), channel_id=1, source_target_pairs={{0,4},{4,0},{1,5},{5,1},{2,6},{6,2},{3,7},{7,3},{8,12},{12,8},{9,1... | collective-permute-start | bytes 1572872 | tf_op jit(solution)/shard_map/ppermute | solution.py:31
